TPU v7x, 512 devices: a whole 4x8x8 slice. The times are simulated.
512 devices in a mesh: tp: 32 (over z, x), dp: 16 (over y, core).
Axes of the slice: x: 4, y: 8, z: 8, core: 2. Of those that a mesh axis runs over, the one named last changes fastest.
Arguments:
- tokens: bfloat16 [256, 4096], P(None, 'dp'), may hold values from -6 to 6
- recurrent_state: float32 [2, 256, 262144], P(None, 'dp', 'tp'), may hold values from -24 to 24
- pre_gain: float32 [2, 4096], P(None, 'dp'), may hold values from 0.1 to 1.9
- w_query: bfloat16 [2, 4096, 2048], P(None, 'dp', 'tp'), may hold values from -0.09375 to 0.09375
- w_key: bfloat16 [2, 4096, 2048], P(None, 'dp', 'tp'), may hold values from -0.09375 to 0.09375
- w_value: bfloat16 [2, 4096, 4096], P(None, 'dp', 'tp'), may hold values from -0.09375 to 0.09375
- w_gate: bfloat16 [2, 4096, 4096], P(None, 'dp', 'tp'), may hold values from -0.09375 to 0.09375
- w_decay: bfloat16 [2, 4096, 2048], P(None, 'dp', 'tp'), may hold values from -1 to 1
- decay_bias: float32 [2, 2048], P(None, 'tp'), may hold values from -5 to 3
- head_gain: float32 [2, 128], replicated, may hold values from 0.1 to 1.9
- w_out: bfloat16 [2, 4096, 4096], P(None, 'tp', 'dp'), may hold values from -0.09375 to 0.09375
- post_gain: float32 [2, 4096], P(None, 'dp'), may hold values from 0.1 to 1.9
Outputs:
- hidden_out: bfloat16 [256, 4096], P(None, 'dp')
- state_out: float32 [2, 256, 262144], P(None, 'dp', 'tp')
All inputs are finite; a program needn't handle non-finite values.
Results may differ from a plain program's by a relative error of at most 0.015.
Values may be sent and summed in bfloat16 or wider, within the bound.
No kernel may reach another device: no remote copies, remote signals or barrier semaphores. Data moves between devices by JAX's collectives and lax.ppermute only.
A program may use at most 64 MiB of HBM per device.

v0:
```python
import jax
import jax.numpy as jnp
from jax import lax
from jax.sharding import PartitionSpec as P

D = 4096
KEY = 64
VAL = 128


epsilon = 1e-06


def split_up(array, dim, size):
    before, after = (array.shape[:dim], array.shape[dim + 1 :])
    return jnp.moveaxis(array.reshape(*before, size, -1, *after), dim, 0)


def summed_on_arrival(array, axis, dim):
    size = lax.axis_size(axis)
    tiles = lax.all_to_all(split_up(array, dim, size), axis, 0, 0, tiled=True)
    return jnp.sum(tiles, axis=0)


def sent_to_all(array, axis):
    size = lax.axis_size(axis)
    return lax.all_to_all(
        jnp.broadcast_to(array[None], (size, *array.shape)), axis, 0, 0, tiled=True
    )


def laid_out(tiles, dim):
    tiles = jnp.moveaxis(tiles, 0, dim)
    shape = tiles.shape
    return tiles.reshape(*shape[:dim], shape[dim] * shape[dim + 1], *shape[dim + 2 :])


def gathered_copies(array, axis, dim):
    tiles = sent_to_all(array, axis)
    return laid_out(tiles, dim)


def sum_at_owner(array, axis, dim):
    tiles = split_up(array, dim, lax.axis_size(axis))
    arrived = lax.all_to_all(tiles, axis, split_axis=0, concat_axis=0, tiled=True)
    return arrived.astype(jnp.float32).sum(axis=0)


def over_copies(array, axis):
    return sent_to_all(array, axis).sum(axis=0)


def local(
    tokens,
    recurrent_state,
    pre_gain,
    w_query,
    w_key,
    w_value,
    w_gate,
    w_decay,
    decay_bias,
    head_gain,
    w_out,
    post_gain,
):
    column_count = lax.axis_size("tp")
    column_rank = lax.axis_index("tp")
    seq_all = tokens.shape[0]
    local_seqs = recurrent_state.shape[1]
    value_cols = recurrent_state.shape[2] // KEY
    heads_here = value_cols // VAL
    highest = lax.Precision.HIGHEST
    spread = (
        jnp.arange(value_cols, dtype=jnp.int32)[None, :] // VAL
        == jnp.arange(heads_here, dtype=jnp.int32)[:, None]
    ).astype(jnp.float32)

    def spread_heads(vectors):
        shaped = vectors.astype(jnp.float32).reshape(local_seqs, heads_here, KEY)
        return jnp.einsum("bhk,hc->bck", shaped, spread, precision=highest)

    residual = tokens
    new_states = []
    for section_index in range(2):
        wide_float = residual.astype(jnp.float32)
        squares_part = jnp.sum(wide_float * wide_float, axis=1)
        normed = (wide_float * pre_gain[section_index]).astype(jnp.bfloat16)
        partials = tuple(
            (
                jnp.dot(normed, weights[section_index], preferred_element_type=jnp.float32)
                for weights in (w_query, w_key, w_value, w_gate, w_decay)
            )
        )
        summed = jax.tree.map(
            lambda part: summed_on_arrival(part, "dp", 0), partials + (squares_part,)
        )
        projected = summed[:5]
        own_squares = summed[5]
        row_scale = lax.rsqrt(own_squares / D + epsilon)[:, None]
        query_part = (projected[0] * row_scale).astype(jnp.bfloat16)
        key_part = (projected[1] * row_scale).astype(jnp.bfloat16)
        values_own = projected[2] * row_scale
        gate_pre = projected[3] * row_scale
        log_decay = jax.nn.log_sigmoid(projected[4] * row_scale + decay_bias[section_index]) / 16.0
        query_cols = spread_heads(query_part)
        key_cols = spread_heads(key_part)
        decay_cols = jnp.exp(spread_heads(log_decay))
        old_state = recurrent_state[section_index].reshape(local_seqs, value_cols, KEY)
        new_state = decay_cols * old_state + key_cols * values_own[:, :, None]
        readout = jnp.sum(query_cols * new_state, axis=2) * KEY ** (-0.5)
        head_mean = jnp.mean(
            (readout * readout).reshape(local_seqs, heads_here, VAL), axis=2, keepdims=True
        )
        scaled = (
            readout.reshape(local_seqs, heads_here, VAL)
            * lax.rsqrt(head_mean + epsilon)
            * head_gain[section_index]
        )
        mixed = (scaled.reshape(local_seqs, value_cols) * jax.nn.silu(gate_pre)).astype(
            jnp.bfloat16
        )
        out_weight = w_out[section_index]
        gathered = gathered_copies(mixed, "dp", 0)
        share_rows = seq_all // column_count
        out_rows = sum_at_owner(
            jnp.dot(gathered, out_weight, preferred_element_type=jnp.float32).astype(jnp.bfloat16),
            "tp",
            0,
        )
        out_squares = over_copies(jnp.sum(out_rows * out_rows, axis=1), "dp")
        own_rows = lax.dynamic_slice_in_dim(
            residual, column_rank * share_rows, share_rows, 0
        ).astype(jnp.float32)
        updated = (
            own_rows
            + out_rows * lax.rsqrt(out_squares / D + epsilon)[:, None] * post_gain[section_index]
        ).astype(jnp.bfloat16)
        residual = gathered_copies(updated, "tp", 0)
        new_states.append(new_state.reshape(local_seqs, value_cols * KEY))
    return (residual, jnp.stack(new_states))


def solution(mesh):
    in_specs = (
        P(None, "dp"),
        P(None, "dp", "tp"),
        P(None, "dp"),
        P(None, "dp", "tp"),
        P(None, "dp", "tp"),
        P(None, "dp", "tp"),
        P(None, "dp", "tp"),
        P(None, "dp", "tp"),
        P(None, "tp"),
        P(),
        P(None, "tp", "dp"),
        P(None, "dp"),
    )
    out_specs = (P(None, "dp"), P(None, "dp", "tp"))
    return jax.shard_map(local, mesh=mesh, in_specs=in_specs, out_specs=out_specs, check_vma=False)
```

profile of v0, /device:TPU:1, one launch (start us, length us, event | category | flops | bytes accessed | tf_op | source)
XLA Modules:
  0.0 265.5 jit_solution(10752713642527964072)
XLA Ops:
  0.6 0.8 fusion.71
  1.4 1.0 fusion.7
  2.5 0.7 all_to_all.69
  3.1 10.1 %all-to-all-start.1 = ((f32[16,1,16]{2,1,0:T(1,128)}), f32[16,1,16]{2,1,0:T(1,128)S(1)}, u32[]{:S(2)}, u32[]{:S(2)}) async-start(f32[16,1,16]{2,1,0:T(1,128)} %all_to_all.69), calls=%async_computation.1 | async-start | bytes 16384 | tf_op jit(solution)/shard_map/all_to_all | solution.py:21
  13.2 1.7 fusion.16
  14.9 0.9 fusion.32
  15.8 0.9 fusion.34
  16.9 0.8 copy-done.7
  17.8 0.8 reshape.815
  18.5 0.7 reshape.817
  19.3 0.7 reshape.819
  20.3 7.0 %all-to-all-start.3 = ((f32[16,1,1024]{2,1,0:T(1,128)}), f32[16,1,1024]{2,1,0:T(1,128)S(1)}, u32[]{:S(2)}, u32[]{:S(2)}) async-start(f32[16,1,1024]{2,1,0:T(1,128)} %reshape.815), calls=%async_computation.3 | async-start | bytes 131072 | tf_op jit(solution)/shard_map/all_to_all | solution.py:21
  27.3 0.8 fusion.18
  28.1 6.9 %all-to-all-done.3 = f32[16,1,1024]{2,1,0:T(1,128)S(1)} async-done(((f32[16,1,1024]{2,1,0:T(1,128)}), f32[16,1,1024]{2,1,0:T(1,128)S(1)}, u32[]{:S(2)}, u32[]{:S(2)}) %all-to-all-start.3) | async-done | bytes 65568 | tf_op jit(solution)/shard_map/all_to_all | solution.py:21
  35.1 3.4 %all-to-all-start = ((f32[16,1,1024]{2,1,0:T(1,128)}), f32[16,1,1024]{2,1,0:T(1,128)S(1)}, u32[]{:S(2)}, u32[]{:S(2)}) async-start(f32[16,1,1024]{2,1,0:T(1,128)} %reshape.819), calls=%async_computation | async-start | bytes 131072 | tf_op jit(solution)/shard_map/all_to_all | solution.py:21
  38.5 7.8 %all-to-all-done = f32[16,1,1024]{2,1,0:T(1,128)S(1)} async-done(((f32[16,1,1024]{2,1,0:T(1,128)}), f32[16,1,1024]{2,1,0:T(1,128)S(1)}, u32[]{:S(2)}, u32[]{:S(2)}) %all-to-all-start) | async-done | bytes 65568 | tf_op jit(solution)/shard_map/all_to_all | solution.py:21
  46.3 3.4 %all-to-all-start.2 = ((f32[16,1,1024]{2,1,0:T(1,128)}), f32[16,1,1024]{2,1,0:T(1,128)S(1)}, u32[]{:S(2)}, u32[]{:S(2)}) async-start(f32[16,1,1024]{2,1,0:T(1,128)} %reshape.817), calls=%async_computation.2 | async-start | bytes 131072 | tf_op jit(solution)/shard_map/all_to_all | solution.py:21
  50.7 6.8 %all-to-all-done.2 = f32[16,1,1024]{2,1,0:T(1,128)S(1)} async-done(((f32[16,1,1024]{2,1,0:T(1,128)}), f32[16,1,1024]{2,1,0:T(1,128)S(1)}, u32[]{:S(2)}, u32[]{:S(2)}) %all-to-all-start.2) | async-done | bytes 65568 | tf_op jit(solution)/shard_map/all_to_all | solution.py:21
  57.6 3.5 %all-to-all-start.4 = ((f32[16,16,128]{2,1,0:T(8,128)}), f32[16,16,128]{2,1,0:T(8,128)S(1)}, u32[]{:S(2)}, u32[]{:S(2)}) async-start(f32[16,16,128]{2,1,0:T(8,128)} %fusion.18), calls=%async_computation.4 | async-start | bytes 262144 | tf_op jit(solution)/shard_map/all_to_all | solution.py:21
  61.6 0.8 reduce.8
  62.6 0.8 reduce.7
  63.5 0.8 reduce.9
  64.6 5.6 %all-to-all-done.4 = f32[16,16,128]{2,1,0:T(8,128)S(1)} async-done(((f32[16,16,128]{2,1,0:T(8,128)}), f32[16,16,128]{2,1,0:T(8,128)S(1)}, u32[]{:S(2)}, u32[]{:S(2)}) %all-to-all-start.4) | async-done | bytes 131104 | tf_op jit(solution)/shard_map/all_to_all | solution.py:21
  70.2 3.4 %all-to-all-start.5 = ((f32[16,16,128]{2,1,0:T(8,128)}), f32[16,16,128]{2,1,0:T(8,128)S(1)}, u32[]{:S(2)}, u32[]{:S(2)}) async-start(f32[16,16,128]{2,1,0:T(8,128)} %fusion.16), calls=%async_computation.5 | async-start | bytes 262144 | tf_op jit(solution)/shard_map/all_to_all | solution.py:21
  73.7 0.7 fusion.5
  74.6 7.5 %all-to-all-done.5 = f32[16,16,128]{2,1,0:T(8,128)S(1)} async-done(((f32[16,16,128]{2,1,0:T(8,128)}), f32[16,16,128]{2,1,0:T(8,128)S(1)}, u32[]{:S(2)}, u32[]{:S(2)}) %all-to-all-start.5) | async-done | bytes 131104 | tf_op jit(solution)/shard_map/all_to_all | solution.py:21
  82.2 10.5 %all_to_all.110 = bf16[16,16,128]{2,1,0:T(8,128)(2,1)S(1)} all-to-all(bf16[16,16,128]{2,1,0:T(8,128)(2,1)S(1)} %broadcast_in_dim.12), channel_id=1, replica_groups=mesh['tp'=32,'dp'=16] {'dp'}, dimensions={0} | all-to-all | bytes 131072 | tf_op jit(solution)/shard_map/all_to_all | solution.py:27
  92.8 21.0 %all_to_all.111 = bf16[32,8,256]{2,1,0:T(8,128)(2,1)S(1)} all-to-all(bf16[32,8,256]{2,1,0:T(8,128)(2,1)S(1)} %fusion), channel_id=1, replica_groups=mesh['tp'=32,'dp'=16] {'tp'}, dimensions={0} | all-to-all | bytes 262144 | tf_op jit(solution)/shard_map/all_to_all | solution.py:45
  114.6 4.9 %all-to-all-start.8 = ((f32[16,1,8]{2,1,0:T(1,128)}), f32[16,1,8]{2,1,0:T(1,128)S(1)}, u32[]{:S(2)}, u32[]{:S(2)}) async-start(f32[16,1,8]{2,1,0:T(1,128)} %broadcast_in_dim.13), calls=%async_computation.8 | async-start | bytes 16384 | tf_op jit(solution)/shard_map/all_to_all | solution.py:27
  120.1 6.5 %all-to-all-done.8 = f32[16,1,8]{2,1,0:T(1,128)S(1)} async-done(((f32[16,1,8]{2,1,0:T(1,128)}), f32[16,1,8]{2,1,0:T(1,128)S(1)}, u32[]{:S(2)}, u32[]{:S(2)}) %all-to-all-start.8) | async-done | bytes 544 | tf_op jit(solution)/shard_map/all_to_all | solution.py:27
  126.6 0.8 add_convert_fusion.1
  128.0 3.9 %all-to-all-start.9 = ((bf16[32,8,256]{2,1,0:T(8,128)(2,1)}), bf16[32,8,256]{2,1,0:T(8,128)(2,1)S(1)}, u32[]{:S(2)}, u32[]{:S(2)}) async-start(bf16[32,8,256]{2,1,0:T(8,128)(2,1)} %broadcast_in_dim.14), calls=%async_computation.9 | async-start | bytes 262144 | tf_op jit(solution)/shard_map/all_to_all | solution.py:27
  132.3 9.0 %all-to-all-done.9 = bf16[32,8,256]{2,1,0:T(8,128)(2,1)S(1)} async-done(((bf16[32,8,256]{2,1,0:T(8,128)(2,1)}), bf16[32,8,256]{2,1,0:T(8,128)(2,1)S(1)}, u32[]{:S(2)}, u32[]{:S(2)}) %all-to-all-start.9) | async-done | bytes 131104 | tf_op jit(solution)/shard_map/all_to_all | solution.py:27
  141.4 0.7 all_to_all.80
  142.1 5.3 %all-to-all-start.11 = ((f32[16,1,16]{2,1,0:T(1,128)}), f32[16,1,16]{2,1,0:T(1,128)S(1)}, u32[]{:S(2)}, u32[]{:S(2)}) async-start(f32[16,1,16]{2,1,0:T(1,128)} %bitcast.35), calls=%async_computation.11 | async-start | bytes 16384 | tf_op jit(solution)/shard_map/all_to_all | solution.py:21
  147.6 0.7 copy-done.6
  148.4 0.8 reshape.821
  149.2 0.7 reshape.823
  150.0 4.5 %all-to-all-done.11 = f32[16,1,16]{2,1,0:T(1,128)S(1)} async-done(((f32[16,1,16]{2,1,0:T(1,128)}), f32[16,1,16]{2,1,0:T(1,128)S(1)}, u32[]{:S(2)}, u32[]{:S(2)}) %all-to-all-start.11) | async-done | bytes 1056 | tf_op jit(solution)/shard_map/all_to_all | solution.py:21
  154.4 4.0 %all-to-all-start.13 = ((f32[16,1,1024]{2,1,0:T(1,128)}), f32[16,1,1024]{2,1,0:T(1,128)S(1)}, u32[]{:S(2)}, u32[]{:S(2)}) async-start(f32[16,1,1024]{2,1,0:T(1,128)} %reshape.821), calls=%async_computation.13 | async-start | bytes 131072 | tf_op jit(solution)/shard_map/all_to_all | solution.py:21
  158.6 0.8 reshape.825
  159.3 6.9 %all-to-all-done.13 = f32[16,1,1024]{2,1,0:T(1,128)S(1)} async-done(((f32[16,1,1024]{2,1,0:T(1,128)}), f32[16,1,1024]{2,1,0:T(1,128)S(1)}, u32[]{:S(2)}, u32[]{:S(2)}) %all-to-all-start.13) | async-done | bytes 65568 | tf_op jit(solution)/shard_map/all_to_all | solution.py:21
  166.2 3.5 %all-to-all-start.10 = ((f32[16,1,1024]{2,1,0:T(1,128)}), f32[16,1,1024]{2,1,0:T(1,128)S(1)}, u32[]{:S(2)}, u32[]{:S(2)}) async-start(f32[16,1,1024]{2,1,0:T(1,128)} %reshape.825), calls=%async_computation.10 | async-start | bytes 131072 | tf_op jit(solution)/shard_map/all_to_all | solution.py:21
  169.7 0.8 fusion.11
  170.5 7.0 %all-to-all-done.10 = f32[16,1,1024]{2,1,0:T(1,128)S(1)} async-done(((f32[16,1,1024]{2,1,0:T(1,128)}), f32[16,1,1024]{2,1,0:T(1,128)S(1)}, u32[]{:S(2)}, u32[]{:S(2)}) %all-to-all-start.10) | async-done | bytes 65568 | tf_op jit(solution)/shard_map/all_to_all | solution.py:21
  177.5 3.4 %all-to-all-start.12 = ((f32[16,1,1024]{2,1,0:T(1,128)}), f32[16,1,1024]{2,1,0:T(1,128)S(1)}, u32[]{:S(2)}, u32[]{:S(2)}) async-start(f32[16,1,1024]{2,1,0:T(1,128)} %reshape.823), calls=%async_computation.12 | async-start | bytes 131072 | tf_op jit(solution)/shard_map/all_to_all | solution.py:21
  180.9 0.8 fusion.13
  181.8 7.0 %all-to-all-done.12 = f32[16,1,1024]{2,1,0:T(1,128)S(1)} async-done(((f32[16,1,1024]{2,1,0:T(1,128)}), f32[16,1,1024]{2,1,0:T(1,128)S(1)}, u32[]{:S(2)}, u32[]{:S(2)}) %all-to-all-start.12) | async-done | bytes 65568 | tf_op jit(solution)/shard_map/all_to_all | solution.py:21
  188.8 3.5 %all-to-all-start.14 = ((f32[16,16,128]{2,1,0:T(8,128)}), f32[16,16,128]{2,1,0:T(8,128)S(1)}, u32[]{:S(2)}, u32[]{:S(2)}) async-start(f32[16,16,128]{2,1,0:T(8,128)} %fusion.13), calls=%async_computation.14 | async-start | bytes 262144 | tf_op jit(solution)/shard_map/all_to_all | solution.py:21
  192.3 0.8 reduce.11
  193.2 0.8 reduce.10
  194.2 0.8 reduce.12
  195.1 0.7 fusion.49
  195.8 5.6 %all-to-all-done.14 = f32[16,16,128]{2,1,0:T(8,128)S(1)} async-done(((f32[16,16,128]{2,1,0:T(8,128)}), f32[16,16,128]{2,1,0:T(8,128)S(1)}, u32[]{:S(2)}, u32[]{:S(2)}) %all-to-all-start.14) | async-done | bytes 131104 | tf_op jit(solution)/shard_map/all_to_all | solution.py:21
  201.4 3.4 %all-to-all-start.15 = ((f32[16,16,128]{2,1,0:T(8,128)}), f32[16,16,128]{2,1,0:T(8,128)S(1)}, u32[]{:S(2)}, u32[]{:S(2)}) async-start(f32[16,16,128]{2,1,0:T(8,128)} %fusion.11), calls=%async_computation.15 | async-start | bytes 262144 | tf_op jit(solution)/shard_map/all_to_all | solution.py:21
  205.6 0.7 fusion.3
  206.4 6.9 %all-to-all-done.15 = f32[16,16,128]{2,1,0:T(8,128)S(1)} async-done(((f32[16,16,128]{2,1,0:T(8,128)}), f32[16,16,128]{2,1,0:T(8,128)S(1)}, u32[]{:S(2)}, u32[]{:S(2)}) %all-to-all-start.15) | async-done | bytes 131104 | tf_op jit(solution)/shard_map/all_to_all | solution.py:21
  214.0 10.5 %all_to_all.112 = bf16[16,16,128]{2,1,0:T(8,128)(2,1)S(1)} all-to-all(bf16[16,16,128]{2,1,0:T(8,128)(2,1)S(1)} %broadcast_in_dim.15), channel_id=1, replica_groups=mesh['tp'=32,'dp'=16] {'dp'}, dimensions={0} | all-to-all | bytes 131072 | tf_op jit(solution)/shard_map/all_to_all | solution.py:27
  224.6 12.8 %all_to_all.113 = bf16[32,8,256]{2,1,0:T(8,128)(2,1)S(1)} all-to-all(bf16[32,8,256]{2,1,0:T(8,128)(2,1)S(1)} %fusion.1), channel_id=1, replica_groups=mesh['tp'=32,'dp'=16] {'tp'}, dimensions={0} | all-to-all | bytes 262144 | tf_op jit(solution)/shard_map/all_to_all | solution.py:45
  238.2 4.9 %all-to-all-start.18 = ((f32[16,1,8]{2,1,0:T(1,128)}), f32[16,1,8]{2,1,0:T(1,128)S(1)}, u32[]{:S(2)}, u32[]{:S(2)}) async-start(f32[16,1,8]{2,1,0:T(1,128)} %broadcast_in_dim.16), calls=%async_computation.18 | async-start | bytes 16384 | tf_op jit(solution)/shard_map/all_to_all | solution.py:27
  243.8 6.3 %all-to-all-done.18 = f32[16,1,8]{2,1,0:T(1,128)S(1)} async-done(((f32[16,1,8]{2,1,0:T(1,128)}), f32[16,1,8]{2,1,0:T(1,128)S(1)}, u32[]{:S(2)}, u32[]{:S(2)}) %all-to-all-start.18) | async-done | bytes 544 | tf_op jit(solution)/shard_map/all_to_all | solution.py:27
  251.6 3.9 %all-to-all-start.19 = ((bf16[32,8,256]{2,1,0:T(8,128)(2,1)}), bf16[32,8,256]{2,1,0:T(8,128)(2,1)S(1)}, u32[]{:S(2)}, u32[]{:S(2)}) async-start(bf16[32,8,256]{2,1,0:T(8,128)(2,1)} %broadcast_in_dim.17), calls=%async_computation.19 | async-start | bytes 262144 | tf_op jit(solution)/shard_map/all_to_all | solution.py:27
  255.4 1.0 pad_maximum_fusion
  256.5 8.4 %all-to-all-done.19 = bf16[32,8,256]{2,1,0:T(8,128)(2,1)S(1)} async-done(((bf16[32,8,256]{2,1,0:T(8,128)(2,1)}), bf16[32,8,256]{2,1,0:T(8,128)(2,1)S(1)}, u32[]{:S(2)}, u32[]{:S(2)}) %all-to-all-start.19) | async-done | bytes 131104 | tf_op jit(solution)/shard_map/all_to_all | solution.py:27
  (97 shorter events, 11.6 us)
Async XLA Ops:
  0.6 16.1 %copy-start = (f32[2,16,8192]{2,1,0:T(8,128)S(1)}, f32[2,16,8192]{2,1,0:T(8,128)}, u32[]{:S(2)}) copy-start(f32[2,16,8192]{2,1,0:T(8,128)} %param.13) | copy-start | bytes 3145732
  3.1 17.1 %all-to-all-start.1 = ((f32[16,1,16]{2,1,0:T(1,128)}), f32[16,1,16]{2,1,0:T(1,128)S(1)}, u32[]{:S(2)}, u32[]{:S(2)}) async-start(f32[16,1,16]{2,1,0:T(1,128)} %all_to_all.69), calls=%async_computation.1 | async-start | bytes 16384 | tf_op jit(solution)/shard_map/all_to_all | solution.py:21
  16.8 0.8 copy-start.7
  19.3 8.0 %copy-start.2 = (bf16[2,256,128]{2,1,0:T(8,128)(2,1)S(1)}, bf16[2,256,128]{2,1,0:T(8,128)(2,1)}, u32[]{:S(2)}) copy-start(bf16[2,256,128]{2,1,0:T(8,128)(2,1)} %param.17) | copy-start | bytes 393220
  20.3 14.8 %all-to-all-start.3 = ((f32[16,1,1024]{2,1,0:T(1,128)}), f32[16,1,1024]{2,1,0:T(1,128)S(1)}, u32[]{:S(2)}, u32[]{:S(2)}) async-start(f32[16,1,1024]{2,1,0:T(1,128)} %reshape.815), calls=%async_computation.3 | async-start | bytes 131072 | tf_op jit(solution)/shard_map/all_to_all | solution.py:21
  28.1 10.3 %copy-start.16 = (f32[2,64]{1,0:T(2,128)S(1)}, f32[2,64]{1,0:T(2,128)}, u32[]{:S(2)}) copy-start(f32[2,64]{1,0:T(2,128)} %param.20) | copy-start | bytes 1540
  35.1 11.2 %all-to-all-start = ((f32[16,1,1024]{2,1,0:T(1,128)}), f32[16,1,1024]{2,1,0:T(1,128)S(1)}, u32[]{:S(2)}, u32[]{:S(2)}) async-start(f32[16,1,1024]{2,1,0:T(1,128)} %reshape.819), calls=%async_computation | async-start | bytes 131072 | tf_op jit(solution)/shard_map/all_to_all | solution.py:21
  38.5 11.2 %copy-start.17 = (f32[2,128]{1,0:T(2,128)S(1)}, f32[2,128]{1,0:T(2,128)}, u32[]{:S(2)}) copy-start(f32[2,128]{1,0:T(2,128)} %param.21) | copy-start | bytes 3076
  46.3 11.3 %all-to-all-start.2 = ((f32[16,1,1024]{2,1,0:T(1,128)}), f32[16,1,1024]{2,1,0:T(1,128)S(1)}, u32[]{:S(2)}, u32[]{:S(2)}) async-start(f32[16,1,1024]{2,1,0:T(1,128)} %reshape.817), calls=%async_computation.2 | async-start | bytes 131072 | tf_op jit(solution)/shard_map/all_to_all | solution.py:21
  50.7 23.0 %copy-start.12 = (f32[128]{0:T(128)}, f32[128]{0:T(128)S(1)}, u32[]{:S(2)}) copy-start(f32[128]{0:T(128)S(1)} %fusion.66) | copy-start | bytes 1540
  57.6 12.6 %all-to-all-start.4 = ((f32[16,16,128]{2,1,0:T(8,128)}), f32[16,16,128]{2,1,0:T(8,128)S(1)}, u32[]{:S(2)}, u32[]{:S(2)}) async-start(f32[16,16,128]{2,1,0:T(8,128)} %fusion.18), calls=%async_computation.4 | async-start | bytes 262144 | tf_op jit(solution)/shard_map/all_to_all | solution.py:21
  70.2 11.9 %all-to-all-start.5 = ((f32[16,16,128]{2,1,0:T(8,128)}), f32[16,16,128]{2,1,0:T(8,128)S(1)}, u32[]{:S(2)}, u32[]{:S(2)}) async-start(f32[16,16,128]{2,1,0:T(8,128)} %fusion.16), calls=%async_computation.5 | async-start | bytes 262144 | tf_op jit(solution)/shard_map/all_to_all | solution.py:21
  82.1 10.6 %copy-start.3 = (bf16[2,128,256]{2,1,0:T(8,128)(2,1)S(1)}, bf16[2,128,256]{2,1,0:T(8,128)(2,1)}, u32[]{:S(2)}) copy-start(bf16[2,128,256]{2,1,0:T(8,128)(2,1)} %param.22) | copy-start | bytes 393220
  114.6 4.9 %copy-start.14 = (f32[2,256]{1,0:T(2,128)S(1)}, f32[2,256]{1,0:T(2,128)}, u32[]{:S(2)}) copy-start(f32[2,256]{1,0:T(2,128)} %param.23) | copy-start | bytes 6148
  114.6 11.9 %all-to-all-start.8 = ((f32[16,1,8]{2,1,0:T(1,128)}), f32[16,1,8]{2,1,0:T(1,128)S(1)}, u32[]{:S(2)}, u32[]{:S(2)}) async-start(f32[16,1,8]{2,1,0:T(1,128)} %broadcast_in_dim.13), calls=%async_computation.8 | async-start | bytes 16384 | tf_op jit(solution)/shard_map/all_to_all | solution.py:27
  128.0 13.3 %all-to-all-start.9 = ((bf16[32,8,256]{2,1,0:T(8,128)(2,1)}), bf16[32,8,256]{2,1,0:T(8,128)(2,1)S(1)}, u32[]{:S(2)}, u32[]{:S(2)}) async-start(bf16[32,8,256]{2,1,0:T(8,128)(2,1)} %broadcast_in_dim.14), calls=%async_computation.9 | async-start | bytes 262144 | tf_op jit(solution)/shard_map/all_to_all | solution.py:27
  141.3 6.1 %copy-start.5 = (bf16[2,256,64]{1,2,0:T(8,128)(2,1)S(1)}, bf16[2,256,64]{1,2,0:T(8,128)(2,1)}, u32[]{:S(2)}) copy-start(bf16[2,256,64]{1,2,0:T(8,128)(2,1)} %param.16) | copy-start | bytes 196612
  142.1 12.3 %all-to-all-start.11 = ((f32[16,1,16]{2,1,0:T(1,128)}), f32[16,1,16]{2,1,0:T(1,128)S(1)}, u32[]{:S(2)}, u32[]{:S(2)}) async-start(f32[16,1,16]{2,1,0:T(1,128)} %bitcast.35), calls=%async_computation.11 | async-start | bytes 16384 | tf_op jit(solution)/shard_map/all_to_all | solution.py:21
  147.4 0.8 copy-start.6
  154.4 11.8 %all-to-all-start.13 = ((f32[16,1,1024]{2,1,0:T(1,128)}), f32[16,1,1024]{2,1,0:T(1,128)S(1)}, u32[]{:S(2)}, u32[]{:S(2)}) async-start(f32[16,1,1024]{2,1,0:T(1,128)} %reshape.821), calls=%async_computation.13 | async-start | bytes 131072 | tf_op jit(solution)/shard_map/all_to_all | solution.py:21
  158.6 11.1 %copy-start.1 = (bf16[2,256,128]{2,1,0:T(8,128)(2,1)S(1)}, bf16[2,256,128]{2,1,0:T(8,128)(2,1)}, u32[]{:S(2)}) copy-start(bf16[2,256,128]{2,1,0:T(8,128)(2,1)} %param.18) | copy-start | bytes 393220
  166.2 11.3 %all-to-all-start.10 = ((f32[16,1,1024]{2,1,0:T(1,128)}), f32[16,1,1024]{2,1,0:T(1,128)S(1)}, u32[]{:S(2)}, u32[]{:S(2)}) async-start(f32[16,1,1024]{2,1,0:T(1,128)} %reshape.825), calls=%async_computation.10 | async-start | bytes 131072 | tf_op jit(solution)/shard_map/all_to_all | solution.py:21
  177.5 11.3 %all-to-all-start.12 = ((f32[16,1,1024]{2,1,0:T(1,128)}), f32[16,1,1024]{2,1,0:T(1,128)S(1)}, u32[]{:S(2)}, u32[]{:S(2)}) async-start(f32[16,1,1024]{2,1,0:T(1,128)} %reshape.823), calls=%async_computation.12 | async-start | bytes 131072 | tf_op jit(solution)/shard_map/all_to_all | solution.py:21
  188.8 12.6 %all-to-all-start.14 = ((f32[16,16,128]{2,1,0:T(8,128)}), f32[16,16,128]{2,1,0:T(8,128)S(1)}, u32[]{:S(2)}, u32[]{:S(2)}) async-start(f32[16,16,128]{2,1,0:T(8,128)} %fusion.13), calls=%async_computation.14 | async-start | bytes 262144 | tf_op jit(solution)/shard_map/all_to_all | solution.py:21
  192.2 12.6 %copy-start.9 = (f32[16]{0:T(128)}, f32[16]{0:T(128)S(1)}, u32[]{:S(2)}) copy-start(f32[16]{0:T(128)S(1)} %add_rsqrt_fusion.1) | copy-start | bytes 196
  201.4 11.9 %all-to-all-start.15 = ((f32[16,16,128]{2,1,0:T(8,128)}), f32[16,16,128]{2,1,0:T(8,128)S(1)}, u32[]{:S(2)}, u32[]{:S(2)}) async-start(f32[16,16,128]{2,1,0:T(8,128)} %fusion.11), calls=%async_computation.15 | async-start | bytes 262144 | tf_op jit(solution)/shard_map/all_to_all | solution.py:21
  204.9 0.7 copy-start.8
  205.0 0.6 copy-start.13
  205.6 7.7 %copy-start.15 = (f32[128]{0:T(128)S(1)}, f32[128]{0:T(128)}, u32[]{:S(2)}) copy-start(f32[128]{0:T(128)} %get-tuple-element.16) | copy-start | bytes 1540
  213.3 0.6 copy-start.10
  213.3 11.1 %copy-start.4 = (bf16[2,128,256]{2,1,0:T(8,128)(2,1)S(1)}, bf16[2,128,256]{2,1,0:T(8,128)(2,1)}, u32[]{:S(2)}) copy-start(bf16[2,128,256]{2,1,0:T(8,128)(2,1)} %param.22) | copy-start | bytes 393220
  238.2 11.9 %all-to-all-start.18 = ((f32[16,1,8]{2,1,0:T(1,128)}), f32[16,1,8]{2,1,0:T(1,128)S(1)}, u32[]{:S(2)}, u32[]{:S(2)}) async-start(f32[16,1,8]{2,1,0:T(1,128)} %broadcast_in_dim.16), calls=%async_computation.18 | async-start | bytes 16384 | tf_op jit(solution)/shard_map/all_to_all | solution.py:27
  250.2 0.6 copy-start.11
  251.6 13.3 %all-to-all-start.19 = ((bf16[32,8,256]{2,1,0:T(8,128)(2,1)}), bf16[32,8,256]{2,1,0:T(8,128)(2,1)S(1)}, u32[]{:S(2)}, u32[]{:S(2)}) async-start(bf16[32,8,256]{2,1,0:T(8,128)(2,1)} %broadcast_in_dim.17), calls=%async_computation.19 | async-start | bytes 262144 | tf_op jit(solution)/shard_map/all_to_all | solution.py:27
where the time goes:
time: 267 us; the launch traced here: 266 us
  waiting for transfers between devices  103 us (39%)
  starting transfers between devices  71.5 us (27%)
  blocking collectives  54.7 us (20%)
  local copies, waits for them, and re-layouts  17 us (6%)
  other arithmetic  11.5 us (4%)
  matrix products  6.92 us (3%)
    all_to_all x12, waiting for transfers between devices, summed_on_arrival(): tiles = lax.all_to_all(split_up(array, dim, size), axis, 0, 0, tiled=True)  72.7 us
    all_to_all x12, starting transfers between devices, summed_on_arrival(): tiles = lax.all_to_all(split_up(array, dim, size), axis, 0, 0, tiled=True)  53.9 us
    all_to_all x2, blocking collectives, sum_at_owner(): lax.all_to_all(tiles, axis, split_axis=0, concat_axis=0, tiled=True)  33.8 us
    all_to_all x4, waiting for transfers between devices, sent_to_all(): lax.all_to_all(jnp.broadcast_to(array[None], (size, *array.shape)), axis,...  30.1 us
    all_to_all x2, blocking collectives, sent_to_all(): lax.all_to_all(jnp.broadcast_to(array[None], (size, *array.shape)), axis,...  20.9 us
    all_to_all x4, starting transfers between devices, sent_to_all(): lax.all_to_all(jnp.broadcast_to(array[None], (size, *array.shape)), axis,...  17.6 us
    unnamed x49, local copies, waits for them, and re-layouts  8.99 us
    dot_general x10, matrix products, local(): jnp.dot(normed, weights[section_index], preferred_element_type=jnp.float32)  6.59 us
  transfers between devices with their start and end apart: 16, of which 16 were waited for; matrix products, arithmetic and copies ran while one was open for 9% of the time, Pallas kernels for 0%

commit v1 on v0

v1 whole, which is shorter than its diff:
```python
import functools

import jax
import jax.numpy as jnp
from jax import lax
from jax.experimental import pallas as pl
from jax.experimental.pallas import tpu as pltpu
from jax.sharding import PartitionSpec as P


D = 4096
KEY = 64
VAL = 128
DP = 16
TP = 32
LS = 16
epsilon = 1e-06
bf16 = jnp.bfloat16
f32 = jnp.float32

SWAP = [(d, d ^ 1) for d in range(DP)]
RING = [(2 * y, 2 * ((y + 1) % 8)) for y in range(8)] + [
    (2 * y + 1, 2 * ((y + 7) % 8) + 1) for y in range(8)
]


def whole(shape, index=None):
    at = index or (0,) * len(shape)
    return pl.BlockSpec(shape, lambda i, at=at: at)


def call(body, out_shape, in_specs, out_specs, scratch=(), aliases=None):
    return pl.pallas_call(
        body,
        grid=(1,),
        out_shape=out_shape,
        in_specs=in_specs,
        out_specs=out_specs,
        scratch_shapes=scratch,
        input_output_aliases=aliases or {},
    )


def owners():
    me = lax.axis_index("dp")
    y = me // 2
    c = me % 2
    sign = 2 * c - 1
    found = []
    for p in range(8):
        if p == 0:
            at, order = y, c
        elif p <= 4:
            at, order = (y + sign * p + 8) % 8, c
        else:
            at, order = (y - sign * (p - 4) + 8) % 8, 1 - c
        found.append((2 * at + order, 2 * at + 1 - order))
    return found


def columns(wq, wk, wv, wg, wd):
    qk = jnp.concatenate([wq[0], wk[0]], axis=0).astype(f32).T.astype(bf16)
    decay = jnp.concatenate([wd[0].astype(f32), jnp.zeros((64, 256), f32)], axis=0).T.astype(bf16)
    return (qk, wv[0], wg[0], decay)


def second_weights_body(wq, wk, wv, wg, wd, wo, out):
    for i, w in enumerate(columns(wq, wk, wv, wg, wd)):
        out[0:256, 128 * i : 128 * i + 128] = w
    out[256:320, 0:256] = wo[0, 0:64, :]
    out[256:320, 256:512] = wo[0, 64:128, :]


def partial_body(tokens, pre, post, wq, wk, wv, wg, wd, wo, pay):
    x = tokens[...].astype(f32)
    squares = jnp.sum(x * x, axis=1, keepdims=True)
    normed = (x * pre[0:1, :]).astype(bf16)
    hi = squares.astype(bf16).astype(f32)
    lane = lax.broadcasted_iota(jnp.int32, (256, 128), 1)
    for i, w in enumerate(columns(wq, wk, wv, wg, wd)):
        acc = jnp.dot(normed, w, preferred_element_type=f32)
        if i == 3:
            acc = jnp.where(lane == 64, hi, jnp.where(lane == 65, squares - hi, acc))
        pay[:, 0:LS, 128 * i : 128 * i + 128] = acc.astype(bf16).reshape(DP, LS, 128)
    pay[:, 0:LS, 512:768] = tokens[...].reshape(DP, LS, 256)
    row = lax.broadcasted_iota(jnp.int32, (8, 256), 0)
    gains = jnp.zeros((8, 256), f32)
    for i, g in enumerate((pre[1:2, :], post[0:1, :], post[1:2, :])):
        high = g.astype(bf16).astype(f32)
        gains = jnp.where(row == i, high, gains)
        gains = jnp.where(row == 3 + i, g - high, gains)
    gains = gains.astype(bf16)
    for half in range(2):
        start = 64 * half
        chunks = (
            wo[0, start : start + 24, :],
            wo[0, start + 24 : start + 48, :],
            jnp.concatenate([wo[0, start + 48 : start + 64, :], gains], axis=0),
        )
        for d in range(half, DP, 2):
            for i, chunk in enumerate(chunks):
                pay[d, LS:40, 256 * i : 256 * i + 256] = chunk


def attend(proj, squares, bias, gain, old, new_ref, wide, reads):
    scale = lax.rsqrt(squares / D + epsilon)
    lane = lax.broadcasted_iota(jnp.int32, (LS, 128), 1)
    low = lane < 64
    qk = (proj[:, 0:128] * scale).astype(bf16).astype(f32)
    kq = pltpu.roll(qk, 64, 1)
    query = jnp.where(low, qk, kq)
    key = jnp.where(low, kq, qk)
    value = proj[:, 128:256] * scale
    gate = proj[:, 256:384] * scale
    wide[0:1, 0:64] = bias
    wide[0:1, 64:128] = jnp.zeros((1, 64), f32)
    z = proj[:, 384:512] * scale + wide[0:1, :]
    log_decay = (jnp.minimum(z, 0.0) - jnp.log1p(jnp.exp(-jnp.abs(z)))) / 16.0
    decay = jnp.exp(log_decay)
    decay = jnp.where(low, decay, pltpu.roll(decay, 64, 1))
    right = (lane >= 64).astype(jnp.int32)
    for b in range(64):
        v = jnp.take_along_axis(value, right + 2 * b, axis=1)
        new = decay * old[0, :, b * 128 : b * 128 + 128] + key * v
        new_ref[0, :, b * 128 : b * 128 + 128] = new
        reads[b * LS : b * LS + LS, :] = query * new
    row = lax.broadcasted_iota(jnp.int32, (128, 128), 0)
    col = lax.broadcasted_iota(jnp.int32, (128, 128), 1)
    fold = ((row >= 64) == (col % 2 == 1)).astype(f32).astype(bf16)
    product = reads[...]
    high = product.astype(bf16)
    rest = (product - high.astype(f32)).astype(bf16)
    sums = jnp.dot(high, fold, preferred_element_type=f32) + jnp.dot(rest, fold, preferred_element_type=f32)
    readout = jnp.zeros((LS, 128), f32)
    for b in range(64):
        readout = jnp.where(lane // 2 == b, sums[b * LS : b * LS + LS, :], readout)
    readout = readout * KEY ** (-0.5)
    mean = jnp.sum(readout * readout, axis=1, keepdims=True) / VAL
    silu = gate / (1.0 + jnp.exp(-gate))
    return (readout * lax.rsqrt(mean + epsilon) * gain * silu).astype(bf16)


def first_state_body(got, bias, gain, old, new_ref, mixed, wide, reads):
    proj = got[0, 0:LS, 0:512].astype(f32)
    for d in range(1, DP):
        proj = proj + got[d, 0:LS, 0:512].astype(f32)
    squares = proj[:, 448:449] + proj[:, 449:450]
    mixed[...] = attend(proj, squares, bias[0:1, :], gain[0:1, :], old, new_ref, wide, reads)


def half_of(got, d):
    return [
        got[d, LS:40, 0:256],
        got[d, LS:40, 256:512],
        got[d, LS:32, 512:768],
    ]


def first_spread_body(mixed, got, swapped, out):
    m = mixed[...].astype(f32)
    m = jnp.where(lax.axis_index("dp") % 2 == 0, m, pltpu.roll(m, 64, 1)).astype(bf16)
    for d in range(DP):
        w = jnp.concatenate(half_of(got, d) + half_of(swapped, d), axis=0)
        part = jnp.dot(m, w, preferred_element_type=f32).astype(bf16)
        out[2 * d] = part[:, 0:128]
        out[2 * d + 1] = part[:, 128:256]


def second_body(normed, squares, bias, gain, old, kept, *refs):
    weights, outs = refs[:8], refs[8:16]
    new_ref, out, wide, reads = refs[16:]
    proj = jnp.zeros((LS, 512), f32)
    where = owners()
    for piece, pair in zip(weights, where):
        for j in range(2):
            proj = proj + jnp.dot(normed[pair[j]], piece[j], preferred_element_type=f32)
    m = attend(proj, squares[:, 0:1], bias[1:2, :], gain[1:2, :], old, new_ref, wide, reads)
    for piece, pair in zip(outs, where):
        for j in range(2):
            w = jnp.concatenate([piece[j, :, 0:256], piece[j, :, 256:512]], axis=0)
            part = jnp.dot(m, w, preferred_element_type=f32).astype(bf16)
            out[2 * pair[j]] = part[:, 0:128]
            out[2 * pair[j] + 1] = part[:, 128:256]


def total_body(arrived, out):
    total = arrived[0].astype(f32)
    for t in range(1, TP):
        total = total + arrived[t].astype(f32)
    total = total.astype(bf16)
    for t in range(TP):
        out[t] = total


def residual_body(b, full, x, gains, *outs):
    squares = jnp.zeros((LS, 128), f32)
    for t in range(TP):
        o = full[t].astype(f32)
        squares = squares + o * o
    scale = lax.rsqrt(jnp.sum(squares, axis=1, keepdims=True) / D + epsilon)
    after = jnp.zeros((LS, 256), f32)
    for d in range(DP):
        g = gains[d].astype(f32)
        o = jnp.concatenate([full[2 * d], full[2 * d + 1]], axis=1).astype(f32)
        post = g[1 + b : 2 + b, :] + g[4 + b : 5 + b, :]
        new = (x[d].astype(f32) + o * scale * post).astype(bf16)
        outs[0][d] = new
        if b == 0:
            wide = new.astype(f32)
            after = after + wide * wide
            outs[1][d] = (wide * (g[0:1, :] + g[3:4, :])).astype(bf16)
    if b == 0:
        total = jnp.sum(after, axis=1, keepdims=True)
        outs[2][...] = jnp.broadcast_to(total, (LS, 128))


def gathered(array, after):
    other = lax.ppermute(array, "dp", SWAP)
    own = jnp.stack([array, other])
    ring = []
    swapped = []
    now, after = lax.optimization_barrier((own, after))
    own = now
    for k in range(4):
        now = lax.ppermute(now, "dp", RING)
        ring.append(now)
        if k < 3:
            swapped.append(lax.ppermute(now, "dp", SWAP))
    return [own, *ring, *swapped], after


def shape(s, t=bf16):
    return jax.ShapeDtypeStruct(s, t)


def local(tokens, recurrent_state, pre_gain, w_query, w_key, w_value, w_gate, w_decay, decay_bias, head_gain, w_out, post_gain):
    turned = lambda w: jnp.swapaxes(w, 1, 2)
    weights = (turned(w_query), turned(w_key), w_value, w_gate, turned(w_decay))

    def weight_specs(b):
        return [whole((1, *w.shape[1:]), (b, 0, 0)) for w in weights]

    pay = call(
        partial_body,
        shape((DP, 40, 768)),
        [whole((256, 256)), whole((2, 256)), whole((2, 256)), *weight_specs(0), whole((1, 128, 256))],
        whole((DP, 40, 768)),
    )(tokens, pre_gain, post_gain, *weights, w_out)
    second = call(
        second_weights_body,
        shape((320, 512)),
        [*weight_specs(1), whole((1, 128, 256), (1, 0, 0))],
        whole((320, 512)),
    )(*weights, w_out)
    got = lax.all_to_all(pay, "dp", 0, 0, tiled=True)
    pieces1, got = gathered(second, got)
    swapped = lax.ppermute(got, "dp", SWAP)
    wide = [pltpu.VMEM((8, 128), f32), pltpu.VMEM((64 * LS, 128), f32)]
    state, mixed = call(
        first_state_body,
        [shape((2, LS, 8192), f32), shape((LS, 128))],
        [whole((DP, 40, 768)), whole((2, 64)), whole((2, 128)), whole((1, LS, 8192))],
        [whole((1, LS, 8192)), whole((LS, 128))],
        wide,
    )(got, decay_bias, head_gain, recurrent_state)
    spread = call(
        first_spread_body,
        shape((TP, LS, 128)),
        [whole((LS, 128))] + [whole((DP, 40, 768))] * 2,
        whole((TP, LS, 128)),
    )(mixed, got, swapped)
    x, x_spec = got, whole((DP, LS, 256), (0, 0, 2))
    for b in range(2):
        arrived = lax.all_to_all(spread, "tp", 0, 0, tiled=True)
        if b == 0:
            arrived, _ = lax.optimization_barrier((arrived, pieces1[2]))
        own = call(
            total_body, shape((TP, LS, 128)), [whole((TP, LS, 128))], whole((TP, LS, 128))
        )(arrived)
        full = lax.all_to_all(own, "tp", 0, 0, tiled=True)
        if b == 0:
            full, _ = lax.optimization_barrier((full, pieces1[3]))
        outs = [shape((DP, LS, 256))]
        if b == 0:
            outs += [shape((DP, LS, 256)), shape((LS, 128), f32)]
        results = call(
            functools.partial(residual_body, b),
            outs,
            [whole((TP, LS, 128)), x_spec, whole((DP, 8, 256), (0, 4, 2))],
            [whole(o.shape) for o in outs],
        )(full, x, got)
        x, x_spec = results[0], whole((DP, LS, 256))
        if b == 0:
            state, spread = call(
                second_body,
                [shape((2, LS, 8192), f32), shape((TP, LS, 128))],
                [whole((DP, LS, 256)), whole((LS, 128)), whole((2, 64)), whole((2, 128))]
                + [whole((1, LS, 8192), (1, 0, 0)), pl.BlockSpec(memory_space=pl.ANY)]
                + [whole((2, 256, 512))] * 8
                + [whole((2, 64, 512), (0, 4, 0))] * 8,
                [whole((1, LS, 8192), (1, 0, 0)), whole((TP, LS, 128))],
                wide,
                {5: 0},
            )(results[1], results[2], decay_bias, head_gain, recurrent_state, state, *pieces1, *pieces1)
    back = lax.all_to_all(x, "dp", 0, 0, tiled=True)
    return (back.reshape(256, 256), state)


def solution(mesh):
    in_specs = (
        P(None, "dp"),
        P(None, "dp", "tp"),
        P(None, "dp"),
        P(None, "dp", "tp"),
        P(None, "dp", "tp"),
        P(None, "dp", "tp"),
        P(None, "dp", "tp"),
        P(None, "dp", "tp"),
        P(None, "tp"),
        P(),
        P(None, "tp", "dp"),
        P(None, "dp"),
    )
    out_specs = (P(None, "dp"), P(None, "dp", "tp"))

    return jax.shard_map(local, mesh=mesh, in_specs=in_specs, out_specs=out_specs, check_vma=False)
```

time: 267 us -> 184 us (0.69)
  waiting for transfers between devices: 103 us -> 41.7 us
  starting transfers between devices: 71.5 us -> 35.8 us
  blocking collectives: 54.7 us -> 81.7 us
  Pallas kernels: 0 us -> 21.4 us
  local copies, waits for them, and re-layouts: 17 us -> 0.67 us
  other arithmetic: 11.5 us -> 1.03 us
  matrix products: 6.92 us -> 0 us
    all_to_all x16 -> x1, waiting for transfers between devices: 103 us -> 20.2 us  [local(): got = lax.all_to_all(pay, 'dp', 0, 0, tiled=True)]
    all_to_all x16 -> x1, starting transfers between devices: 71.5 us -> 10.3 us  [local(): got = lax.all_to_all(pay, 'dp', 0, 0, tiled=True)]
    all_to_all x4 -> x5, blocking collectives: 54.7 us -> 81.7 us  [the longest x2 35.1 us: local(): arrived = lax.all_to_all(spread, 'tp', 0, 0, tiled=True)]
    ppermute x0 -> x9, starting transfers between devices: none -> 25.6 us  [the longest x3 11.1 us: gathered(): swapped.append(lax.ppermute(now, 'dp', SWAP))]
    ppermute x0 -> x9, waiting for transfers between devices: none -> 21.5 us  [the longest x4 19.9 us: gathered(): now = lax.ppermute(now, 'dp', RING)]
    pallas_call x0 -> x9, Pallas kernels: none -> 21.4 us  [the longest x1 5.18 us: local(): call(second_body, [shape((2, LS, 8192), f32), shape((TP, LS, 128))], [who...]
    unnamed x49 -> x9, local copies, waits for them, and re-layouts: 8.99 us -> 0.67 us
    dot_general x12 -> x0, matrix products: 6.92 us -> none  [the longest x10 6.59 us: local(): jnp.dot(normed, weights[section_index], preferred_element_type=jnp.float32)]
  transfers between devices with their start and end apart: 16 -> 10, of which waited for: 16 -> 5; matrix products, arithmetic and copies ran while one was open for 9% -> 1% of each run, Pallas kernels for 0% -> 6%
where the time goes in v1:
time: 184 us; the launch traced here: 183 us
  blocking collectives  81.7 us (44%)
  waiting for transfers between devices  41.7 us (23%)
  starting transfers between devices  35.8 us (19%)
  Pallas kernels  21.4 us (12%)
    all_to_all x2, blocking collectives, local(): arrived = lax.all_to_all(spread, 'tp', 0, 0, tiled=True)  35.1 us
    all_to_all x2, blocking collectives, local(): full = lax.all_to_all(own, 'tp', 0, 0, tiled=True)  27.9 us
    all_to_all x1, waiting for transfers between devices, local(): got = lax.all_to_all(pay, 'dp', 0, 0, tiled=True)  20.2 us
    ppermute x4, waiting for transfers between devices, gathered(): now = lax.ppermute(now, 'dp', RING)  19.9 us
    all_to_all x1, blocking collectives, local(): back = lax.all_to_all(x, 'dp', 0, 0, tiled=True)  18.7 us
    ppermute x3, starting transfers between devices, gathered(): swapped.append(lax.ppermute(now, 'dp', SWAP))  11.1 us
    ppermute x4, starting transfers between devices, gathered(): now = lax.ppermute(now, 'dp', RING)  10.4 us
    all_to_all x1, starting transfers between devices, local(): got = lax.all_to_all(pay, 'dp', 0, 0, tiled=True)  10.3 us
  transfers between devices with their start and end apart: 10, of which 5 were waited for; matrix products, arithmetic and copies ran while one was open for 1% of the time, Pallas kernels for 6%

profile of v1, /device:TPU:1, one launch (start us, length us, event | category | flops | bytes accessed | tf_op | source)
XLA Modules:
  0.0 183.1 jit_solution(685027086679159480)
XLA Ops:
  0.6 2.4 %shard_map.132 = bf16[16,40,768]{2,1,0:T(8,128)(2,1)} custom-call(bf16[256,256]{1,0:T(8,128)(2,1)} %tokens.1, f32[2,256]{1,0:T(2,128)} %pre.1, f32[2,256]{1,0:T(2,128)} %post.1, bf16[2,64,256]{2,1,0:T(8,128)(2,1)} %bitcast.9, bf16[2,64,256]{2,1,0:T(8,128)(2,1)} %bitcast.11, bf16[2,256,128]{2,1,0:T(8,128)(2,1)} %wv.3, bf16[2,256,128]{2,1,0:T(8,128)(2,1)} %wg.3, ...), custom_call_target="tpu_custom_call" | custom-call | tf_op jit(solution)/shard_map/pallas_call | solution.py:243
  3.0 10.3 %all-to-all-start = ((bf16[16,40,768]{2,1,0:T(8,128)(2,1)}), bf16[16,40,768]{2,1,0:T(8,128)(2,1)S(1)}, u32[]{:S(2)}, u32[]{:S(2)}) async-start(bf16[16,40,768]{2,1,0:T(8,128)(2,1)} %shard_map.132), calls=%async_computation | async-start | bytes 1966080 | tf_op jit(solution)/shard_map/all_to_all | solution.py:255
  13.3 1.8 shard_map.131
  15.0 2.1 %collective-permute-start = (bf16[320,512]{1,0:T(8,128)(2,1)}, bf16[320,512]{1,0:T(8,128)(2,1)S(1)}, u32[]{:S(2)}, u32[]{:S(2)}) collective-permute-start(bf16[320,512]{1,0:T(8,128)(2,1)} %shard_map.131), channel_id=1, source_target_pairs={{0,1},{1,0},{2,3},{3,2},{4,5},{5,4},{6,7},{7,6},{8,9},{9,8},{10,11... | collective-permute-start | bytes 983048 | tf_op jit(solution)/shard_map/ppermute | solution.py:218
  17.2 1.6 collective-permute-done
  18.8 1.0 pad_maximum_fusion.refs_0_.refs_8_
  19.8 0.0 copy-start.1
  19.8 20.2 %all-to-all-done.got.x.gains = bf16[16,40,768]{2,1,0:T(8,128)(2,1)S(1)} async-done(((bf16[16,40,768]{2,1,0:T(8,128)(2,1)}), bf16[16,40,768]{2,1,0:T(8,128)(2,1)S(1)}, u32[]{:S(2)}, u32[]{:S(2)}) %all-to-all-start) | async-done | bytes 983072 | tf_op jit(solution)/shard_map/all_to_all | solution.py:255
  40.0 0.0 copy-start
  40.0 1.9 %collective-permute-start.2 = (bf16[2,320,512]{2,1,0:T(8,128)(2,1)S(1)}, bf16[2,320,512]{2,1,0:T(8,128)(2,1)S(1)}, u32[]{:S(2)}, u32[]{:S(2)}) collective-permute-start(bf16[2,320,512]{2,1,0:T(8,128)(2,1)S(1)} %pad_maximum_fusion.refs_0_.refs_8_), channel_id=1, source_target_pairs={{0,2},{2,4},{4,6},{6,8},{8,10},{10,12},{12,14},{14,0},{1,15},{3,1}... | collective-permute-start | bytes 1966088 | tf_op jit(solution)/shard_map/ppermute | solution.py:225
  41.9 9.7 %collective-permute-done.2.refs_1_.refs_9_ = bf16[2,320,512]{2,1,0:T(8,128)(2,1)S(1)} collective-permute-done((bf16[2,320,512]{2,1,0:T(8,128)(2,1)S(1)}, bf16[2,320,512]{2,1,0:T(8,128)(2,1)S(1)}, u32[]{:S(2)}, u32[]{:S(2)}) %collective-permute-start.2) | collective-permute-done | bytes 655392 | tf_op jit(solution)/shard_map/ppermute | solution.py:225
  51.6 0.0 copy-start.2
  51.6 2.8 %collective-permute-start.3 = (bf16[2,320,512]{2,1,0:T(8,128)(2,1)S(1)}, bf16[2,320,512]{2,1,0:T(8,128)(2,1)S(1)}, u32[]{:S(2)}, u32[]{:S(2)}) collective-permute-start(bf16[2,320,512]{2,1,0:T(8,128)(2,1)S(1)} %collective-permute-done.2.refs_1_.refs_9_), channel_id=1, source_target_pairs={{0,2},{2,4},{4,6},{6,8},{8,10},{10,12},{12,14},{14,0},{1,15},{3,1}... | collective-permute-start | bytes 1966088 | tf_op jit(solution)/shard_map/ppermute | solution.py:225
  54.4 1.9 %collective-permute-start.1 = (bf16[16,40,768]{2,1,0:T(8,128)(2,1)S(1)}, bf16[16,40,768]{2,1,0:T(8,128)(2,1)}, u32[]{:S(2)}, u32[]{:S(2)}) collective-permute-start(bf16[16,40,768]{2,1,0:T(8,128)(2,1)S(1)} %all-to-all-done.got.x.gains), channel_id=1, source_target_pairs={{0,1},{1,0},{2,3},{3,2},{4,5},{5,4},{6,7},{7,6},{8,9},{9,8},{10,11... | collective-permute-start | bytes 2949128 | tf_op jit(solution)/shard_map/ppermute | solution.py:257
  56.4 6.9 %collective-permute-done.3.refs_2_.refs_10_ = bf16[2,320,512]{2,1,0:T(8,128)(2,1)S(1)} collective-permute-done((bf16[2,320,512]{2,1,0:T(8,128)(2,1)S(1)}, bf16[2,320,512]{2,1,0:T(8,128)(2,1)S(1)}, u32[]{:S(2)}, u32[]{:S(2)}) %collective-permute-start.3) | collective-permute-done | bytes 655392 | tf_op jit(solution)/shard_map/ppermute | solution.py:225
  63.2 0.0 copy-start.3
  63.2 3.7 %collective-permute-start.4 = (bf16[2,320,512]{2,1,0:T(8,128)(2,1)S(1)}, bf16[2,320,512]{2,1,0:T(8,128)(2,1)}, u32[]{:S(2)}, u32[]{:S(2)}) collective-permute-start(bf16[2,320,512]{2,1,0:T(8,128)(2,1)S(1)} %collective-permute-done.3.refs_2_.refs_10_), channel_id=1, source_target_pairs={{0,2},{2,4},{4,6},{6,8},{8,10},{10,12},{12,14},{14,0},{1,15},{3,1}... | collective-permute-start | bytes 1966088 | tf_op jit(solution)/shard_map/ppermute | solution.py:225
  67.0 2.7 %collective-permute-start.6 = (bf16[2,320,512]{2,1,0:T(8,128)(2,1)S(1)}, bf16[2,320,512]{2,1,0:T(8,128)(2,1)}, u32[]{:S(2)}, u32[]{:S(2)}) collective-permute-start(bf16[2,320,512]{2,1,0:T(8,128)(2,1)S(1)} %collective-permute-done.2.refs_1_.refs_9_), channel_id=1, source_target_pairs={{0,1},{1,0},{2,3},{3,2},{4,5},{5,4},{6,7},{7,6},{8,9},{9,8},{10,11... | collective-permute-start | bytes 1966088 | tf_op jit(solution)/shard_map/ppermute | solution.py:228
  69.6 1.9 %collective-permute-start.7 = (bf16[2,320,512]{2,1,0:T(8,128)(2,1)S(1)}, bf16[2,320,512]{2,1,0:T(8,128)(2,1)}, u32[]{:S(2)}, u32[]{:S(2)}) collective-permute-start(bf16[2,320,512]{2,1,0:T(8,128)(2,1)S(1)} %collective-permute-done.3.refs_2_.refs_10_), channel_id=1, source_target_pairs={{0,1},{1,0},{2,3},{3,2},{4,5},{5,4},{6,7},{7,6},{8,9},{9,8},{10,11... | collective-permute-start | bytes 1966088 | tf_op jit(solution)/shard_map/ppermute | solution.py:228
  71.6 3.4 %collective-permute-done.4.refs_3_.refs_11_ = bf16[2,320,512]{2,1,0:T(8,128)(2,1)} collective-permute-done((bf16[2,320,512]{2,1,0:T(8,128)(2,1)S(1)}, bf16[2,320,512]{2,1,0:T(8,128)(2,1)}, u32[]{:S(2)}, u32[]{:S(2)}) %collective-permute-start.4) | collective-permute-done | bytes 655392 | tf_op jit(solution)/shard_map/ppermute | solution.py:225
  74.9 6.5 %collective-permute-start.8 = (bf16[2,320,512]{2,1,0:T(8,128)(2,1)}, bf16[2,320,512]{2,1,0:T(8,128)(2,1)}, u32[]{:S(2)}, u32[]{:S(2)}) collective-permute-start(bf16[2,320,512]{2,1,0:T(8,128)(2,1)} %collective-permute-done.4.refs_3_.refs_11_), channel_id=1, source_target_pairs={{0,1},{1,0},{2,3},{3,2},{4,5},{5,4},{6,7},{7,6},{8,9},{9,8},{10,11... | collective-permute-start | bytes 1966088 | tf_op jit(solution)/shard_map/ppermute | solution.py:228
  81.5 1.9 %collective-permute-start.5 = (bf16[2,320,512]{2,1,0:T(8,128)(2,1)}, bf16[2,320,512]{2,1,0:T(8,128)(2,1)}, u32[]{:S(2)}, u32[]{:S(2)}) collective-permute-start(bf16[2,320,512]{2,1,0:T(8,128)(2,1)} %collective-permute-done.4.refs_3_.refs_11_), channel_id=1, source_target_pairs={{0,2},{2,4},{4,6},{6,8},{8,10},{10,12},{12,14},{14,0},{1,15},{3,1}... | collective-permute-start | bytes 1966088 | tf_op jit(solution)/shard_map/ppermute | solution.py:225
  83.4 0.0 copy-done
  83.4 2.8 %shard_map.133 = (f32[2,16,8192]{2,1,0:T(8,128)}, bf16[16,128]{1,0:T(8,128)(2,1)}) custom-call(bf16[16,40,768]{2,1,0:T(8,128)(2,1)} %copy-done, f32[2,64]{1,0:T(2,128)} %bias.3, f32[2,128]{1,0:T(2,128)} %gain.3, f32[2,16,8192]{2,1,0:T(8,128)} %old.3), custom_call_target="tpu_custom_call" | custom-call | tf_op jit(solution)/shard_map/pallas_call | solution.py:259
  86.2 0.0 copy-done.2
  86.2 0.0 copy-done.3
  86.2 0.0 collective-permute-done.1.swapped
  86.2 2.5 %shard_map.134 = bf16[32,16,128]{2,1,0:T(8,128)(2,1)} custom-call(bf16[16,128]{1,0:T(8,128)(2,1)} %get-tuple-element.14.mixed, bf16[16,40,768]{2,1,0:T(8,128)(2,1)} %copy-done, bf16[16,40,768]{2,1,0:T(8,128)(2,1)} %collective-permute-done.1.swapped), custom_call_target="tpu_custom_call" | custom-call | tf_op jit(solution)/shard_map/pallas_call | solution.py:266
  88.7 0.0 copy-done.1
  88.7 21.1 %all_to_all.30.arrived = bf16[32,16,128]{2,1,0:T(8,128)(2,1)} all-to-all(bf16[32,16,128]{2,1,0:T(8,128)(2,1)} %shard_map.134), channel_id=1, replica_groups=mesh['tp'=32,'dp'=16] {'tp'}, dimensions={0} | all-to-all | bytes 262144 | tf_op jit(solution)/shard_map/all_to_all | solution.py:274
  109.8 1.6 shard_map.135
  111.4 13.9 %all_to_all.31.full = bf16[32,16,128]{2,1,0:T(8,128)(2,1)} all-to-all(bf16[32,16,128]{2,1,0:T(8,128)(2,1)} %shard_map.135), channel_id=1, replica_groups=mesh['tp'=32,'dp'=16] {'tp'}, dimensions={0} | all-to-all | bytes 262144 | tf_op jit(solution)/shard_map/all_to_all | solution.py:280
  125.4 1.9 %shard_map.136 = (bf16[16,16,256]{2,1,0:T(8,128)(2,1)}, bf16[16,16,256]{2,1,0:T(8,128)(2,1)}, f32[16,128]{1,0:T(8,128)}) custom-call(bf16[32,16,128]{2,1,0:T(8,128)(2,1)} %all_to_all.31.full, bf16[16,40,768]{2,1,0:T(8,128)(2,1)} %copy-done, bf16[16,40,768]{2,1,0:T(8,128)(2,1)} %copy-done), custom_call_target="tpu_custom_call" | custom-call | tf_op jit(solution)/shard_map/pallas_call | solution.py:286
  127.2 0.0 collective-permute-done.6.refs_5_.refs_13_
  127.2 0.0 collective-permute-done.7.refs_6_.refs_14_
  127.2 0.0 collective-permute-done.8.refs_7_.refs_15_
  127.2 0.0 collective-permute-done.5.refs_4_.refs_12_
  127.3 5.2 %shard_map.137 = (f32[2,16,8192]{2,1,0:T(8,128)}, bf16[32,16,128]{2,1,0:T(8,128)(2,1)}) custom-call(bf16[16,16,256]{2,1,0:T(8,128)(2,1)} %get-tuple-element.18.normed, f32[16,128]{1,0:T(8,128)} %get-tuple-element.19.squares, f32[2,64]{1,0:T(2,128)} %bias.3, f32[2,128]{1,0:T(2,128)} %gain.3, f32[2,16,8192]{2,1,0:T(8,128)} %old.3, ...), custom_call_target="tpu_custom_call", output_to_operand_aliasing={{0}: (5, {})} | custom-call | tf_op jit(solution)/shard_map/pallas_call | solution.py:294
  132.4 13.9 %all_to_all.32.arrived = bf16[32,16,128]{2,1,0:T(8,128)(2,1)} all-to-all(bf16[32,16,128]{2,1,0:T(8,128)(2,1)} %get-tuple-element.21), channel_id=1, replica_groups=mesh['tp'=32,'dp'=16] {'tp'}, dimensions={0} | all-to-all | bytes 262144 | tf_op jit(solution)/shard_map/all_to_all | solution.py:274
  146.4 1.6 shard_map.138
  148.0 14.0 %all_to_all.33.full = bf16[32,16,128]{2,1,0:T(8,128)(2,1)} all-to-all(bf16[32,16,128]{2,1,0:T(8,128)(2,1)} %shard_map.138), channel_id=1, replica_groups=mesh['tp'=32,'dp'=16] {'tp'}, dimensions={0} | all-to-all | bytes 262144 | tf_op jit(solution)/shard_map/all_to_all | solution.py:280
  161.9 1.8 shard_map.139
  163.7 18.7 %all_to_all.34 = bf16[16,16,256]{2,1,0:T(8,128)(2,1)S(1)} all-to-all(bf16[16,16,256]{2,1,0:T(8,128)(2,1)} %shard_map.139), channel_id=1, replica_groups=mesh['tp'=32,'dp'=16] {'dp'}, dimensions={0} | all-to-all | bytes 262144 | tf_op jit(solution)/shard_map/all_to_all | solution.py:305
  182.4 0.7 copy.17
Async XLA Ops:
  3.0 37.0 %all-to-all-start = ((bf16[16,40,768]{2,1,0:T(8,128)(2,1)}), bf16[16,40,768]{2,1,0:T(8,128)(2,1)S(1)}, u32[]{:S(2)}, u32[]{:S(2)}) async-start(bf16[16,40,768]{2,1,0:T(8,128)(2,1)} %shard_map.132), calls=%async_computation | async-start | bytes 1966080 | tf_op jit(solution)/shard_map/all_to_all | solution.py:255
  15.0 3.7 %collective-permute-start = (bf16[320,512]{1,0:T(8,128)(2,1)}, bf16[320,512]{1,0:T(8,128)(2,1)S(1)}, u32[]{:S(2)}, u32[]{:S(2)}) collective-permute-start(bf16[320,512]{1,0:T(8,128)(2,1)} %shard_map.131), channel_id=1, source_target_pairs={{0,1},{1,0},{2,3},{3,2},{4,5},{5,4},{6,7},{7,6},{8,9},{9,8},{10,11... | collective-permute-start | bytes 983048 | tf_op jit(solution)/shard_map/ppermute | solution.py:218
  19.8 68.9 %copy-start.1 = (bf16[2,320,512]{2,1,0:T(8,128)(2,1)}, bf16[2,320,512]{2,1,0:T(8,128)(2,1)S(1)}, u32[]{:S(2)}) copy-start(bf16[2,320,512]{2,1,0:T(8,128)(2,1)S(1)} %pad_maximum_fusion.refs_0_.refs_8_) | copy-start | bytes 1966084
  40.0 43.4 %copy-start = (bf16[16,40,768]{2,1,0:T(8,128)(2,1)}, bf16[16,40,768]{2,1,0:T(8,128)(2,1)S(1)}, u32[]{:S(2)}) copy-start(bf16[16,40,768]{2,1,0:T(8,128)(2,1)S(1)} %all-to-all-done.got.x.gains) | copy-start | bytes 2949124
  40.0 11.6 %collective-permute-start.2 = (bf16[2,320,512]{2,1,0:T(8,128)(2,1)S(1)}, bf16[2,320,512]{2,1,0:T(8,128)(2,1)S(1)}, u32[]{:S(2)}, u32[]{:S(2)}) collective-permute-start(bf16[2,320,512]{2,1,0:T(8,128)(2,1)S(1)} %pad_maximum_fusion.refs_0_.refs_8_), channel_id=1, source_target_pairs={{0,2},{2,4},{4,6},{6,8},{8,10},{10,12},{12,14},{14,0},{1,15},{3,1}... | collective-permute-start | bytes 1966088 | tf_op jit(solution)/shard_map/ppermute | solution.py:225
  51.6 34.6 %copy-start.2 = (bf16[2,320,512]{2,1,0:T(8,128)(2,1)}, bf16[2,320,512]{2,1,0:T(8,128)(2,1)S(1)}, u32[]{:S(2)}) copy-start(bf16[2,320,512]{2,1,0:T(8,128)(2,1)S(1)} %collective-permute-done.2.refs_1_.refs_9_) | copy-start | bytes 1966084
  51.6 11.6 %collective-permute-start.3 = (bf16[2,320,512]{2,1,0:T(8,128)(2,1)S(1)}, bf16[2,320,512]{2,1,0:T(8,128)(2,1)S(1)}, u32[]{:S(2)}, u32[]{:S(2)}) collective-permute-start(bf16[2,320,512]{2,1,0:T(8,128)(2,1)S(1)} %collective-permute-done.2.refs_1_.refs_9_), channel_id=1, source_target_pairs={{0,2},{2,4},{4,6},{6,8},{8,10},{10,12},{12,14},{14,0},{1,15},{3,1}... | collective-permute-start | bytes 1966088 | tf_op jit(solution)/shard_map/ppermute | solution.py:225
  54.4 31.8 %collective-permute-start.1 = (bf16[16,40,768]{2,1,0:T(8,128)(2,1)S(1)}, bf16[16,40,768]{2,1,0:T(8,128)(2,1)}, u32[]{:S(2)}, u32[]{:S(2)}) collective-permute-start(bf16[16,40,768]{2,1,0:T(8,128)(2,1)S(1)} %all-to-all-done.got.x.gains), channel_id=1, source_target_pairs={{0,1},{1,0},{2,3},{3,2},{4,5},{5,4},{6,7},{7,6},{8,9},{9,8},{10,11... | collective-permute-start | bytes 2949128 | tf_op jit(solution)/shard_map/ppermute | solution.py:257
  63.2 23.0 %copy-start.3 = (bf16[2,320,512]{2,1,0:T(8,128)(2,1)}, bf16[2,320,512]{2,1,0:T(8,128)(2,1)S(1)}, u32[]{:S(2)}) copy-start(bf16[2,320,512]{2,1,0:T(8,128)(2,1)S(1)} %collective-permute-done.3.refs_2_.refs_10_) | copy-start | bytes 1966084
  63.2 11.7 %collective-permute-start.4 = (bf16[2,320,512]{2,1,0:T(8,128)(2,1)S(1)}, bf16[2,320,512]{2,1,0:T(8,128)(2,1)}, u32[]{:S(2)}, u32[]{:S(2)}) collective-permute-start(bf16[2,320,512]{2,1,0:T(8,128)(2,1)S(1)} %collective-permute-done.3.refs_2_.refs_10_), channel_id=1, source_target_pairs={{0,2},{2,4},{4,6},{6,8},{8,10},{10,12},{12,14},{14,0},{1,15},{3,1}... | collective-permute-start | bytes 1966088 | tf_op jit(solution)/shard_map/ppermute | solution.py:225
  67.0 60.3 %collective-permute-start.6 = (bf16[2,320,512]{2,1,0:T(8,128)(2,1)S(1)}, bf16[2,320,512]{2,1,0:T(8,128)(2,1)}, u32[]{:S(2)}, u32[]{:S(2)}) collective-permute-start(bf16[2,320,512]{2,1,0:T(8,128)(2,1)S(1)} %collective-permute-done.2.refs_1_.refs_9_), channel_id=1, source_target_pairs={{0,1},{1,0},{2,3},{3,2},{4,5},{5,4},{6,7},{7,6},{8,9},{9,8},{10,11... | collective-permute-start | bytes 1966088 | tf_op jit(solution)/shard_map/ppermute | solution.py:228
  69.6 57.6 %collective-permute-start.7 = (bf16[2,320,512]{2,1,0:T(8,128)(2,1)S(1)}, bf16[2,320,512]{2,1,0:T(8,128)(2,1)}, u32[]{:S(2)}, u32[]{:S(2)}) collective-permute-start(bf16[2,320,512]{2,1,0:T(8,128)(2,1)S(1)} %collective-permute-done.3.refs_2_.refs_10_), channel_id=1, source_target_pairs={{0,1},{1,0},{2,3},{3,2},{4,5},{5,4},{6,7},{7,6},{8,9},{9,8},{10,11... | collective-permute-start | bytes 1966088 | tf_op jit(solution)/shard_map/ppermute | solution.py:228
  74.9 52.3 %collective-permute-start.8 = (bf16[2,320,512]{2,1,0:T(8,128)(2,1)}, bf16[2,320,512]{2,1,0:T(8,128)(2,1)}, u32[]{:S(2)}, u32[]{:S(2)}) collective-permute-start(bf16[2,320,512]{2,1,0:T(8,128)(2,1)} %collective-permute-done.4.refs_3_.refs_11_), channel_id=1, source_target_pairs={{0,1},{1,0},{2,3},{3,2},{4,5},{5,4},{6,7},{7,6},{8,9},{9,8},{10,11... | collective-permute-start | bytes 1966088 | tf_op jit(solution)/shard_map/ppermute | solution.py:228
  81.5 45.8 %collective-permute-start.5 = (bf16[2,320,512]{2,1,0:T(8,128)(2,1)}, bf16[2,320,512]{2,1,0:T(8,128)(2,1)}, u32[]{:S(2)}, u32[]{:S(2)}) collective-permute-start(bf16[2,320,512]{2,1,0:T(8,128)(2,1)} %collective-permute-done.4.refs_3_.refs_11_), channel_id=1, source_target_pairs={{0,2},{2,4},{4,6},{6,8},{8,10},{10,12},{12,14},{14,0},{1,15},{3,1}... | collective-permute-start | bytes 1966088 | tf_op jit(solution)/shard_map/ppermute | solution.py:225

commit v2 on v1

v2 whole, which is shorter than its diff:
```python
import jax
import jax.numpy as jnp
from jax import lax
from jax.experimental import pallas as pl
from jax.experimental.pallas import tpu as pltpu
from jax.sharding import PartitionSpec as P


D = 4096
KEY = 64
VAL = 128
DP = 16
TP = 32
LS = 16
epsilon = 1e-06
bf16 = jnp.bfloat16
f32 = jnp.float32

SWAP = [(d, d ^ 1) for d in range(DP)]
RING = [(2 * y, 2 * ((y + 1) % 8)) for y in range(8)] + [
    (2 * y + 1, 2 * ((y + 7) % 8) + 1) for y in range(8)
]


def whole(shape, index=None):
    at = index or (0,) * len(shape)
    return pl.BlockSpec(shape, lambda i, at=at: at)


def call(body, out_shape, in_specs, out_specs, scratch=(), aliases=None, limit=16):
    return pl.pallas_call(
        body,
        grid=(1,),
        out_shape=out_shape,
        in_specs=in_specs,
        out_specs=out_specs,
        scratch_shapes=scratch,
        input_output_aliases=aliases or {},
        compiler_params=pltpu.CompilerParams(vmem_limit_bytes=limit * 1024 * 1024),
    )


def owners():
    me = lax.axis_index("dp")
    y = me // 2
    c = me % 2
    sign = 2 * c - 1
    found = []
    for p in range(8):
        if p == 0:
            at, order = y, c
        elif p <= 4:
            at, order = (y + sign * p + 8) % 8, c
        else:
            at, order = (y - sign * (p - 4) + 8) % 8, 1 - c
        found.append((2 * at + order, 2 * at + 1 - order))
    return found


def columns(wq, wk, wv, wg, wd):
    qk = jnp.concatenate([wq[0], wk[0]], axis=0).astype(f32).T.astype(bf16)
    decay = jnp.concatenate([wd[0].astype(f32), jnp.zeros((64, 256), f32)], axis=0).T.astype(bf16)
    return (qk, wv[0], wg[0], decay)


def split3(value):
    high = value.astype(bf16).astype(f32)
    mid = (value - high).astype(bf16).astype(f32)
    return high, mid, value - high - mid


def place(acc, lane, start, values):
    for i, value in enumerate(values):
        acc = jnp.where(lane == start + i, value, acc)
    return acc


def partial_body(tokens, pre, wq, wk, wv, wg, wd, pay):
    x = tokens[...].astype(f32)
    squares = jnp.sum(x * x, axis=1, keepdims=True)
    normed = (x * pre[0:1, :]).astype(bf16)
    lane = lax.broadcasted_iota(jnp.int32, (256, 128), 1)
    for i, w in enumerate(columns(wq, wk, wv, wg, wd)):
        acc = jnp.dot(normed, w, preferred_element_type=f32)
        if i == 3:
            acc = place(acc, lane, 64, split3(squares))
        pay[:, :, 128 * i : 128 * i + 128] = acc.astype(bf16).reshape(DP, LS, 128)


def first_state_body(got, bias, gain, old, new_ref, mixed, wide, reads):
    proj = got[0].astype(f32)
    for d in range(1, DP):
        proj = proj + got[d].astype(f32)
    squares = proj[:, 448:449] + proj[:, 449:450] + proj[:, 450:451]
    m = attend(proj, squares, bias[0:1, :], gain[0:1, :], old, new_ref, wide, reads)
    for d in range(DP):
        mixed[d] = m


def first_out_body(mixed, wo, out):
    m = mixed[...].reshape(DP * LS, VAL)
    part = jnp.dot(m, wo[0], preferred_element_type=f32)
    out[...] = part.reshape(TP, 8, 256).astype(bf16)


def total_body(arrived, out):
    total = arrived[0].astype(f32)
    for t in range(1, TP):
        total = total + arrived[t].astype(f32)
    total = total.astype(bf16)
    for t in range(TP):
        out[t] = total


def second_partial_body(full, tokens, pre, post, wq, wk, wv, wg, wd, pay):
    x = tokens[...].astype(f32)
    out = full[...].astype(f32).reshape(256, 256)
    step = out * post[0:1, :]
    stats = []
    for value in (out * out, x * x, x * step, step * step):
        stats += split3(jnp.sum(value, axis=1, keepdims=True))
    gain = pre[1:2, :]
    lhs = ((step * gain).astype(bf16), (x * gain).astype(bf16))
    lane = lax.broadcasted_iota(jnp.int32, (256, 128), 1)
    for i, w in enumerate(columns(wq, wk, wv, wg, wd)):
        for j in range(2):
            acc = jnp.dot(lhs[j], w, preferred_element_type=f32)
            if i == 3 and j == 0:
                acc = place(acc, lane, 64, stats)
            at = 512 * j + 128 * i
            pay[:, :, at : at + 128] = acc.astype(bf16).reshape(DP, LS, 128)


def second_state_body(got, bias, gain, old, kept, *refs):
    pieces = refs[:8]
    new_ref, out, norm, wide, reads = refs[8:]
    total = got[0].astype(f32)
    for d in range(1, DP):
        total = total + got[d].astype(f32)
    stats = []
    for i in range(4):
        at = 448 + 3 * i
        stats.append(total[:, at : at + 1] + total[:, at + 1 : at + 2] + total[:, at + 2 : at + 3])
    scale = lax.rsqrt(stats[0] / D + epsilon)
    squares = stats[1] + 2.0 * scale * stats[2] + scale * scale * stats[3]
    proj = total[:, 512:1024] + scale * total[:, 0:512]
    norm[...] = jnp.broadcast_to(scale, (LS, 128))
    m = attend(proj, jnp.maximum(squares, 0.0), bias[1:2, :], gain[1:2, :], old, new_ref, wide, reads)
    for piece, pair in zip(pieces, owners()):
        for j in range(2):
            part = jnp.dot(m, piece[j], preferred_element_type=f32).astype(bf16)
            out[2 * pair[j]] = part[:, 0:128]
            out[2 * pair[j] + 1] = part[:, 128:256]


def scaled_body(full, norm, pay):
    squares = jnp.zeros((LS, 128), f32)
    for t in range(TP):
        o = full[t].astype(f32)
        squares = squares + o * o
    scale = lax.rsqrt(jnp.sum(squares, axis=1, keepdims=True) / D + epsilon)
    lane = lax.broadcasted_iota(jnp.int32, (LS, 128), 1)
    first = place(jnp.zeros((LS, 128), f32), lane, 0, split3(norm[...])).astype(bf16)
    for d in range(DP):
        pay[d, :, 0:128] = (full[2 * d].astype(f32) * scale).astype(bf16)
        pay[d, :, 128:256] = (full[2 * d + 1].astype(f32) * scale).astype(bf16)
        pay[d, :, 256:384] = first


def final_body(got, full, tokens, post, hidden):
    came = got[...].astype(f32).reshape(256, 384)
    scale = came[:, 256:257] + came[:, 257:258] + came[:, 258:259]
    out = full[...].astype(f32).reshape(256, 256)
    x = (tokens[...].astype(f32) + out * scale * post[0:1, :]).astype(bf16).astype(f32)
    hidden[...] = (x + came[:, 0:256] * post[1:2, :]).astype(bf16)


def attend(proj, squares, bias, gain, old, new_ref, wide, reads):
    scale = lax.rsqrt(squares / D + epsilon)
    lane = lax.broadcasted_iota(jnp.int32, (LS, 128), 1)
    low = lane < 64
    qk = (proj[:, 0:128] * scale).astype(bf16).astype(f32)
    kq = pltpu.roll(qk, 64, 1)
    query = jnp.where(low, qk, kq)
    key = jnp.where(low, kq, qk)
    value = proj[:, 128:256] * scale
    gate = proj[:, 256:384] * scale
    wide[0:1, 0:64] = bias
    wide[0:1, 64:128] = jnp.zeros((1, 64), f32)
    z = proj[:, 384:512] * scale + wide[0:1, :]
    log_decay = (jnp.minimum(z, 0.0) - jnp.log1p(jnp.exp(-jnp.abs(z)))) / 16.0
    decay = jnp.exp(log_decay)
    decay = jnp.where(low, decay, pltpu.roll(decay, 64, 1))
    right = (lane >= 64).astype(jnp.int32)
    for b in range(64):
        v = jnp.take_along_axis(value, right + 2 * b, axis=1)
        new = decay * old[0, :, b * 128 : b * 128 + 128] + key * v
        new_ref[0, :, b * 128 : b * 128 + 128] = new
        reads[b * LS : b * LS + LS, :] = query * new
    row = lax.broadcasted_iota(jnp.int32, (128, 128), 0)
    col = lax.broadcasted_iota(jnp.int32, (128, 128), 1)
    fold = ((row >= 64) == (col % 2 == 1)).astype(f32).astype(bf16)
    product = reads[...]
    high = product.astype(bf16)
    rest = (product - high.astype(f32)).astype(bf16)
    sums = jnp.dot(high, fold, preferred_element_type=f32) + jnp.dot(rest, fold, preferred_element_type=f32)
    readout = jnp.zeros((LS, 128), f32)
    for b in range(64):
        readout = jnp.where(lane // 2 == b, sums[b * LS : b * LS + LS, :], readout)
    readout = readout * KEY ** (-0.5)
    mean = jnp.sum(readout * readout, axis=1, keepdims=True) / VAL
    silu = gate / (1.0 + jnp.exp(-gate))
    return (readout * lax.rsqrt(mean + epsilon) * gain * silu).astype(bf16)


def gathered(array):
    other = lax.ppermute(array, "dp", SWAP)
    own = jnp.stack([array, other])
    ring = []
    swapped = []
    now = own
    for k in range(4):
        now = lax.ppermute(now, "dp", RING)
        ring.append(now)
        if k < 3:
            swapped.append(lax.ppermute(now, "dp", SWAP))
    return [own, *ring, *swapped]


def shape(s, t=bf16):
    return jax.ShapeDtypeStruct(s, t)


def local(tokens, recurrent_state, pre_gain, w_query, w_key, w_value, w_gate, w_decay, decay_bias, head_gain, w_out, post_gain):
    turned = lambda w: jnp.swapaxes(w, 1, 2)
    weights = (turned(w_query), turned(w_key), w_value, w_gate, turned(w_decay))

    def weight_specs(b):
        return [whole((1, *w.shape[1:]), (b, 0, 0)) for w in weights]

    def exchange(array, axis, beside=None):
        came = lax.all_to_all(array, axis, 0, 0, tiled=True)
        if beside is not None:
            came, _ = lax.optimization_barrier((came, beside))
        return came

    pair = whole((2, 256))
    pay = call(
        partial_body,
        shape((DP, LS, 512)),
        [whole((256, 256)), pair, *weight_specs(0)],
        whole((DP, LS, 512)),
        limit=60,
    )(tokens, pre_gain, *weights)
    pieces = gathered(w_out[1])
    got = exchange(pay, "dp", pieces[1])
    scratch = [pltpu.VMEM((8, 128), f32), pltpu.VMEM((64 * LS, 128), f32)]
    state, mixed = call(
        first_state_body,
        [shape((2, LS, 8192), f32), shape((DP, LS, 128))],
        [whole((DP, LS, 512)), whole((2, 64)), whole((2, 128)), whole((1, LS, 8192))],
        [whole((1, LS, 8192)), whole((DP, LS, 128))],
        scratch,
    )(got, decay_bias, head_gain, recurrent_state)
    mixed = exchange(mixed, "dp", pieces[2])
    spread = call(
        first_out_body,
        shape((TP, 8, 256)),
        [whole((DP, LS, 128)), whole((1, 128, 256))],
        whole((TP, 8, 256)),
    )(mixed, w_out)
    arrived = exchange(spread, "tp", pieces[3])
    own = call(total_body, shape((TP, 8, 256)), [whole((TP, 8, 256))], whole((TP, 8, 256)))(arrived)
    full0 = exchange(own, "tp", pieces[4])
    pay = call(
        second_partial_body,
        shape((DP, LS, 1024)),
        [whole((TP, 8, 256)), whole((256, 256)), pair, pair, *weight_specs(1)],
        whole((DP, LS, 1024)),
    )(full0, tokens, pre_gain, post_gain, *weights)
    got = exchange(pay, "dp")
    state, spread, norm = call(
        second_state_body,
        [shape((2, LS, 8192), f32), shape((TP, LS, 128)), shape((LS, 128), f32)],
        [whole((DP, LS, 1024)), whole((2, 64)), whole((2, 128))]
        + [whole((1, LS, 8192), (1, 0, 0)), pl.BlockSpec(memory_space=pl.ANY)]
        + [whole((2, 128, 256))] * 8,
        [whole((1, LS, 8192), (1, 0, 0)), whole((TP, LS, 128)), whole((LS, 128))],
        scratch,
        {4: 0},
    )(got, decay_bias, head_gain, recurrent_state, state, *pieces)
    arrived = exchange(spread, "tp")
    own = call(total_body, shape((TP, LS, 128)), [whole((TP, LS, 128))], whole((TP, LS, 128)))(arrived)
    full1 = exchange(own, "tp")
    pay = call(
        scaled_body,
        shape((DP, LS, 384)),
        [whole((TP, LS, 128)), whole((LS, 128))],
        whole((DP, LS, 384)),
    )(full1, norm)
    got = exchange(pay, "dp")
    hidden = call(
        final_body,
        shape((256, 256)),
        [whole((DP, LS, 384)), whole((TP, 8, 256)), whole((256, 256)), pair],
        whole((256, 256)),
    )(got, full0, tokens, post_gain)
    return (hidden, state)


def solution(mesh):
    in_specs = (
        P(None, "dp"),
        P(None, "dp", "tp"),
        P(None, "dp"),
        P(None, "dp", "tp"),
        P(None, "dp", "tp"),
        P(None, "dp", "tp"),
        P(None, "dp", "tp"),
        P(None, "dp", "tp"),
        P(None, "tp"),
        P(),
        P(None, "tp", "dp"),
        P(None, "dp"),
    )
    out_specs = (P(None, "dp"), P(None, "dp", "tp"))

    return jax.shard_map(local, mesh=mesh, in_specs=in_specs, out_specs=out_specs, check_vma=False)
```

time: 184 us -> 156 us (0.85)
  blocking collectives: 81.7 us -> 44.6 us
  starting transfers between devices: 35.8 us -> 64.4 us
  Pallas kernels: 21.4 us -> 9.64 us
  waiting for transfers between devices: 41.7 us -> 35.5 us
    all_to_all x5 -> x3, blocking collectives: 81.7 us -> 44.6 us  [exchange(): came = lax.all_to_all(array, axis, 0, 0, tiled=True)]
    all_to_all x1 -> x5, starting transfers between devices: 10.3 us -> 41.1 us  [exchange(): came = lax.all_to_all(array, axis, 0, 0, tiled=True)]
    ppermute x4, waiting for transfers between devices: 19.9 us -> 8.49 us  [gathered(): now = lax.ppermute(now, 'dp', RING)]
    pallas_call x7 -> x8, Pallas kernels: 18.2 us -> 9.6 us  [the longest x1 2.14 us: local(): call(partial_body, shape((DP, LS, 512)), [whole((256, 256)), pair, *weigh...]
    all_to_all x1 -> x5, waiting for transfers between devices: 20.2 us -> 25 us  [exchange(): came = lax.all_to_all(array, axis, 0, 0, tiled=True)]
    ppermute x3, starting transfers between devices: 11.1 us -> 6.45 us  [gathered(): swapped.append(lax.ppermute(now, 'dp', SWAP))]
    ppermute x4, starting transfers between devices: 10.4 us -> 14.7 us  [gathered(): now = lax.ppermute(now, 'dp', RING)]
    pallas_call x2 -> x1, Pallas kernels: 3.2 us -> 0.04 us  [local(): call(total_body, shape((TP, LS, 128)), [whole((TP, LS, 128))], whole((TP,...]
  transfers between devices with their start and end apart: 10 -> 13, of which waited for: 5 -> 9; matrix products, arithmetic and copies ran while one was open for 1% -> 0% of each run, Pallas kernels for 6% -> 1%
where the time goes in v2:
time: 156 us; the launch traced here: 155 us
  starting transfers between devices  64.4 us (41%)
  blocking collectives  44.6 us (29%)
  waiting for transfers between devices  35.5 us (23%)
  Pallas kernels  9.64 us (6%)
    all_to_all x3, blocking collectives, exchange(): came = lax.all_to_all(array, axis, 0, 0, tiled=True)  44.6 us
    all_to_all x5, starting transfers between devices, exchange(): came = lax.all_to_all(array, axis, 0, 0, tiled=True)  41.1 us
    all_to_all x5, waiting for transfers between devices, exchange(): came = lax.all_to_all(array, axis, 0, 0, tiled=True)  25 us
    ppermute x4, starting transfers between devices, gathered(): now = lax.ppermute(now, 'dp', RING)  14.7 us
    ppermute x4, waiting for transfers between devices, gathered(): now = lax.ppermute(now, 'dp', RING)  8.49 us
    ppermute x3, starting transfers between devices, gathered(): swapped.append(lax.ppermute(now, 'dp', SWAP))  6.45 us
  transfers between devices with their start and end apart: 13, of which 9 were waited for; matrix products, arithmetic and copies ran while one was open for 0% of the time, Pallas kernels for 1%

profile of v2, /device:TPU:1, one launch (start us, length us, event | category | flops | bytes accessed | tf_op | source)
XLA Modules:
  0.0 155.1 jit_solution(9373537221332693798)
XLA Ops:
  0.6 0.0 copy-start
  0.6 2.1 %shard_map.131 = bf16[16,16,512]{2,1,0:T(8,128)(2,1)} custom-call(bf16[256,256]{1,0:T(8,128)(2,1)} %tokens.5, f32[2,256]{1,0:T(2,128)} %pre.3, bf16[2,64,256]{2,1,0:T(8,128)(2,1)} %bitcast.6, bf16[2,64,256]{2,1,0:T(8,128)(2,1)} %bitcast.8, bf16[2,256,128]{2,1,0:T(8,128)(2,1)} %wv.3, bf16[2,256,128]{2,1,0:T(8,128)(2,1)} %wg.3, bf16[2,64,256]{2,1,0:T(8,128)(2,1)} %bitcast.10), custom_call_target="tpu_custom_call" | custom-call | tf_op jit(solution)/shard_map/pallas_call | solution.py:248
  2.8 0.0 copy-start.4
  2.8 10.3 %all-to-all-start = ((bf16[16,16,512]{2,1,0:T(8,128)(2,1)}), bf16[16,16,512]{2,1,0:T(8,128)(2,1)S(1)}, u32[]{:S(2)}, u32[]{:S(2)}) async-start(bf16[16,16,512]{2,1,0:T(8,128)(2,1)} %shard_map.131), calls=%async_computation | async-start | bytes 524288 | tf_op jit(solution)/shard_map/all_to_all | solution.py:242
  13.1 0.0 copy-done.4
  13.1 2.1 %collective-permute-start = (bf16[128,256]{1,0:T(8,128)(2,1)S(1)}, bf16[128,256]{1,0:T(8,128)(2,1)S(1)}, u32[]{:S(2)}, u32[]{:S(2)}) collective-permute-start(bf16[128,256]{1,0:T(8,128)(2,1)S(1)} %get-tuple-element.21), channel_id=1, source_target_pairs={{0,1},{1,0},{2,3},{3,2},{4,5},{5,4},{6,7},{7,6},{8,9},{9,8},{10,11... | collective-permute-start | bytes 196616 | tf_op jit(solution)/shard_map/ppermute | solution.py:217
  15.2 1.0 collective-permute-done
  16.2 0.0 copy-start.10
  16.2 0.0 copy-start.11
  16.3 4.6 %collective-permute-start.1 = (bf16[2,128,256]{2,1,0:T(8,128)(2,1)S(1)}, bf16[2,128,256]{2,1,0:T(8,128)(2,1)S(1)}, u32[]{:S(2)}, u32[]{:S(2)}) collective-permute-start(bf16[2,128,256]{2,1,0:T(8,128)(2,1)S(1)} %pad_maximum_fusion.refs_0_), channel_id=1, source_target_pairs={{0,2},{2,4},{4,6},{6,8},{8,10},{10,12},{12,14},{14,0},{1,15},{3,1}... | collective-permute-start | bytes 393224 | tf_op jit(solution)/shard_map/ppermute | solution.py:223
  20.9 2.0 %collective-permute-done.1.refs_1_ = bf16[2,128,256]{2,1,0:T(8,128)(2,1)S(1)} collective-permute-done((bf16[2,128,256]{2,1,0:T(8,128)(2,1)S(1)}, bf16[2,128,256]{2,1,0:T(8,128)(2,1)S(1)}, u32[]{:S(2)}, u32[]{:S(2)}) %collective-permute-start.1) | collective-permute-done | bytes 131104 | tf_op jit(solution)/shard_map/ppermute | solution.py:223
  22.9 4.9 %collective-permute-start.2 = (bf16[2,128,256]{2,1,0:T(8,128)(2,1)S(1)}, bf16[2,128,256]{2,1,0:T(8,128)(2,1)S(1)}, u32[]{:S(2)}, u32[]{:S(2)}) collective-permute-start(bf16[2,128,256]{2,1,0:T(8,128)(2,1)S(1)} %collective-permute-done.1.refs_1_), channel_id=1, source_target_pairs={{0,2},{2,4},{4,6},{6,8},{8,10},{10,12},{12,14},{14,0},{1,15},{3,1}... | collective-permute-start | bytes 393224 | tf_op jit(solution)/shard_map/ppermute | solution.py:223
  27.8 0.0 all-to-all-done.got
  27.8 0.0 copy-done
  27.8 0.0 copy-done.10
  27.8 0.0 copy-done.11
  27.8 1.4 shard_map.132
  29.3 6.3 %all-to-all-start.1 = ((bf16[16,16,128]{2,1,0:T(8,128)(2,1)}), bf16[16,16,128]{2,1,0:T(8,128)(2,1)S(1)}, u32[]{:S(2)}, u32[]{:S(2)}) async-start(bf16[16,16,128]{2,1,0:T(8,128)(2,1)} %get-tuple-element.12), calls=%async_computation.1 | async-start | bytes 131072 | tf_op jit(solution)/shard_map/all_to_all | solution.py:242
  35.5 0.0 collective-permute-done.2.refs_2_
  35.6 7.8 %all-to-all-done.1.mixed = bf16[16,16,128]{2,1,0:T(8,128)(2,1)S(1)} async-done(((bf16[16,16,128]{2,1,0:T(8,128)(2,1)}), bf16[16,16,128]{2,1,0:T(8,128)(2,1)S(1)}, u32[]{:S(2)}, u32[]{:S(2)}) %all-to-all-start.1) | async-done | bytes 65568 | tf_op jit(solution)/shard_map/all_to_all | solution.py:242
  43.3 0.8 shard_map.133
  44.2 0.0 copy-start.7
  44.2 0.0 copy-start.8
  44.2 0.0 copy-start.9
  44.2 11.4 %all-to-all-start.2 = ((bf16[32,8,256]{2,1,0:T(8,128)(2,1)}), bf16[32,8,256]{2,1,0:T(8,128)(2,1)S(1)}, u32[]{:S(2)}, u32[]{:S(2)}) async-start(bf16[32,8,256]{2,1,0:T(8,128)(2,1)} %shard_map.133), calls=%async_computation.2 | async-start | bytes 262144 | tf_op jit(solution)/shard_map/all_to_all | solution.py:242
  55.6 2.0 %collective-permute-start.3 = (bf16[2,128,256]{2,1,0:T(8,128)(2,1)S(1)}, bf16[2,128,256]{2,1,0:T(8,128)(2,1)S(1)}, u32[]{:S(2)}, u32[]{:S(2)}) collective-permute-start(bf16[2,128,256]{2,1,0:T(8,128)(2,1)S(1)} %collective-permute-done.2.refs_2_), channel_id=1, source_target_pairs={{0,2},{2,4},{4,6},{6,8},{8,10},{10,12},{12,14},{14,0},{1,15},{3,1}... | collective-permute-start | bytes 393224 | tf_op jit(solution)/shard_map/ppermute | solution.py:223
  57.6 4.0 %collective-permute-done.3.refs_3_ = bf16[2,128,256]{2,1,0:T(8,128)(2,1)S(1)} collective-permute-done((bf16[2,128,256]{2,1,0:T(8,128)(2,1)S(1)}, bf16[2,128,256]{2,1,0:T(8,128)(2,1)S(1)}, u32[]{:S(2)}, u32[]{:S(2)}) %collective-permute-start.3) | collective-permute-done | bytes 131104 | tf_op jit(solution)/shard_map/ppermute | solution.py:223
  61.6 3.8 %all-to-all-done.2.arrived = bf16[32,8,256]{2,1,0:T(8,128)(2,1)S(1)} async-done(((bf16[32,8,256]{2,1,0:T(8,128)(2,1)}), bf16[32,8,256]{2,1,0:T(8,128)(2,1)S(1)}, u32[]{:S(2)}, u32[]{:S(2)}) %all-to-all-start.2) | async-done | bytes 131104 | tf_op jit(solution)/shard_map/all_to_all | solution.py:242
  65.4 0.0 copy-start.3
  65.4 0.0 copy-start.5
  65.4 0.0 copy-start.6
  65.4 0.7 shard_map.134
  66.1 0.0 copy-start.1
  66.1 0.0 copy-start.2
  66.1 5.2 %all-to-all-start.3 = ((bf16[32,8,256]{2,1,0:T(8,128)(2,1)}), bf16[32,8,256]{2,1,0:T(8,128)(2,1)S(1)}, u32[]{:S(2)}, u32[]{:S(2)}) async-start(bf16[32,8,256]{2,1,0:T(8,128)(2,1)} %shard_map.134), calls=%async_computation.3 | async-start | bytes 262144 | tf_op jit(solution)/shard_map/all_to_all | solution.py:242
  71.4 3.2 %collective-permute-start.4 = (bf16[2,128,256]{2,1,0:T(8,128)(2,1)S(1)}, bf16[2,128,256]{2,1,0:T(8,128)(2,1)S(1)}, u32[]{:S(2)}, u32[]{:S(2)}) collective-permute-start(bf16[2,128,256]{2,1,0:T(8,128)(2,1)S(1)} %collective-permute-done.3.refs_3_), channel_id=1, source_target_pairs={{0,2},{2,4},{4,6},{6,8},{8,10},{10,12},{12,14},{14,0},{1,15},{3,1}... | collective-permute-start | bytes 393224 | tf_op jit(solution)/shard_map/ppermute | solution.py:223
  74.6 2.5 %collective-permute-done.4.refs_4_ = bf16[2,128,256]{2,1,0:T(8,128)(2,1)S(1)} collective-permute-done((bf16[2,128,256]{2,1,0:T(8,128)(2,1)S(1)}, bf16[2,128,256]{2,1,0:T(8,128)(2,1)S(1)}, u32[]{:S(2)}, u32[]{:S(2)}) %collective-permute-start.4) | collective-permute-done | bytes 131104 | tf_op jit(solution)/shard_map/ppermute | solution.py:223
  77.1 3.6 %all-to-all-done.3.full = bf16[32,8,256]{2,1,0:T(8,128)(2,1)S(1)} async-done(((bf16[32,8,256]{2,1,0:T(8,128)(2,1)}), bf16[32,8,256]{2,1,0:T(8,128)(2,1)S(1)}, u32[]{:S(2)}, u32[]{:S(2)}) %all-to-all-start.3) | async-done | bytes 131104 | tf_op jit(solution)/shard_map/all_to_all | solution.py:242
  80.7 0.0 copy-done.7
  80.7 0.0 copy-done.8
  80.7 0.0 copy-done.9
  80.7 0.0 copy-done.3
  80.7 0.0 copy-done.5
  80.7 0.0 copy-done.6
  80.8 0.0 copy-done.1
  80.8 0.0 copy-done.2
  80.8 1.4 shard_map.135
  82.2 7.8 %all-to-all-start.4 = ((bf16[16,16,1024]{2,1,0:T(8,128)(2,1)}), bf16[16,16,1024]{2,1,0:T(8,128)(2,1)S(1)}, u32[]{:S(2)}, u32[]{:S(2)}) async-start(bf16[16,16,1024]{2,1,0:T(8,128)(2,1)} %shard_map.135), calls=%async_computation.4 | async-start | bytes 1048576 | tf_op jit(solution)/shard_map/all_to_all | solution.py:242
  90.0 2.1 %collective-permute-start.5 = (bf16[2,128,256]{2,1,0:T(8,128)(2,1)S(1)}, bf16[2,128,256]{2,1,0:T(8,128)(2,1)S(1)}, u32[]{:S(2)}, u32[]{:S(2)}) collective-permute-start(bf16[2,128,256]{2,1,0:T(8,128)(2,1)S(1)} %collective-permute-done.1.refs_1_), channel_id=1, source_target_pairs={{0,1},{1,0},{2,3},{3,2},{4,5},{5,4},{6,7},{7,6},{8,9},{9,8},{10,11... | collective-permute-start | bytes 393224 | tf_op jit(solution)/shard_map/ppermute | solution.py:226
  92.1 2.2 %collective-permute-start.6 = (bf16[2,128,256]{2,1,0:T(8,128)(2,1)S(1)}, bf16[2,128,256]{2,1,0:T(8,128)(2,1)S(1)}, u32[]{:S(2)}, u32[]{:S(2)}) collective-permute-start(bf16[2,128,256]{2,1,0:T(8,128)(2,1)S(1)} %collective-permute-done.2.refs_2_), channel_id=1, source_target_pairs={{0,1},{1,0},{2,3},{3,2},{4,5},{5,4},{6,7},{7,6},{8,9},{9,8},{10,11... | collective-permute-start | bytes 393224 | tf_op jit(solution)/shard_map/ppermute | solution.py:226
  94.3 2.1 %collective-permute-start.7 = (bf16[2,128,256]{2,1,0:T(8,128)(2,1)S(1)}, bf16[2,128,256]{2,1,0:T(8,128)(2,1)S(1)}, u32[]{:S(2)}, u32[]{:S(2)}) collective-permute-start(bf16[2,128,256]{2,1,0:T(8,128)(2,1)S(1)} %collective-permute-done.3.refs_3_), channel_id=1, source_target_pairs={{0,1},{1,0},{2,3},{3,2},{4,5},{5,4},{6,7},{7,6},{8,9},{9,8},{10,11... | collective-permute-start | bytes 393224 | tf_op jit(solution)/shard_map/ppermute | solution.py:226
  96.5 0.0 collective-permute-done.5.refs_5_
  96.5 0.0 collective-permute-done.6.refs_6_
  96.5 1.1 collective-permute-done.7.refs_7_
  97.6 9.7 %all-to-all-done.4.got = bf16[16,16,1024]{2,1,0:T(8,128)(2,1)S(1)} async-done(((bf16[16,16,1024]{2,1,0:T(8,128)(2,1)}), bf16[16,16,1024]{2,1,0:T(8,128)(2,1)S(1)}, u32[]{:S(2)}, u32[]{:S(2)}) %all-to-all-start.4) | async-done | bytes 524320 | tf_op jit(solution)/shard_map/all_to_all | solution.py:242
  107.3 2.1 %shard_map.136 = (f32[2,16,8192]{2,1,0:T(8,128)}, bf16[32,16,128]{2,1,0:T(8,128)(2,1)S(1)}, f32[16,128]{1,0:T(8,128)S(1)}) custom-call(bf16[16,16,1024]{2,1,0:T(8,128)(2,1)S(1)} %all-to-all-done.4.got, f32[2,64]{1,0:T(2,128)S(1)} %copy-done.10, f32[2,128]{1,0:T(2,128)S(1)} %copy-done.11, ...), custom_call_target="tpu_custom_call", output_to_operand_aliasing={{0}: (4, {})} | custom-call | tf_op jit(solution)/shard_map/pallas_call | solution.py:282
  109.4 17.2 %all_to_all.40.arrived = bf16[32,16,128]{2,1,0:T(8,128)(2,1)S(1)} all-to-all(bf16[32,16,128]{2,1,0:T(8,128)(2,1)S(1)} %get-tuple-element.17), channel_id=1, replica_groups=mesh['tp'=32,'dp'=16] {'tp'}, dimensions={0} | all-to-all | bytes 262144 | tf_op jit(solution)/shard_map/all_to_all | solution.py:242
  126.7 12.7 %all_to_all.41.full = bf16[32,16,128]{2,1,0:T(8,128)(2,1)S(1)} all-to-all(bf16[32,16,128]{2,1,0:T(8,128)(2,1)S(1)} %shard_map.137), channel_id=1, replica_groups=mesh['tp'=32,'dp'=16] {'tp'}, dimensions={0} | all-to-all | bytes 262144 | tf_op jit(solution)/shard_map/all_to_all | solution.py:242
  139.4 0.1 shard_map.138
  139.5 14.7 %all_to_all.42.got = bf16[16,16,384]{2,1,0:T(8,128)(2,1)S(1)} all-to-all(bf16[16,16,384]{2,1,0:T(8,128)(2,1)S(1)} %shard_map.138), channel_id=1, replica_groups=mesh['tp'=32,'dp'=16] {'dp'}, dimensions={0} | all-to-all | bytes 393216 | tf_op jit(solution)/shard_map/all_to_all | solution.py:242
  154.2 0.9 shard_map.139
  (3 shorter events, 0.1 us)
Async XLA Ops:
  0.6 27.2 %copy-start = (f32[2,16,8192]{2,1,0:T(8,128)S(1)}, f32[2,16,8192]{2,1,0:T(8,128)}, u32[]{:S(2)}) copy-start(f32[2,16,8192]{2,1,0:T(8,128)} %old.3) | copy-start | bytes 3145732
  2.8 10.3 %copy-start.4 = (bf16[2,128,256]{2,1,0:T(8,128)(2,1)S(1)}, bf16[2,128,256]{2,1,0:T(8,128)(2,1)}, u32[]{:S(2)}) copy-start(bf16[2,128,256]{2,1,0:T(8,128)(2,1)} %wo.1) | copy-start | bytes 393220
  2.8 25.0 %all-to-all-start = ((bf16[16,16,512]{2,1,0:T(8,128)(2,1)}), bf16[16,16,512]{2,1,0:T(8,128)(2,1)S(1)}, u32[]{:S(2)}, u32[]{:S(2)}) async-start(bf16[16,16,512]{2,1,0:T(8,128)(2,1)} %shard_map.131), calls=%async_computation | async-start | bytes 524288 | tf_op jit(solution)/shard_map/all_to_all | solution.py:242
  13.1 3.1 %collective-permute-start = (bf16[128,256]{1,0:T(8,128)(2,1)S(1)}, bf16[128,256]{1,0:T(8,128)(2,1)S(1)}, u32[]{:S(2)}, u32[]{:S(2)}) collective-permute-start(bf16[128,256]{1,0:T(8,128)(2,1)S(1)} %get-tuple-element.21), channel_id=1, source_target_pairs={{0,1},{1,0},{2,3},{3,2},{4,5},{5,4},{6,7},{7,6},{8,9},{9,8},{10,11... | collective-permute-start | bytes 196616 | tf_op jit(solution)/shard_map/ppermute | solution.py:217
  16.2 11.6 %copy-start.10 = (f32[2,64]{1,0:T(2,128)S(1)}, f32[2,64]{1,0:T(2,128)}, u32[]{:S(2)}) copy-start(f32[2,64]{1,0:T(2,128)} %bias.3) | copy-start | bytes 1540
  16.2 11.6 %copy-start.11 = (f32[2,128]{1,0:T(2,128)S(1)}, f32[2,128]{1,0:T(2,128)}, u32[]{:S(2)}) copy-start(f32[2,128]{1,0:T(2,128)} %gain.3) | copy-start | bytes 3076
  16.3 6.6 %collective-permute-start.1 = (bf16[2,128,256]{2,1,0:T(8,128)(2,1)S(1)}, bf16[2,128,256]{2,1,0:T(8,128)(2,1)S(1)}, u32[]{:S(2)}, u32[]{:S(2)}) collective-permute-start(bf16[2,128,256]{2,1,0:T(8,128)(2,1)S(1)} %pad_maximum_fusion.refs_0_), channel_id=1, source_target_pairs={{0,2},{2,4},{4,6},{6,8},{8,10},{10,12},{12,14},{14,0},{1,15},{3,1}... | collective-permute-start | bytes 393224 | tf_op jit(solution)/shard_map/ppermute | solution.py:223
  22.9 12.6 %collective-permute-start.2 = (bf16[2,128,256]{2,1,0:T(8,128)(2,1)S(1)}, bf16[2,128,256]{2,1,0:T(8,128)(2,1)S(1)}, u32[]{:S(2)}, u32[]{:S(2)}) collective-permute-start(bf16[2,128,256]{2,1,0:T(8,128)(2,1)S(1)} %collective-permute-done.1.refs_1_), channel_id=1, source_target_pairs={{0,2},{2,4},{4,6},{6,8},{8,10},{10,12},{12,14},{14,0},{1,15},{3,1}... | collective-permute-start | bytes 393224 | tf_op jit(solution)/shard_map/ppermute | solution.py:223
  29.3 14.1 %all-to-all-start.1 = ((bf16[16,16,128]{2,1,0:T(8,128)(2,1)}), bf16[16,16,128]{2,1,0:T(8,128)(2,1)S(1)}, u32[]{:S(2)}, u32[]{:S(2)}) async-start(bf16[16,16,128]{2,1,0:T(8,128)(2,1)} %get-tuple-element.12), calls=%async_computation.1 | async-start | bytes 131072 | tf_op jit(solution)/shard_map/all_to_all | solution.py:242
  44.2 36.6 %copy-start.7 = (bf16[2,256,64]{1,2,0:T(8,128)(2,1)S(1)}, bf16[2,256,64]{1,2,0:T(8,128)(2,1)}, u32[]{:S(2)}) copy-start(bf16[2,256,64]{1,2,0:T(8,128)(2,1)} %param.19) | copy-start | bytes 196612
  44.2 36.6 %copy-start.8 = (f32[2,256]{1,0:T(2,128)S(1)}, f32[2,256]{1,0:T(2,128)}, u32[]{:S(2)}) copy-start(f32[2,256]{1,0:T(2,128)} %pre.3) | copy-start | bytes 6148
  44.2 36.6 %copy-start.9 = (f32[2,256]{1,0:T(2,128)S(1)}, f32[2,256]{1,0:T(2,128)}, u32[]{:S(2)}) copy-start(f32[2,256]{1,0:T(2,128)} %post.3) | copy-start | bytes 6148
  44.2 21.3 %all-to-all-start.2 = ((bf16[32,8,256]{2,1,0:T(8,128)(2,1)}), bf16[32,8,256]{2,1,0:T(8,128)(2,1)S(1)}, u32[]{:S(2)}, u32[]{:S(2)}) async-start(bf16[32,8,256]{2,1,0:T(8,128)(2,1)} %shard_map.133), calls=%async_computation.2 | async-start | bytes 262144 | tf_op jit(solution)/shard_map/all_to_all | solution.py:242
  55.6 6.0 %collective-permute-start.3 = (bf16[2,128,256]{2,1,0:T(8,128)(2,1)S(1)}, bf16[2,128,256]{2,1,0:T(8,128)(2,1)S(1)}, u32[]{:S(2)}, u32[]{:S(2)}) collective-permute-start(bf16[2,128,256]{2,1,0:T(8,128)(2,1)S(1)} %collective-permute-done.2.refs_2_), channel_id=1, source_target_pairs={{0,2},{2,4},{4,6},{6,8},{8,10},{10,12},{12,14},{14,0},{1,15},{3,1}... | collective-permute-start | bytes 393224 | tf_op jit(solution)/shard_map/ppermute | solution.py:223
  65.4 15.3 %copy-start.3 = (bf16[2,256,128]{2,1,0:T(8,128)(2,1)S(1)}, bf16[2,256,128]{2,1,0:T(8,128)(2,1)}, u32[]{:S(2)}) copy-start(bf16[2,256,128]{2,1,0:T(8,128)(2,1)} %wg.3) | copy-start | bytes 393220
  65.4 15.3 %copy-start.5 = (bf16[2,256,64]{1,2,0:T(8,128)(2,1)S(1)}, bf16[2,256,64]{1,2,0:T(8,128)(2,1)}, u32[]{:S(2)}) copy-start(bf16[2,256,64]{1,2,0:T(8,128)(2,1)} %param.15) | copy-start | bytes 196612
  65.4 15.3 %copy-start.6 = (bf16[2,256,64]{1,2,0:T(8,128)(2,1)S(1)}, bf16[2,256,64]{1,2,0:T(8,128)(2,1)}, u32[]{:S(2)}) copy-start(bf16[2,256,64]{1,2,0:T(8,128)(2,1)} %param.16) | copy-start | bytes 196612
  66.1 14.6 %copy-start.1 = (bf16[256,256]{1,0:T(8,128)(2,1)S(1)}, bf16[256,256]{1,0:T(8,128)(2,1)}, u32[]{:S(2)}) copy-start(bf16[256,256]{1,0:T(8,128)(2,1)} %tokens.5) | copy-start | bytes 393220
  66.1 14.6 %copy-start.2 = (bf16[2,256,128]{2,1,0:T(8,128)(2,1)S(1)}, bf16[2,256,128]{2,1,0:T(8,128)(2,1)}, u32[]{:S(2)}) copy-start(bf16[2,256,128]{2,1,0:T(8,128)(2,1)} %wv.3) | copy-start | bytes 393220
  66.1 14.6 %all-to-all-start.3 = ((bf16[32,8,256]{2,1,0:T(8,128)(2,1)}), bf16[32,8,256]{2,1,0:T(8,128)(2,1)S(1)}, u32[]{:S(2)}, u32[]{:S(2)}) async-start(bf16[32,8,256]{2,1,0:T(8,128)(2,1)} %shard_map.134), calls=%async_computation.3 | async-start | bytes 262144 | tf_op jit(solution)/shard_map/all_to_all | solution.py:242
  71.4 5.7 %collective-permute-start.4 = (bf16[2,128,256]{2,1,0:T(8,128)(2,1)S(1)}, bf16[2,128,256]{2,1,0:T(8,128)(2,1)S(1)}, u32[]{:S(2)}, u32[]{:S(2)}) collective-permute-start(bf16[2,128,256]{2,1,0:T(8,128)(2,1)S(1)} %collective-permute-done.3.refs_3_), channel_id=1, source_target_pairs={{0,2},{2,4},{4,6},{6,8},{8,10},{10,12},{12,14},{14,0},{1,15},{3,1}... | collective-permute-start | bytes 393224 | tf_op jit(solution)/shard_map/ppermute | solution.py:223
  82.2 25.1 %all-to-all-start.4 = ((bf16[16,16,1024]{2,1,0:T(8,128)(2,1)}), bf16[16,16,1024]{2,1,0:T(8,128)(2,1)S(1)}, u32[]{:S(2)}, u32[]{:S(2)}) async-start(bf16[16,16,1024]{2,1,0:T(8,128)(2,1)} %shard_map.135), calls=%async_computation.4 | async-start | bytes 1048576 | tf_op jit(solution)/shard_map/all_to_all | solution.py:242
  90.0 6.5 %collective-permute-start.5 = (bf16[2,128,256]{2,1,0:T(8,128)(2,1)S(1)}, bf16[2,128,256]{2,1,0:T(8,128)(2,1)S(1)}, u32[]{:S(2)}, u32[]{:S(2)}) collective-permute-start(bf16[2,128,256]{2,1,0:T(8,128)(2,1)S(1)} %collective-permute-done.1.refs_1_), channel_id=1, source_target_pairs={{0,1},{1,0},{2,3},{3,2},{4,5},{5,4},{6,7},{7,6},{8,9},{9,8},{10,11... | collective-permute-start | bytes 393224 | tf_op jit(solution)/shard_map/ppermute | solution.py:226
  92.1 4.4 %collective-permute-start.6 = (bf16[2,128,256]{2,1,0:T(8,128)(2,1)S(1)}, bf16[2,128,256]{2,1,0:T(8,128)(2,1)S(1)}, u32[]{:S(2)}, u32[]{:S(2)}) collective-permute-start(bf16[2,128,256]{2,1,0:T(8,128)(2,1)S(1)} %collective-permute-done.2.refs_2_), channel_id=1, source_target_pairs={{0,1},{1,0},{2,3},{3,2},{4,5},{5,4},{6,7},{7,6},{8,9},{9,8},{10,11... | collective-permute-start | bytes 393224 | tf_op jit(solution)/shard_map/ppermute | solution.py:226
  94.3 3.2 %collective-permute-start.7 = (bf16[2,128,256]{2,1,0:T(8,128)(2,1)S(1)}, bf16[2,128,256]{2,1,0:T(8,128)(2,1)S(1)}, u32[]{:S(2)}, u32[]{:S(2)}) collective-permute-start(bf16[2,128,256]{2,1,0:T(8,128)(2,1)S(1)} %collective-permute-done.3.refs_3_), channel_id=1, source_target_pairs={{0,1},{1,0},{2,3},{3,2},{4,5},{5,4},{6,7},{7,6},{8,9},{9,8},{10,11... | collective-permute-start | bytes 393224 | tf_op jit(solution)/shard_map/ppermute | solution.py:226

commit v3 on v2

--- a/solution.py
+++ b/solution.py
@@ -4,7 +4,6 @@
 from jax.experimental import pallas as pl
 from jax.experimental.pallas import tpu as pltpu
 from jax.sharding import PartitionSpec as P
-
 
 D = 4096
 KEY = 64
@@ -15,12 +14,6 @@
 epsilon = 1e-06
 bf16 = jnp.bfloat16
 f32 = jnp.float32
-
-SWAP = [(d, d ^ 1) for d in range(DP)]
-RING = [(2 * y, 2 * ((y + 1) % 8)) for y in range(8)] + [
-    (2 * y + 1, 2 * ((y + 7) % 8) + 1) for y in range(8)
-]
-
 
 def whole(shape, index=None):
     at = index or (0,) * len(shape)
@@ -38,23 +31,6 @@
         input_output_aliases=aliases or {},
         compiler_params=pltpu.CompilerParams(vmem_limit_bytes=limit * 1024 * 1024),
     )
-
-
-def owners():
-    me = lax.axis_index("dp")
-    y = me // 2
-    c = me % 2
-    sign = 2 * c - 1
-    found = []
-    for p in range(8):
-        if p == 0:
-            at, order = y, c
-        elif p <= 4:
-            at, order = (y + sign * p + 8) % 8, c
-        else:
-            at, order = (y - sign * (p - 4) + 8) % 8, 1 - c
-        found.append((2 * at + order, 2 * at + 1 - order))
-    return found
 
 
 def columns(wq, wk, wv, wg, wd):
@@ -131,9 +107,7 @@
             pay[:, :, at : at + 128] = acc.astype(bf16).reshape(DP, LS, 128)
 
 
-def second_state_body(got, bias, gain, old, kept, *refs):
-    pieces = refs[:8]
-    new_ref, out, norm, wide, reads = refs[8:]
+def second_state_body(got, bias, gain, old, kept, new_ref, mixed, wide, reads):
     total = got[0].astype(f32)
     for d in range(1, DP):
         total = total + got[d].astype(f32)
@@ -144,35 +118,37 @@
     scale = lax.rsqrt(stats[0] / D + epsilon)
     squares = stats[1] + 2.0 * scale * stats[2] + scale * scale * stats[3]
     proj = total[:, 512:1024] + scale * total[:, 0:512]
-    norm[...] = jnp.broadcast_to(scale, (LS, 128))
     m = attend(proj, jnp.maximum(squares, 0.0), bias[1:2, :], gain[1:2, :], old, new_ref, wide, reads)
-    for piece, pair in zip(pieces, owners()):
-        for j in range(2):
-            part = jnp.dot(m, piece[j], preferred_element_type=f32).astype(bf16)
-            out[2 * pair[j]] = part[:, 0:128]
-            out[2 * pair[j] + 1] = part[:, 128:256]
-
-
-def scaled_body(full, norm, pay):
-    squares = jnp.zeros((LS, 128), f32)
-    for t in range(TP):
-        o = full[t].astype(f32)
-        squares = squares + o * o
-    scale = lax.rsqrt(jnp.sum(squares, axis=1, keepdims=True) / D + epsilon)
+    for d in range(DP):
+        mixed[d] = m
+
+
+def squares_body(full1, full0, pay):
     lane = lax.broadcasted_iota(jnp.int32, (LS, 128), 1)
-    first = place(jnp.zeros((LS, 128), f32), lane, 0, split3(norm[...])).astype(bf16)
-    for d in range(DP):
-        pay[d, :, 0:128] = (full[2 * d].astype(f32) * scale).astype(bf16)
-        pay[d, :, 128:256] = (full[2 * d + 1].astype(f32) * scale).astype(bf16)
-        pay[d, :, 256:384] = first
-
-
-def final_body(got, full, tokens, post, hidden):
-    came = got[...].astype(f32).reshape(256, 384)
-    scale = came[:, 256:257] + came[:, 257:258] + came[:, 258:259]
-    out = full[...].astype(f32).reshape(256, 256)
-    x = (tokens[...].astype(f32) + out * scale * post[0:1, :]).astype(bf16).astype(f32)
-    hidden[...] = (x + came[:, 0:256] * post[1:2, :]).astype(bf16)
+    acc = jnp.zeros((LS, 128), f32)
+    for i, full in enumerate((full1, full0)):
+        out = full[...].astype(f32).reshape(256, 256)
+        parts = split3(jnp.sum(out * out, axis=1, keepdims=True))
+        for d in range(DP):
+            for j in range(3):
+                acc = jnp.where(lane == 48 * i + 16 * j + d, parts[j][LS * d : LS * d + LS], acc)
+    acc = acc.astype(bf16)
+    for d in range(DP):
+        pay[d] = acc
+
+
+def final_body(got, full1, full0, tokens, post, hidden):
+    total = got[0].astype(f32)
+    for d in range(1, DP):
+        total = total + got[d].astype(f32)
+    total = total + pltpu.roll(total, 112, 1) + pltpu.roll(total, 96, 1)
+    scale = lax.rsqrt(total / D + epsilon)
+    for d in range(DP):
+        at = slice(LS * d, LS * d + LS)
+        outs = [full[2 * d : 2 * d + 2].astype(f32).reshape(LS, 256) for full in (full1, full0)]
+        x = tokens[at, :].astype(f32) + outs[1] * scale[:, 48 + d : 49 + d] * post[0:1, :]
+        x = x.astype(bf16).astype(f32)
+        hidden[at, :] = (x + outs[0] * scale[:, d : d + 1] * post[1:2, :]).astype(bf16)
 
 
 def attend(proj, squares, bias, gain, old, new_ref, wide, reads):
@@ -213,20 +189,6 @@
     return (readout * lax.rsqrt(mean + epsilon) * gain * silu).astype(bf16)
 
 
-def gathered(array):
-    other = lax.ppermute(array, "dp", SWAP)
-    own = jnp.stack([array, other])
-    ring = []
-    swapped = []
-    now = own
-    for k in range(4):
-        now = lax.ppermute(now, "dp", RING)
-        ring.append(now)
-        if k < 3:
-            swapped.append(lax.ppermute(now, "dp", SWAP))
-    return [own, *ring, *swapped]
-
-
 def shape(s, t=bf16):
     return jax.ShapeDtypeStruct(s, t)
 
@@ -238,13 +200,26 @@
     def weight_specs(b):
         return [whole((1, *w.shape[1:]), (b, 0, 0)) for w in weights]
 
-    def exchange(array, axis, beside=None):
-        came = lax.all_to_all(array, axis, 0, 0, tiled=True)
-        if beside is not None:
-            came, _ = lax.optimization_barrier((came, beside))
-        return came
+    def exchange(array, axis):
+        return lax.all_to_all(array, axis, 0, 0, tiled=True)
 
     pair = whole((2, 256))
+    scratch = [pltpu.VMEM((8, 128), f32), pltpu.VMEM((64 * LS, 128), f32)]
+    state_shapes = [shape((2, LS, 8192), f32), shape((DP, LS, 128))]
+    out_spec = whole((TP, 8, 256))
+
+    def shared(mixed, b):
+        mixed = exchange(mixed, "dp")
+        spread = call(
+            first_out_body,
+            shape((TP, 8, 256)),
+            [whole((DP, LS, 128)), whole((1, 128, 256), (b, 0, 0))],
+            out_spec,
+        )(mixed, w_out)
+        arrived = exchange(spread, "tp")
+        own = call(total_body, shape((TP, 8, 256)), [out_spec], out_spec)(arrived)
+        return exchange(own, "tp")
+
     pay = call(
         partial_body,
         shape((DP, LS, 512)),
@@ -252,59 +227,45 @@
         whole((DP, LS, 512)),
         limit=60,
     )(tokens, pre_gain, *weights)
-    pieces = gathered(w_out[1])
-    got = exchange(pay, "dp", pieces[1])
-    scratch = [pltpu.VMEM((8, 128), f32), pltpu.VMEM((64 * LS, 128), f32)]
+    got = exchange(pay, "dp")
     state, mixed = call(
         first_state_body,
-        [shape((2, LS, 8192), f32), shape((DP, LS, 128))],
+        state_shapes,
         [whole((DP, LS, 512)), whole((2, 64)), whole((2, 128)), whole((1, LS, 8192))],
         [whole((1, LS, 8192)), whole((DP, LS, 128))],
         scratch,
     )(got, decay_bias, head_gain, recurrent_state)
-    mixed = exchange(mixed, "dp", pieces[2])
-    spread = call(
-        first_out_body,
-        shape((TP, 8, 256)),
-        [whole((DP, LS, 128)), whole((1, 128, 256))],
-        whole((TP, 8, 256)),
-    )(mixed, w_out)
-    arrived = exchange(spread, "tp", pieces[3])
-    own = call(total_body, shape((TP, 8, 256)), [whole((TP, 8, 256))], whole((TP, 8, 256)))(arrived)
-    full0 = exchange(own, "tp", pieces[4])
+    full0 = shared(mixed, 0)
     pay = call(
         second_partial_body,
         shape((DP, LS, 1024)),
-        [whole((TP, 8, 256)), whole((256, 256)), pair, pair, *weight_specs(1)],
+        [out_spec, whole((256, 256)), pair, pair, *weight_specs(1)],
         whole((DP, LS, 1024)),
     )(full0, tokens, pre_gain, post_gain, *weights)
     got = exchange(pay, "dp")
-    state, spread, norm = call(
+    state, mixed = call(
         second_state_body,
-        [shape((2, LS, 8192), f32), shape((TP, LS, 128)), shape((LS, 128), f32)],
+        state_shapes,
         [whole((DP, LS, 1024)), whole((2, 64)), whole((2, 128))]
-        + [whole((1, LS, 8192), (1, 0, 0)), pl.BlockSpec(memory_space=pl.ANY)]
-        + [whole((2, 128, 256))] * 8,
-        [whole((1, LS, 8192), (1, 0, 0)), whole((TP, LS, 128)), whole((LS, 128))],
+        + [whole((1, LS, 8192), (1, 0, 0)), pl.BlockSpec(memory_space=pl.ANY)],
+        [whole((1, LS, 8192), (1, 0, 0)), whole((DP, LS, 128))],
         scratch,
         {4: 0},
-    )(got, decay_bias, head_gain, recurrent_state, state, *pieces)
-    arrived = exchange(spread, "tp")
-    own = call(total_body, shape((TP, LS, 128)), [whole((TP, LS, 128))], whole((TP, LS, 128)))(arrived)
-    full1 = exchange(own, "tp")
+    )(got, decay_bias, head_gain, recurrent_state, state)
+    full1 = shared(mixed, 1)
     pay = call(
-        scaled_body,
-        shape((DP, LS, 384)),
-        [whole((TP, LS, 128)), whole((LS, 128))],
-        whole((DP, LS, 384)),
-    )(full1, norm)
+        squares_body,
+        shape((DP, LS, 128)),
+        [out_spec, out_spec],
+        whole((DP, LS, 128)),
+    )(full1, full0)
     got = exchange(pay, "dp")
     hidden = call(
         final_body,
         shape((256, 256)),
-        [whole((DP, LS, 384)), whole((TP, 8, 256)), whole((256, 256)), pair],
+        [whole((DP, LS, 128)), out_spec, out_spec, whole((256, 256)), pair],
         whole((256, 256)),
-    )(got, full0, tokens, post_gain)
+    )(got, full1, full0, tokens, post_gain)
     return (hidden, state)
 
 

time: 156 us -> 146 us (0.936)
  blocking collectives: 44.6 us -> 138 us
  starting transfers between devices: 64.4 us -> 0 us
  waiting for transfers between devices: 35.5 us -> 0 us
  Pallas kernels: 9.64 us -> 7.13 us
    all_to_all x3 -> x9, blocking collectives: 44.6 us -> 138 us  [exchange(): return lax.all_to_all(array, axis, 0, 0, tiled=True)]
    all_to_all x5 -> x0, starting transfers between devices: 41.1 us -> none  [exchange(): came = lax.all_to_all(array, axis, 0, 0, tiled=True)]
    all_to_all x5 -> x0, waiting for transfers between devices: 25 us -> none  [exchange(): came = lax.all_to_all(array, axis, 0, 0, tiled=True)]
    ppermute x8 -> x0, starting transfers between devices: 23.3 us -> none  [the longest x4 14.7 us: gathered(): now = lax.ppermute(now, 'dp', RING)]
    ppermute x8 -> x0, waiting for transfers between devices: 10.6 us -> none  [the longest x4 8.49 us: gathered(): now = lax.ppermute(now, 'dp', RING)]
    pallas_call x8 -> x9, Pallas kernels: 7.5 us -> 4.99 us  [the longest x1 1.51 us: local(): call(second_state_body, state_shapes, [whole((DP, LS, 1024)), whole((2, 6...]
  transfers between devices with their start and end apart: 13 -> 0, of which waited for: 9 -> 0; matrix products, arithmetic and copies ran while one was open for 0% -> 0% of each run, Pallas kernels for 1% -> 0%
where the time goes in v3:
time: 146 us
  blocking collectives  138 us (95%)
  Pallas kernels  7.13 us (5%)
    all_to_all x9, blocking collectives, exchange(): return lax.all_to_all(array, axis, 0, 0, tiled=True)  138 us

profile of v3, /device:TPU:1, one launch (start us, length us, event | category | flops | bytes accessed | tf_op | source)
XLA Modules:
  0.0 145.8 jit_solution(8267922364212661947)
XLA Ops:
  0.6 0.0 copy-start
  0.6 2.1 %shard_map.131 = bf16[16,16,512]{2,1,0:T(8,128)(2,1)} custom-call(bf16[256,256]{1,0:T(8,128)(2,1)} %tokens.5, f32[2,256]{1,0:T(2,128)} %pre.3, bf16[2,64,256]{2,1,0:T(8,128)(2,1)} %bitcast.3, bf16[2,64,256]{2,1,0:T(8,128)(2,1)} %bitcast.5, bf16[2,256,128]{2,1,0:T(8,128)(2,1)} %wv.3, bf16[2,256,128]{2,1,0:T(8,128)(2,1)} %wg.3, bf16[2,64,256]{2,1,0:T(8,128)(2,1)} %bitcast.7), custom_call_target="tpu_custom_call" | custom-call | tf_op jit(solution)/shard_map/pallas_call | solution.py:223
  2.8 0.0 copy-start.10
  2.8 0.0 copy-start.11
  2.8 22.0 %all_to_all.45.got = bf16[16,16,512]{2,1,0:T(8,128)(2,1)S(1)} all-to-all(bf16[16,16,512]{2,1,0:T(8,128)(2,1)} %shard_map.131), channel_id=1, replica_groups=mesh['tp'=32,'dp'=16] {'dp'}, dimensions={0} | all-to-all | bytes 524288 | tf_op jit(solution)/shard_map/all_to_all | solution.py:204
  24.8 0.0 copy-done
  24.8 0.0 copy-done.10
  24.8 0.0 copy-done.11
  24.8 1.4 shard_map.132
  26.2 0.0 copy-start.4
  26.2 10.5 %all_to_all.46.mixed = bf16[16,16,128]{2,1,0:T(8,128)(2,1)S(1)} all-to-all(bf16[16,16,128]{2,1,0:T(8,128)(2,1)S(1)} %get-tuple-element.6), channel_id=1, replica_groups=mesh['tp'=32,'dp'=16] {'dp'}, dimensions={0} | all-to-all | bytes 131072 | tf_op jit(solution)/shard_map/all_to_all | solution.py:204
  36.7 0.0 copy-done.4
  36.7 0.2 shard_map.133
  36.9 0.0 copy-start.7
  36.9 0.0 copy-start.8
  36.9 0.0 copy-start.9
  37.0 21.1 %all_to_all.47.arrived = bf16[32,8,256]{2,1,0:T(8,128)(2,1)S(1)} all-to-all(bf16[32,8,256]{2,1,0:T(8,128)(2,1)S(1)} %shard_map.133), channel_id=1, replica_groups=mesh['tp'=32,'dp'=16] {'tp'}, dimensions={0} | all-to-all | bytes 262144 | tf_op jit(solution)/shard_map/all_to_all | solution.py:204
  58.0 0.0 copy-start.3
  58.0 0.0 copy-start.5
  58.0 0.0 copy-start.6
  58.1 0.0 copy-start.1
  58.1 0.0 copy-start.2
  58.1 12.8 %all_to_all.48.full.full0 = bf16[32,8,256]{2,1,0:T(8,128)(2,1)S(1)} all-to-all(bf16[32,8,256]{2,1,0:T(8,128)(2,1)S(1)} %shard_map.134), channel_id=1, replica_groups=mesh['tp'=32,'dp'=16] {'tp'}, dimensions={0} | all-to-all | bytes 262144 | tf_op jit(solution)/shard_map/all_to_all | solution.py:204
  70.9 0.0 copy-done.7
  70.9 0.0 copy-done.8
  70.9 0.0 copy-done.9
  70.9 0.0 copy-done.3
  70.9 0.0 copy-done.5
  71.0 0.0 copy-done.6
  71.0 0.0 copy-done.1
  71.0 0.0 copy-done.2
  71.0 0.6 shard_map.135
  71.6 22.5 %all_to_all.49.got = bf16[16,16,1024]{2,1,0:T(8,128)(2,1)S(1)} all-to-all(bf16[16,16,1024]{2,1,0:T(8,128)(2,1)S(1)} %shard_map.135), channel_id=1, replica_groups=mesh['tp'=32,'dp'=16] {'dp'}, dimensions={0} | all-to-all | bytes 1048576 | tf_op jit(solution)/shard_map/all_to_all | solution.py:204
  94.1 1.5 %shard_map.136 = (f32[2,16,8192]{2,1,0:T(8,128)}, bf16[16,16,128]{2,1,0:T(8,128)(2,1)S(1)}) custom-call(bf16[16,16,1024]{2,1,0:T(8,128)(2,1)S(1)} %all_to_all.49.got, f32[2,64]{1,0:T(2,128)S(1)} %copy-done.10, f32[2,128]{1,0:T(2,128)S(1)} %copy-done.11, f32[2,16,8192]{2,1,0:T(8,128)S(1)} %copy-done, ...), custom_call_target="tpu_custom_call", output_to_operand_aliasing={{0}: (4, {})} | custom-call | tf_op jit(solution)/shard_map/pallas_call | solution.py:246
  95.6 10.5 %all_to_all.50.mixed = bf16[16,16,128]{2,1,0:T(8,128)(2,1)S(1)} all-to-all(bf16[16,16,128]{2,1,0:T(8,128)(2,1)S(1)} %get-tuple-element.8), channel_id=1, replica_groups=mesh['tp'=32,'dp'=16] {'dp'}, dimensions={0} | all-to-all | bytes 131072 | tf_op jit(solution)/shard_map/all_to_all | solution.py:204
  106.1 0.2 shard_map.137
  106.2 12.8 %all_to_all.51.arrived = bf16[32,8,256]{2,1,0:T(8,128)(2,1)S(1)} all-to-all(bf16[32,8,256]{2,1,0:T(8,128)(2,1)S(1)} %shard_map.137), channel_id=1, replica_groups=mesh['tp'=32,'dp'=16] {'tp'}, dimensions={0} | all-to-all | bytes 262144 | tf_op jit(solution)/shard_map/all_to_all | solution.py:204
  119.1 12.7 %all_to_all.52.full1 = bf16[32,8,256]{2,1,0:T(8,128)(2,1)S(1)} all-to-all(bf16[32,8,256]{2,1,0:T(8,128)(2,1)S(1)} %shard_map.138), channel_id=1, replica_groups=mesh['tp'=32,'dp'=16] {'tp'}, dimensions={0} | all-to-all | bytes 262144 | tf_op jit(solution)/shard_map/all_to_all | solution.py:204
  131.8 0.2 shard_map.139
  131.9 13.0 %all_to_all.53.got = bf16[16,16,128]{2,1,0:T(8,128)(2,1)S(1)} all-to-all(bf16[16,16,128]{2,1,0:T(8,128)(2,1)S(1)} %shard_map.139), channel_id=1, replica_groups=mesh['tp'=32,'dp'=16] {'dp'}, dimensions={0} | all-to-all | bytes 131072 | tf_op jit(solution)/shard_map/all_to_all | solution.py:204
  144.9 0.9 shard_map.140
  (2 shorter events, 0.1 us)
Async XLA Ops:
  0.6 24.2 %copy-start = (f32[2,16,8192]{2,1,0:T(8,128)S(1)}, f32[2,16,8192]{2,1,0:T(8,128)}, u32[]{:S(2)}) copy-start(f32[2,16,8192]{2,1,0:T(8,128)} %old.3) | copy-start | bytes 3145732
  2.8 22.0 %copy-start.10 = (f32[2,64]{1,0:T(2,128)S(1)}, f32[2,64]{1,0:T(2,128)}, u32[]{:S(2)}) copy-start(f32[2,64]{1,0:T(2,128)} %bias.3) | copy-start | bytes 1540
  2.8 22.0 %copy-start.11 = (f32[2,128]{1,0:T(2,128)S(1)}, f32[2,128]{1,0:T(2,128)}, u32[]{:S(2)}) copy-start(f32[2,128]{1,0:T(2,128)} %gain.3) | copy-start | bytes 3076
  26.2 10.5 %copy-start.4 = (bf16[2,128,256]{2,1,0:T(8,128)(2,1)S(1)}, bf16[2,128,256]{2,1,0:T(8,128)(2,1)}, u32[]{:S(2)}) copy-start(bf16[2,128,256]{2,1,0:T(8,128)(2,1)} %wo.3) | copy-start | bytes 393220
  36.9 34.0 %copy-start.7 = (bf16[2,256,64]{1,2,0:T(8,128)(2,1)S(1)}, bf16[2,256,64]{1,2,0:T(8,128)(2,1)}, u32[]{:S(2)}) copy-start(bf16[2,256,64]{1,2,0:T(8,128)(2,1)} %param.19) | copy-start | bytes 196612
  36.9 34.0 %copy-start.8 = (f32[2,256]{1,0:T(2,128)S(1)}, f32[2,256]{1,0:T(2,128)}, u32[]{:S(2)}) copy-start(f32[2,256]{1,0:T(2,128)} %pre.3) | copy-start | bytes 6148
  36.9 34.0 %copy-start.9 = (f32[2,256]{1,0:T(2,128)S(1)}, f32[2,256]{1,0:T(2,128)}, u32[]{:S(2)}) copy-start(f32[2,256]{1,0:T(2,128)} %post.3) | copy-start | bytes 6148
  58.0 12.9 %copy-start.3 = (bf16[2,256,128]{2,1,0:T(8,128)(2,1)S(1)}, bf16[2,256,128]{2,1,0:T(8,128)(2,1)}, u32[]{:S(2)}) copy-start(bf16[2,256,128]{2,1,0:T(8,128)(2,1)} %wg.3) | copy-start | bytes 393220
  58.0 12.9 %copy-start.5 = (bf16[2,256,64]{1,2,0:T(8,128)(2,1)S(1)}, bf16[2,256,64]{1,2,0:T(8,128)(2,1)}, u32[]{:S(2)}) copy-start(bf16[2,256,64]{1,2,0:T(8,128)(2,1)} %param.15) | copy-start | bytes 196612
  58.0 12.9 %copy-start.6 = (bf16[2,256,64]{1,2,0:T(8,128)(2,1)S(1)}, bf16[2,256,64]{1,2,0:T(8,128)(2,1)}, u32[]{:S(2)}) copy-start(bf16[2,256,64]{1,2,0:T(8,128)(2,1)} %param.16) | copy-start | bytes 196612
  58.1 12.9 %copy-start.1 = (bf16[256,256]{1,0:T(8,128)(2,1)S(1)}, bf16[256,256]{1,0:T(8,128)(2,1)}, u32[]{:S(2)}) copy-start(bf16[256,256]{1,0:T(8,128)(2,1)} %tokens.5) | copy-start | bytes 393220
  58.1 12.9 %copy-start.2 = (bf16[2,256,128]{2,1,0:T(8,128)(2,1)S(1)}, bf16[2,256,128]{2,1,0:T(8,128)(2,1)}, u32[]{:S(2)}) copy-start(bf16[2,256,128]{2,1,0:T(8,128)(2,1)} %wv.3) | copy-start | bytes 393220

commit v4 on v3

--- a/solution.py
+++ b/solution.py
@@ -51,7 +51,15 @@
     return acc
 
 
-def partial_body(tokens, pre, wq, wk, wv, wg, wd, pay):
+def late_columns(wd):
+    return jnp.concatenate([jnp.zeros((64, 256), f32), wd[0].astype(f32)], axis=0).T.astype(bf16)
+
+
+def turned_columns(wq, wk):
+    return jnp.concatenate([wq[0], wk[0]], axis=0).astype(f32).T.astype(bf16)
+
+
+def partial_body(tokens, pre, wq, wk, wv, wg, wd, wd1, pay):
     x = tokens[...].astype(f32)
     squares = jnp.sum(x * x, axis=1, keepdims=True)
     normed = (x * pre[0:1, :]).astype(bf16)
@@ -59,18 +67,31 @@
     for i, w in enumerate(columns(wq, wk, wv, wg, wd)):
         acc = jnp.dot(normed, w, preferred_element_type=f32)
         if i == 3:
-            acc = place(acc, lane, 64, split3(squares))
+            late = (x * pre[1:2, :]).astype(bf16)
+            acc = acc + jnp.dot(late, late_columns(wd1), preferred_element_type=f32)
+            acc = place(acc, lane, 125, split3(squares))
         pay[:, :, 128 * i : 128 * i + 128] = acc.astype(bf16).reshape(DP, LS, 128)
 
 
-def first_state_body(got, bias, gain, old, new_ref, mixed, wide, reads):
-    proj = got[0].astype(f32)
+def summed(came, start):
+    total = came[0, :, start : start + 128].astype(f32)
     for d in range(1, DP):
-        proj = proj + got[d].astype(f32)
-    squares = proj[:, 448:449] + proj[:, 449:450] + proj[:, 450:451]
-    m = attend(proj, squares, bias[0:1, :], gain[0:1, :], old, new_ref, wide, reads)
+        total = total + came[d, :, start : start + 128].astype(f32)
+    return total
+
+
+def last_three(tile):
+    return tile[:, 125:126] + tile[:, 126:127] + tile[:, 127:128]
+
+
+def first_state_body(got, bias, gain, old, tokens, pre, wq1, wk1, new_ref, pay, wide, reads):
+    tiles = [summed(got, 128 * i) for i in range(4)]
+    m = attend(tiles, last_three(tiles[3]), bias[0:1, :], gain[0:1, :], old, new_ref, wide, reads)
+    late = (tokens[...].astype(f32) * pre[1:2, :]).astype(bf16)
+    part = jnp.dot(late, turned_columns(wq1, wk1), preferred_element_type=f32)
+    pay[:, :, 128:256] = part.astype(bf16).reshape(DP, LS, 128)
     for d in range(DP):
-        mixed[d] = m
+        pay[d, :, 0:128] = m
 
 
 def first_out_body(mixed, wo, out):
@@ -93,32 +114,34 @@
     out = full[...].astype(f32).reshape(256, 256)
     step = out * post[0:1, :]
     stats = []
-    for value in (out * out, x * x, x * step, step * step):
+    for value in (out * out, x * step, step * step):
         stats += split3(jnp.sum(value, axis=1, keepdims=True))
     gain = pre[1:2, :]
-    lhs = ((step * gain).astype(bf16), (x * gain).astype(bf16))
+    lhs, late = (step * gain).astype(bf16), (x * gain).astype(bf16)
     lane = lax.broadcasted_iota(jnp.int32, (256, 128), 1)
-    for i, w in enumerate(columns(wq, wk, wv, wg, wd)):
-        for j in range(2):
-            acc = jnp.dot(lhs[j], w, preferred_element_type=f32)
-            if i == 3 and j == 0:
-                acc = place(acc, lane, 64, stats)
-            at = 512 * j + 128 * i
-            pay[:, :, at : at + 128] = acc.astype(bf16).reshape(DP, LS, 128)
-
-
-def second_state_body(got, bias, gain, old, kept, new_ref, mixed, wide, reads):
-    total = got[0].astype(f32)
-    for d in range(1, DP):
-        total = total + got[d].astype(f32)
+    tiles = columns(wq, wk, wv, wg, wd)
+    results = [jnp.dot(lhs, w, preferred_element_type=f32) for w in tiles]
+    ends = jnp.dot(late, late_columns(wd), preferred_element_type=f32)
+    results[3] = place(jnp.where(lane >= 125, ends, results[3]), lane, 64, stats)
+    results += [jnp.dot(late, w, preferred_element_type=f32) for w in tiles[1:3]]
+    for i, acc in enumerate(results):
+        pay[:, :, 128 * i : 128 * i + 128] = acc.astype(bf16).reshape(DP, LS, 128)
+
+
+def second_state_body(got, first, mid, bias, gain, old, kept, new_ref, mixed, wide, reads):
+    step = [summed(got, 128 * i) for i in range(4)]
+    early = summed(first, 0)
     stats = []
-    for i in range(4):
-        at = 448 + 3 * i
-        stats.append(total[:, at : at + 1] + total[:, at + 1 : at + 2] + total[:, at + 2 : at + 3])
+    for i in range(3):
+        at = 64 + 3 * i
+        stats.append(step[3][:, at : at + 1] + step[3][:, at + 1 : at + 2] + step[3][:, at + 2 : at + 3])
     scale = lax.rsqrt(stats[0] / D + epsilon)
-    squares = stats[1] + 2.0 * scale * stats[2] + scale * scale * stats[3]
-    proj = total[:, 512:1024] + scale * total[:, 0:512]
-    m = attend(proj, jnp.maximum(squares, 0.0), bias[1:2, :], gain[1:2, :], old, new_ref, wide, reads)
+    squares = last_three(early) + 2.0 * scale * stats[1] + scale * scale * stats[2]
+    lane = lax.broadcasted_iota(jnp.int32, (LS, 128), 1)
+    decay = pltpu.roll(jnp.where(lane >= 125, step[3], early), 64, 1)
+    base = [summed(mid, 0), summed(got, 512), summed(got, 640), decay]
+    tiles = [x + scale * b for x, b in zip(base, step)]
+    m = attend(tiles, jnp.maximum(squares, 0.0), bias[1:2, :], gain[1:2, :], old, new_ref, wide, reads)
     for d in range(DP):
         mixed[d] = m
 
@@ -151,19 +174,19 @@
         hidden[at, :] = (x + outs[0] * scale[:, d : d + 1] * post[1:2, :]).astype(bf16)
 
 
-def attend(proj, squares, bias, gain, old, new_ref, wide, reads):
+def attend(tiles, squares, bias, gain, old, new_ref, wide, reads):
     scale = lax.rsqrt(squares / D + epsilon)
     lane = lax.broadcasted_iota(jnp.int32, (LS, 128), 1)
     low = lane < 64
-    qk = (proj[:, 0:128] * scale).astype(bf16).astype(f32)
+    qk = (tiles[0] * scale).astype(bf16).astype(f32)
     kq = pltpu.roll(qk, 64, 1)
     query = jnp.where(low, qk, kq)
     key = jnp.where(low, kq, qk)
-    value = proj[:, 128:256] * scale
-    gate = proj[:, 256:384] * scale
+    value = tiles[1] * scale
+    gate = tiles[2] * scale
     wide[0:1, 0:64] = bias
     wide[0:1, 64:128] = jnp.zeros((1, 64), f32)
-    z = proj[:, 384:512] * scale + wide[0:1, :]
+    z = tiles[3] * scale + wide[0:1, :]
     log_decay = (jnp.minimum(z, 0.0) - jnp.log1p(jnp.exp(-jnp.abs(z)))) / 16.0
     decay = jnp.exp(log_decay)
     decay = jnp.where(low, decay, pltpu.roll(decay, 64, 1))
@@ -204,12 +227,11 @@
         return lax.all_to_all(array, axis, 0, 0, tiled=True)
 
     pair = whole((2, 256))
+    second_narrow = whole((1, 64, 256), (1, 0, 0))
     scratch = [pltpu.VMEM((8, 128), f32), pltpu.VMEM((64 * LS, 128), f32)]
-    state_shapes = [shape((2, LS, 8192), f32), shape((DP, LS, 128))]
     out_spec = whole((TP, 8, 256))
 
     def shared(mixed, b):
-        mixed = exchange(mixed, "dp")
         spread = call(
             first_out_body,
             shape((TP, 8, 256)),
@@ -223,36 +245,38 @@
     pay = call(
         partial_body,
         shape((DP, LS, 512)),
-        [whole((256, 256)), pair, *weight_specs(0)],
+        [whole((256, 256)), pair, *weight_specs(0), second_narrow],
         whole((DP, LS, 512)),
-        limit=60,
-    )(tokens, pre_gain, *weights)
+    )(*(pltpu.with_memory_space_constraint(a, pltpu.HBM) for a in (tokens, pre_gain, *weights, weights[4])))
     got = exchange(pay, "dp")
     state, mixed = call(
         first_state_body,
-        state_shapes,
-        [whole((DP, LS, 512)), whole((2, 64)), whole((2, 128)), whole((1, LS, 8192))],
-        [whole((1, LS, 8192)), whole((DP, LS, 128))],
+        [shape((2, LS, 8192), f32), shape((DP, LS, 256))],
+        [whole((DP, LS, 512)), whole((2, 64)), whole((2, 128)), whole((1, LS, 8192))]
+        + [whole((256, 256)), pair, second_narrow, second_narrow],
+        [whole((1, LS, 8192)), whole((DP, LS, 256))],
         scratch,
-    )(got, decay_bias, head_gain, recurrent_state)
-    full0 = shared(mixed, 0)
+    )(got, decay_bias, head_gain, recurrent_state, tokens, pre_gain, weights[0], weights[1])
+    first, mid = got, exchange(mixed, "dp")
+    full0 = shared(mid, 0)
     pay = call(
         second_partial_body,
-        shape((DP, LS, 1024)),
+        shape((DP, LS, 768)),
         [out_spec, whole((256, 256)), pair, pair, *weight_specs(1)],
-        whole((DP, LS, 1024)),
+        whole((DP, LS, 768)),
     )(full0, tokens, pre_gain, post_gain, *weights)
     got = exchange(pay, "dp")
     state, mixed = call(
         second_state_body,
-        state_shapes,
-        [whole((DP, LS, 1024)), whole((2, 64)), whole((2, 128))]
+        [shape((2, LS, 8192), f32), shape((DP, LS, 128))],
+        [whole((DP, LS, 768)), whole((DP, LS, 128), (0, 0, 3)), whole((DP, LS, 128), (0, 0, 1))]
+        + [whole((2, 64)), whole((2, 128))]
         + [whole((1, LS, 8192), (1, 0, 0)), pl.BlockSpec(memory_space=pl.ANY)],
         [whole((1, LS, 8192), (1, 0, 0)), whole((DP, LS, 128))],
         scratch,
-        {4: 0},
-    )(got, decay_bias, head_gain, recurrent_state, state)
-    full1 = shared(mixed, 1)
+        {6: 0},
+    )(got, first, mid, decay_bias, head_gain, recurrent_state, state)
+    full1 = shared(exchange(mixed, "dp"), 1)
     pay = call(
         squares_body,
         shape((DP, LS, 128)),

time: 146 us -> 144 us (0.986)
  blocking collectives: 138 us -> 136 us
    all_to_all x9, blocking collectives: 138 us -> 136 us  [exchange(): return lax.all_to_all(array, axis, 0, 0, tiled=True)]
where the time goes in v4:
time: 144 us; the launch traced here: 143 us
  blocking collectives  136 us (94%)
  Pallas kernels  6.52 us (5%)
    all_to_all x9, blocking collectives, exchange(): return lax.all_to_all(array, axis, 0, 0, tiled=True)  136 us

profile of v4, /device:TPU:1, one launch (start us, length us, event | category | flops | bytes accessed | tf_op | source)
XLA Modules:
  0.0 143.2 jit_solution(994578932041799400)
XLA Ops:
  0.6 0.0 copy-start
  0.6 1.5 %shard_map.131 = bf16[16,16,512]{2,1,0:T(8,128)(2,1)S(1)} custom-call(bf16[256,256]{1,0:T(8,128)(2,1)} %tokens.7, f32[2,256]{1,0:T(2,128)} %pre.5, bf16[2,64,256]{2,1,0:T(8,128)(2,1)} %bitcast.6, bf16[2,64,256]{2,1,0:T(8,128)(2,1)} %bitcast.9, bf16[2,256,128]{2,1,0:T(8,128)(2,1)} %wv.3, bf16[2,256,128]{2,1,0:T(8,128)(2,1)} %wg.3, ...), custom_call_target="tpu_custom_call" | custom-call | tf_op jit(solution)/shard_map/pallas_call | solution.py:245
  2.1 0.0 copy-start.1
  2.2 0.0 copy-start.3
  2.2 0.0 copy-start.4
  2.2 0.0 copy-start.8
  2.2 0.0 copy-start.10
  2.2 0.0 copy-start.11
  2.2 21.1 %all_to_all.45.got.first = bf16[16,16,512]{2,1,0:T(8,128)(2,1)S(1)} all-to-all(bf16[16,16,512]{2,1,0:T(8,128)(2,1)S(1)} %shard_map.131), channel_id=1, replica_groups=mesh['tp'=32,'dp'=16] {'dp'}, dimensions={0} | all-to-all | bytes 524288 | tf_op jit(solution)/shard_map/all_to_all | solution.py:227
  23.3 0.0 copy-done
  23.3 0.0 copy-done.1
  23.3 0.0 copy-done.3
  23.4 0.0 copy-done.4
  23.4 0.0 copy-done.8
  23.4 0.0 copy-done.10
  23.4 0.0 copy-done.11
  23.4 1.5 %shard_map.132 = (f32[2,16,8192]{2,1,0:T(8,128)}, bf16[16,16,256]{2,1,0:T(8,128)(2,1)S(1)}) custom-call(bf16[16,16,512]{2,1,0:T(8,128)(2,1)S(1)} %all_to_all.45.got.first, f32[2,64]{1,0:T(2,128)S(1)} %copy-done.10, f32[2,128]{1,0:T(2,128)S(1)} %copy-done.11, f32[2,16,8192]{2,1,0:T(8,128)S(1)} %copy-done, bf16[256,256]{1,0:T(8,128)(2,1)S(1)} %copy-done.1, ...), custom_call_target="tpu_custom_call" | custom-call | tf_op jit(solution)/shard_map/pallas_call | solution.py:252
  24.9 0.0 copy-start.7
  24.9 11.7 %all_to_all.46.mixed.mid = bf16[16,16,256]{2,1,0:T(8,128)(2,1)S(1)} all-to-all(bf16[16,16,256]{2,1,0:T(8,128)(2,1)S(1)} %get-tuple-element.6), channel_id=1, replica_groups=mesh['tp'=32,'dp'=16] {'dp'}, dimensions={0} | all-to-all | bytes 262144 | tf_op jit(solution)/shard_map/all_to_all | solution.py:227
  36.5 0.0 copy-done.7
  36.5 0.2 shard_map.133
  36.7 21.7 %all_to_all.47.arrived = bf16[32,8,256]{2,1,0:T(8,128)(2,1)S(1)} all-to-all(bf16[32,8,256]{2,1,0:T(8,128)(2,1)S(1)} %shard_map.133), channel_id=1, replica_groups=mesh['tp'=32,'dp'=16] {'tp'}, dimensions={0} | all-to-all | bytes 262144 | tf_op jit(solution)/shard_map/all_to_all | solution.py:227
  58.4 0.0 copy-start.6
  58.5 0.0 copy-start.2
  58.5 0.0 copy-start.5
  58.5 0.0 copy-start.9
  58.5 12.8 %all_to_all.48.full.full0 = bf16[32,8,256]{2,1,0:T(8,128)(2,1)S(1)} all-to-all(bf16[32,8,256]{2,1,0:T(8,128)(2,1)S(1)} %shard_map.134), channel_id=1, replica_groups=mesh['tp'=32,'dp'=16] {'tp'}, dimensions={0} | all-to-all | bytes 262144 | tf_op jit(solution)/shard_map/all_to_all | solution.py:227
  71.3 0.0 copy-done.6
  71.3 0.0 copy-done.2
  71.3 0.0 copy-done.5
  71.3 0.0 copy-done.9
  71.3 0.5 shard_map.135
  71.8 19.6 %all_to_all.49.got = bf16[16,16,768]{2,1,0:T(8,128)(2,1)S(1)} all-to-all(bf16[16,16,768]{2,1,0:T(8,128)(2,1)S(1)} %shard_map.135), channel_id=1, replica_groups=mesh['tp'=32,'dp'=16] {'dp'}, dimensions={0} | all-to-all | bytes 786432 | tf_op jit(solution)/shard_map/all_to_all | solution.py:227
  91.5 1.5 %shard_map.136 = (f32[2,16,8192]{2,1,0:T(8,128)}, bf16[16,16,128]{2,1,0:T(8,128)(2,1)S(1)}) custom-call(bf16[16,16,768]{2,1,0:T(8,128)(2,1)S(1)} %all_to_all.49.got, bf16[16,16,512]{2,1,0:T(8,128)(2,1)S(1)} %all_to_all.45.got.first, bf16[16,16,256]{2,1,0:T(8,128)(2,1)S(1)} %all_to_all.46.mixed.mid, ...), custom_call_target="tpu_custom_call", output_to_operand_aliasing={{0}: (6, {})} | custom-call | tf_op jit(solution)/shard_map/pallas_call | solution.py:269
  93.0 10.5 %all_to_all.50.mixed = bf16[16,16,128]{2,1,0:T(8,128)(2,1)S(1)} all-to-all(bf16[16,16,128]{2,1,0:T(8,128)(2,1)S(1)} %get-tuple-element.8), channel_id=1, replica_groups=mesh['tp'=32,'dp'=16] {'dp'}, dimensions={0} | all-to-all | bytes 131072 | tf_op jit(solution)/shard_map/all_to_all | solution.py:227
  103.5 0.2 shard_map.137
  103.6 12.8 %all_to_all.51.arrived = bf16[32,8,256]{2,1,0:T(8,128)(2,1)S(1)} all-to-all(bf16[32,8,256]{2,1,0:T(8,128)(2,1)S(1)} %shard_map.137), channel_id=1, replica_groups=mesh['tp'=32,'dp'=16] {'tp'}, dimensions={0} | all-to-all | bytes 262144 | tf_op jit(solution)/shard_map/all_to_all | solution.py:227
  116.5 12.7 %all_to_all.52.full1 = bf16[32,8,256]{2,1,0:T(8,128)(2,1)S(1)} all-to-all(bf16[32,8,256]{2,1,0:T(8,128)(2,1)S(1)} %shard_map.138), channel_id=1, replica_groups=mesh['tp'=32,'dp'=16] {'tp'}, dimensions={0} | all-to-all | bytes 262144 | tf_op jit(solution)/shard_map/all_to_all | solution.py:227
  129.2 0.2 shard_map.139
  129.3 13.0 %all_to_all.53.got = bf16[16,16,128]{2,1,0:T(8,128)(2,1)S(1)} all-to-all(bf16[16,16,128]{2,1,0:T(8,128)(2,1)S(1)} %shard_map.139), channel_id=1, replica_groups=mesh['tp'=32,'dp'=16] {'dp'}, dimensions={0} | all-to-all | bytes 131072 | tf_op jit(solution)/shard_map/all_to_all | solution.py:227
  142.3 0.9 shard_map.140
  (2 shorter events, 0.1 us)
Async XLA Ops:
  0.6 22.7 %copy-start = (f32[2,16,8192]{2,1,0:T(8,128)S(1)}, f32[2,16,8192]{2,1,0:T(8,128)}, u32[]{:S(2)}) copy-start(f32[2,16,8192]{2,1,0:T(8,128)} %old.3) | copy-start | bytes 3145732
  2.1 21.2 %copy-start.1 = (bf16[256,256]{1,0:T(8,128)(2,1)S(1)}, bf16[256,256]{1,0:T(8,128)(2,1)}, u32[]{:S(2)}) copy-start(bf16[256,256]{1,0:T(8,128)(2,1)} %tokens.7) | copy-start | bytes 393220
  2.2 21.2 %copy-start.3 = (bf16[2,256,64]{1,2,0:T(8,128)(2,1)S(1)}, bf16[2,256,64]{1,2,0:T(8,128)(2,1)}, u32[]{:S(2)}) copy-start(bf16[2,256,64]{1,2,0:T(8,128)(2,1)} %param.15) | copy-start | bytes 196612
  2.2 21.2 %copy-start.4 = (bf16[2,256,64]{1,2,0:T(8,128)(2,1)S(1)}, bf16[2,256,64]{1,2,0:T(8,128)(2,1)}, u32[]{:S(2)}) copy-start(bf16[2,256,64]{1,2,0:T(8,128)(2,1)} %param.16) | copy-start | bytes 196612
  2.2 21.2 %copy-start.8 = (f32[2,256]{1,0:T(2,128)S(1)}, f32[2,256]{1,0:T(2,128)}, u32[]{:S(2)}) copy-start(f32[2,256]{1,0:T(2,128)} %pre.5) | copy-start | bytes 6148
  2.2 21.2 %copy-start.10 = (f32[2,64]{1,0:T(2,128)S(1)}, f32[2,64]{1,0:T(2,128)}, u32[]{:S(2)}) copy-start(f32[2,64]{1,0:T(2,128)} %bias.3) | copy-start | bytes 1540
  2.2 21.2 %copy-start.11 = (f32[2,128]{1,0:T(2,128)S(1)}, f32[2,128]{1,0:T(2,128)}, u32[]{:S(2)}) copy-start(f32[2,128]{1,0:T(2,128)} %gain.3) | copy-start | bytes 3076
  24.9 11.7 %copy-start.7 = (bf16[2,128,256]{2,1,0:T(8,128)(2,1)S(1)}, bf16[2,128,256]{2,1,0:T(8,128)(2,1)}, u32[]{:S(2)}) copy-start(bf16[2,128,256]{2,1,0:T(8,128)(2,1)} %wo.3) | copy-start | bytes 393220
  58.4 12.9 %copy-start.6 = (bf16[2,256,128]{2,1,0:T(8,128)(2,1)S(1)}, bf16[2,256,128]{2,1,0:T(8,128)(2,1)}, u32[]{:S(2)}) copy-start(bf16[2,256,128]{2,1,0:T(8,128)(2,1)} %wg.3) | copy-start | bytes 393220
  58.5 12.8 %copy-start.2 = (bf16[2,256,64]{1,2,0:T(8,128)(2,1)S(1)}, bf16[2,256,64]{1,2,0:T(8,128)(2,1)}, u32[]{:S(2)}) copy-start(bf16[2,256,64]{1,2,0:T(8,128)(2,1)} %param.19) | copy-start | bytes 196612
  58.5 12.8 %copy-start.5 = (bf16[2,256,128]{2,1,0:T(8,128)(2,1)S(1)}, bf16[2,256,128]{2,1,0:T(8,128)(2,1)}, u32[]{:S(2)}) copy-start(bf16[2,256,128]{2,1,0:T(8,128)(2,1)} %wv.3) | copy-start | bytes 393220
  58.5 12.8 %copy-start.9 = (f32[2,256]{1,0:T(2,128)S(1)}, f32[2,256]{1,0:T(2,128)}, u32[]{:S(2)}) copy-start(f32[2,256]{1,0:T(2,128)} %post.3) | copy-start | bytes 6148

commit v5 on v4

--- a/solution.py
+++ b/solution.py
@@ -53,10 +53,6 @@
 
 def late_columns(wd):
     return jnp.concatenate([jnp.zeros((64, 256), f32), wd[0].astype(f32)], axis=0).T.astype(bf16)
-
-
-def turned_columns(wq, wk):
-    return jnp.concatenate([wq[0], wk[0]], axis=0).astype(f32).T.astype(bf16)
 
 
 def partial_body(tokens, pre, wq, wk, wv, wg, wd, wd1, pay):
@@ -84,14 +80,11 @@
     return tile[:, 125:126] + tile[:, 126:127] + tile[:, 127:128]
 
 
-def first_state_body(got, bias, gain, old, tokens, pre, wq1, wk1, new_ref, pay, wide, reads):
+def first_state_body(got, bias, gain, old, new_ref, mixed, wide, reads):
     tiles = [summed(got, 128 * i) for i in range(4)]
     m = attend(tiles, last_three(tiles[3]), bias[0:1, :], gain[0:1, :], old, new_ref, wide, reads)
-    late = (tokens[...].astype(f32) * pre[1:2, :]).astype(bf16)
-    part = jnp.dot(late, turned_columns(wq1, wk1), preferred_element_type=f32)
-    pay[:, :, 128:256] = part.astype(bf16).reshape(DP, LS, 128)
     for d in range(DP):
-        pay[d, :, 0:128] = m
+        mixed[d] = m
 
 
 def first_out_body(mixed, wo, out):
@@ -123,12 +116,12 @@
     results = [jnp.dot(lhs, w, preferred_element_type=f32) for w in tiles]
     ends = jnp.dot(late, late_columns(wd), preferred_element_type=f32)
     results[3] = place(jnp.where(lane >= 125, ends, results[3]), lane, 64, stats)
-    results += [jnp.dot(late, w, preferred_element_type=f32) for w in tiles[1:3]]
+    results += [jnp.dot(late, w, preferred_element_type=f32) for w in tiles[0:3]]
     for i, acc in enumerate(results):
         pay[:, :, 128 * i : 128 * i + 128] = acc.astype(bf16).reshape(DP, LS, 128)
 
 
-def second_state_body(got, first, mid, bias, gain, old, kept, new_ref, mixed, wide, reads):
+def second_state_body(got, first, bias, gain, old, kept, new_ref, mixed, wide, reads):
     step = [summed(got, 128 * i) for i in range(4)]
     early = summed(first, 0)
     stats = []
@@ -139,7 +132,7 @@
     squares = last_three(early) + 2.0 * scale * stats[1] + scale * scale * stats[2]
     lane = lax.broadcasted_iota(jnp.int32, (LS, 128), 1)
     decay = pltpu.roll(jnp.where(lane >= 125, step[3], early), 64, 1)
-    base = [summed(mid, 0), summed(got, 512), summed(got, 640), decay]
+    base = [summed(got, 512), summed(got, 640), summed(got, 768), decay]
     tiles = [x + scale * b for x, b in zip(base, step)]
     m = attend(tiles, jnp.maximum(squares, 0.0), bias[1:2, :], gain[1:2, :], old, new_ref, wide, reads)
     for d in range(DP):
@@ -147,14 +140,15 @@
 
 
 def squares_body(full1, full0, pay):
-    lane = lax.broadcasted_iota(jnp.int32, (LS, 128), 1)
-    acc = jnp.zeros((LS, 128), f32)
+    lane = lax.broadcasted_iota(jnp.int32, (8, 128), 1)
+    acc = jnp.zeros((8, 128), f32)
     for i, full in enumerate((full1, full0)):
         out = full[...].astype(f32).reshape(256, 256)
-        parts = split3(jnp.sum(out * out, axis=1, keepdims=True))
-        for d in range(DP):
-            for j in range(3):
-                acc = jnp.where(lane == 48 * i + 16 * j + d, parts[j][LS * d : LS * d + LS], acc)
+        total = jnp.sum(out * out, axis=1, keepdims=True)
+        high = total.astype(bf16).astype(f32)
+        for j, part in enumerate((high, total - high)):
+            for t in range(TP):
+                acc = jnp.where(lane == 64 * i + 32 * j + t, part[8 * t : 8 * t + 8], acc)
     acc = acc.astype(bf16)
     for d in range(DP):
         pay[d] = acc
@@ -164,14 +158,17 @@
     total = got[0].astype(f32)
     for d in range(1, DP):
         total = total + got[d].astype(f32)
-    total = total + pltpu.roll(total, 112, 1) + pltpu.roll(total, 96, 1)
-    scale = lax.rsqrt(total / D + epsilon)
+    scale = lax.rsqrt((total + pltpu.roll(total, 96, 1)) / D + epsilon)
     for d in range(DP):
         at = slice(LS * d, LS * d + LS)
         outs = [full[2 * d : 2 * d + 2].astype(f32).reshape(LS, 256) for full in (full1, full0)]
-        x = tokens[at, :].astype(f32) + outs[1] * scale[:, 48 + d : 49 + d] * post[0:1, :]
+        rates = [
+            jnp.concatenate([scale[:, i : i + 1], scale[:, i + 1 : i + 2]], axis=0)
+            for i in (2 * d, 64 + 2 * d)
+        ]
+        x = tokens[at, :].astype(f32) + outs[1] * rates[1] * post[0:1, :]
         x = x.astype(bf16).astype(f32)
-        hidden[at, :] = (x + outs[0] * scale[:, d : d + 1] * post[1:2, :]).astype(bf16)
+        hidden[at, :] = (x + outs[0] * rates[0] * post[1:2, :]).astype(bf16)
 
 
 def attend(tiles, squares, bias, gain, old, new_ref, wide, reads):
@@ -195,14 +192,11 @@
         v = jnp.take_along_axis(value, right + 2 * b, axis=1)
         new = decay * old[0, :, b * 128 : b * 128 + 128] + key * v
         new_ref[0, :, b * 128 : b * 128 + 128] = new
-        reads[b * LS : b * LS + LS, :] = query * new
+        reads[b * LS : b * LS + LS, :] = (query * new).astype(bf16)
     row = lax.broadcasted_iota(jnp.int32, (128, 128), 0)
     col = lax.broadcasted_iota(jnp.int32, (128, 128), 1)
     fold = ((row >= 64) == (col % 2 == 1)).astype(f32).astype(bf16)
-    product = reads[...]
-    high = product.astype(bf16)
-    rest = (product - high.astype(f32)).astype(bf16)
-    sums = jnp.dot(high, fold, preferred_element_type=f32) + jnp.dot(rest, fold, preferred_element_type=f32)
+    sums = jnp.dot(reads[...], fold, preferred_element_type=f32)
     readout = jnp.zeros((LS, 128), f32)
     for b in range(64):
         readout = jnp.where(lane // 2 == b, sums[b * LS : b * LS + LS, :], readout)
@@ -228,7 +222,7 @@
 
     pair = whole((2, 256))
     second_narrow = whole((1, 64, 256), (1, 0, 0))
-    scratch = [pltpu.VMEM((8, 128), f32), pltpu.VMEM((64 * LS, 128), f32)]
+    scratch = [pltpu.VMEM((8, 128), f32), pltpu.VMEM((64 * LS, 128), bf16)]
     out_spec = whole((TP, 8, 256))
 
     def shared(mixed, b):
@@ -251,43 +245,42 @@
     got = exchange(pay, "dp")
     state, mixed = call(
         first_state_body,
-        [shape((2, LS, 8192), f32), shape((DP, LS, 256))],
-        [whole((DP, LS, 512)), whole((2, 64)), whole((2, 128)), whole((1, LS, 8192))]
-        + [whole((256, 256)), pair, second_narrow, second_narrow],
-        [whole((1, LS, 8192)), whole((DP, LS, 256))],
+        [shape((2, LS, 8192), f32), shape((DP, LS, 128))],
+        [whole((DP, LS, 512)), whole((2, 64)), whole((2, 128)), whole((1, LS, 8192))],
+        [whole((1, LS, 8192)), whole((DP, LS, 128))],
         scratch,
-    )(got, decay_bias, head_gain, recurrent_state, tokens, pre_gain, weights[0], weights[1])
-    first, mid = got, exchange(mixed, "dp")
-    full0 = shared(mid, 0)
+    )(got, decay_bias, head_gain, recurrent_state)
+    first = got
+    full0 = shared(exchange(mixed, "dp"), 0)
     pay = call(
         second_partial_body,
-        shape((DP, LS, 768)),
+        shape((DP, LS, 896)),
         [out_spec, whole((256, 256)), pair, pair, *weight_specs(1)],
-        whole((DP, LS, 768)),
+        whole((DP, LS, 896)),
     )(full0, tokens, pre_gain, post_gain, *weights)
     got = exchange(pay, "dp")
     state, mixed = call(
         second_state_body,
         [shape((2, LS, 8192), f32), shape((DP, LS, 128))],
-        [whole((DP, LS, 768)), whole((DP, LS, 128), (0, 0, 3)), whole((DP, LS, 128), (0, 0, 1))]
+        [whole((DP, LS, 896)), whole((DP, LS, 128), (0, 0, 3))]
         + [whole((2, 64)), whole((2, 128))]
         + [whole((1, LS, 8192), (1, 0, 0)), pl.BlockSpec(memory_space=pl.ANY)],
         [whole((1, LS, 8192), (1, 0, 0)), whole((DP, LS, 128))],
         scratch,
-        {6: 0},
-    )(got, first, mid, decay_bias, head_gain, recurrent_state, state)
+        {5: 0},
+    )(got, first, decay_bias, head_gain, recurrent_state, state)
     full1 = shared(exchange(mixed, "dp"), 1)
     pay = call(
         squares_body,
-        shape((DP, LS, 128)),
+        shape((DP, 8, 128)),
         [out_spec, out_spec],
-        whole((DP, LS, 128)),
+        whole((DP, 8, 128)),
     )(full1, full0)
     got = exchange(pay, "dp")
     hidden = call(
         final_body,
         shape((256, 256)),
-        [whole((DP, LS, 128)), out_spec, out_spec, whole((256, 256)), pair],
+        [whole((DP, 8, 128)), out_spec, out_spec, whole((256, 256)), pair],
         whole((256, 256)),
     )(got, full1, full0, tokens, post_gain)
     return (hidden, state)

time: 144 us -> 144 us (level)
  no operation moved by 1% of the time
where the time goes in v5:
time: 144 us; the launch traced here: 143 us
  blocking collectives  136 us (94%)
  Pallas kernels  6.52 us (5%)
    all_to_all x9, blocking collectives, exchange(): return lax.all_to_all(array, axis, 0, 0, tiled=True)  136 us

profile of v5, /device:TPU:1, one launch (start us, length us, event | category | flops | bytes accessed | tf_op | source)
XLA Modules:
  0.0 143.2 jit_solution(18238385720604799797)
XLA Ops:
  0.6 0.0 copy-start
  0.6 1.5 %shard_map.131 = bf16[16,16,512]{2,1,0:T(8,128)(2,1)S(1)} custom-call(bf16[256,256]{1,0:T(8,128)(2,1)} %tokens.5, f32[2,256]{1,0:T(2,128)} %pre.3, bf16[2,64,256]{2,1,0:T(8,128)(2,1)} %bitcast.6, bf16[2,64,256]{2,1,0:T(8,128)(2,1)} %bitcast.8, bf16[2,256,128]{2,1,0:T(8,128)(2,1)} %wv.3, bf16[2,256,128]{2,1,0:T(8,128)(2,1)} %wg.3, ...), custom_call_target="tpu_custom_call" | custom-call | tf_op jit(solution)/shard_map/pallas_call | solution.py:239
  2.1 0.0 copy-start.10
  2.2 0.0 copy-start.11
  2.2 21.0 %all_to_all.45.got.first = bf16[16,16,512]{2,1,0:T(8,128)(2,1)S(1)} all-to-all(bf16[16,16,512]{2,1,0:T(8,128)(2,1)S(1)} %shard_map.131), channel_id=1, replica_groups=mesh['tp'=32,'dp'=16] {'dp'}, dimensions={0} | all-to-all | bytes 524288 | tf_op jit(solution)/shard_map/all_to_all | solution.py:221
  23.2 0.0 copy-done
  23.2 0.0 copy-done.10
  23.2 0.0 copy-done.11
  23.2 1.4 shard_map.132
  24.6 0.0 copy-start.5
  24.6 10.5 %all_to_all.46.mixed = bf16[16,16,128]{2,1,0:T(8,128)(2,1)S(1)} all-to-all(bf16[16,16,128]{2,1,0:T(8,128)(2,1)S(1)} %get-tuple-element.6), channel_id=1, replica_groups=mesh['tp'=32,'dp'=16] {'dp'}, dimensions={0} | all-to-all | bytes 131072 | tf_op jit(solution)/shard_map/all_to_all | solution.py:221
  35.1 0.0 copy-done.5
  35.1 0.2 shard_map.133
  35.3 0.0 copy-start.7
  35.3 0.0 copy-start.8
  35.3 0.0 copy-start.9
  35.3 21.8 %all_to_all.47.arrived = bf16[32,8,256]{2,1,0:T(8,128)(2,1)S(1)} all-to-all(bf16[32,8,256]{2,1,0:T(8,128)(2,1)S(1)} %shard_map.133), channel_id=1, replica_groups=mesh['tp'=32,'dp'=16] {'tp'}, dimensions={0} | all-to-all | bytes 262144 | tf_op jit(solution)/shard_map/all_to_all | solution.py:221
  57.1 0.0 copy-start.3
  57.1 0.0 copy-start.4
  57.1 0.0 copy-start.1
  57.2 0.0 copy-start.2
  57.2 0.0 copy-start.6
  57.2 12.8 %all_to_all.48.full.full0 = bf16[32,8,256]{2,1,0:T(8,128)(2,1)S(1)} all-to-all(bf16[32,8,256]{2,1,0:T(8,128)(2,1)S(1)} %shard_map.134), channel_id=1, replica_groups=mesh['tp'=32,'dp'=16] {'tp'}, dimensions={0} | all-to-all | bytes 262144 | tf_op jit(solution)/shard_map/all_to_all | solution.py:221
  70.0 0.0 copy-done.7
  70.0 0.0 copy-done.8
  70.0 0.0 copy-done.9
  70.0 0.0 copy-done.3
  70.0 0.0 copy-done.4
  70.0 0.0 copy-done.1
  70.0 0.0 copy-done.2
  70.0 0.0 copy-done.6
  70.1 0.5 shard_map.135
  70.6 21.1 %all_to_all.49.got = bf16[16,16,896]{2,1,0:T(8,128)(2,1)S(1)} all-to-all(bf16[16,16,896]{2,1,0:T(8,128)(2,1)S(1)} %shard_map.135), channel_id=1, replica_groups=mesh['tp'=32,'dp'=16] {'dp'}, dimensions={0} | all-to-all | bytes 917504 | tf_op jit(solution)/shard_map/all_to_all | solution.py:221
  91.7 1.5 %shard_map.136 = (f32[2,16,8192]{2,1,0:T(8,128)}, bf16[16,16,128]{2,1,0:T(8,128)(2,1)S(1)}) custom-call(bf16[16,16,896]{2,1,0:T(8,128)(2,1)S(1)} %all_to_all.49.got, bf16[16,16,512]{2,1,0:T(8,128)(2,1)S(1)} %all_to_all.45.got.first, f32[2,64]{1,0:T(2,128)S(1)} %copy-done.10, f32[2,128]{1,0:T(2,128)S(1)} %copy-done.11, ...), custom_call_target="tpu_custom_call", output_to_operand_aliasing={{0}: (5, {})} | custom-call | tf_op jit(solution)/shard_map/pallas_call | solution.py:262
  93.3 10.4 %all_to_all.50.mixed = bf16[16,16,128]{2,1,0:T(8,128)(2,1)S(1)} all-to-all(bf16[16,16,128]{2,1,0:T(8,128)(2,1)S(1)} %get-tuple-element.8), channel_id=1, replica_groups=mesh['tp'=32,'dp'=16] {'dp'}, dimensions={0} | all-to-all | bytes 131072 | tf_op jit(solution)/shard_map/all_to_all | solution.py:221
  103.7 0.2 shard_map.137
  103.9 12.8 %all_to_all.51.arrived = bf16[32,8,256]{2,1,0:T(8,128)(2,1)S(1)} all-to-all(bf16[32,8,256]{2,1,0:T(8,128)(2,1)S(1)} %shard_map.137), channel_id=1, replica_groups=mesh['tp'=32,'dp'=16] {'tp'}, dimensions={0} | all-to-all | bytes 262144 | tf_op jit(solution)/shard_map/all_to_all | solution.py:221
  116.7 12.7 %all_to_all.52.full1 = bf16[32,8,256]{2,1,0:T(8,128)(2,1)S(1)} all-to-all(bf16[32,8,256]{2,1,0:T(8,128)(2,1)S(1)} %shard_map.138), channel_id=1, replica_groups=mesh['tp'=32,'dp'=16] {'tp'}, dimensions={0} | all-to-all | bytes 262144 | tf_op jit(solution)/shard_map/all_to_all | solution.py:221
  129.4 0.2 shard_map.139
  129.6 12.6 %all_to_all.53.got = bf16[16,8,128]{2,1,0:T(8,128)(2,1)S(1)} all-to-all(bf16[16,8,128]{2,1,0:T(8,128)(2,1)S(1)} %shard_map.139), channel_id=1, replica_groups=mesh['tp'=32,'dp'=16] {'dp'}, dimensions={0} | all-to-all | bytes 65536 | tf_op jit(solution)/shard_map/all_to_all | solution.py:221
  142.2 1.0 shard_map.140
  (2 shorter events, 0.1 us)
Async XLA Ops:
  0.6 22.5 %copy-start = (f32[2,16,8192]{2,1,0:T(8,128)S(1)}, f32[2,16,8192]{2,1,0:T(8,128)}, u32[]{:S(2)}) copy-start(f32[2,16,8192]{2,1,0:T(8,128)} %old.3) | copy-start | bytes 3145732
  2.1 21.0 %copy-start.10 = (f32[2,64]{1,0:T(2,128)S(1)}, f32[2,64]{1,0:T(2,128)}, u32[]{:S(2)}) copy-start(f32[2,64]{1,0:T(2,128)} %bias.3) | copy-start | bytes 1540
  2.2 21.0 %copy-start.11 = (f32[2,128]{1,0:T(2,128)S(1)}, f32[2,128]{1,0:T(2,128)}, u32[]{:S(2)}) copy-start(f32[2,128]{1,0:T(2,128)} %gain.3) | copy-start | bytes 3076
  24.6 10.5 %copy-start.5 = (bf16[2,128,256]{2,1,0:T(8,128)(2,1)S(1)}, bf16[2,128,256]{2,1,0:T(8,128)(2,1)}, u32[]{:S(2)}) copy-start(bf16[2,128,256]{2,1,0:T(8,128)(2,1)} %wo.3) | copy-start | bytes 393220
  35.3 34.7 %copy-start.7 = (bf16[2,256,64]{1,2,0:T(8,128)(2,1)S(1)}, bf16[2,256,64]{1,2,0:T(8,128)(2,1)}, u32[]{:S(2)}) copy-start(bf16[2,256,64]{1,2,0:T(8,128)(2,1)} %param.16) | copy-start | bytes 196612
  35.3 34.7 %copy-start.8 = (f32[2,256]{1,0:T(2,128)S(1)}, f32[2,256]{1,0:T(2,128)}, u32[]{:S(2)}) copy-start(f32[2,256]{1,0:T(2,128)} %pre.3) | copy-start | bytes 6148
  35.3 34.7 %copy-start.9 = (f32[2,256]{1,0:T(2,128)S(1)}, f32[2,256]{1,0:T(2,128)}, u32[]{:S(2)}) copy-start(f32[2,256]{1,0:T(2,128)} %post.3) | copy-start | bytes 6148
  57.1 12.9 %copy-start.3 = (bf16[2,256,128]{2,1,0:T(8,128)(2,1)S(1)}, bf16[2,256,128]{2,1,0:T(8,128)(2,1)}, u32[]{:S(2)}) copy-start(bf16[2,256,128]{2,1,0:T(8,128)(2,1)} %wv.3) | copy-start | bytes 393220
  57.1 12.9 %copy-start.4 = (bf16[2,256,128]{2,1,0:T(8,128)(2,1)S(1)}, bf16[2,256,128]{2,1,0:T(8,128)(2,1)}, u32[]{:S(2)}) copy-start(bf16[2,256,128]{2,1,0:T(8,128)(2,1)} %wg.3) | copy-start | bytes 393220
  57.1 12.9 %copy-start.1 = (bf16[256,256]{1,0:T(8,128)(2,1)S(1)}, bf16[256,256]{1,0:T(8,128)(2,1)}, u32[]{:S(2)}) copy-start(bf16[256,256]{1,0:T(8,128)(2,1)} %tokens.5) | copy-start | bytes 393220
  57.2 12.9 %copy-start.2 = (bf16[2,256,64]{1,2,0:T(8,128)(2,1)S(1)}, bf16[2,256,64]{1,2,0:T(8,128)(2,1)}, u32[]{:S(2)}) copy-start(bf16[2,256,64]{1,2,0:T(8,128)(2,1)} %param.19) | copy-start | bytes 196612
  57.2 12.9 %copy-start.6 = (bf16[2,256,64]{1,2,0:T(8,128)(2,1)S(1)}, bf16[2,256,64]{1,2,0:T(8,128)(2,1)}, u32[]{:S(2)}) copy-start(bf16[2,256,64]{1,2,0:T(8,128)(2,1)} %param.15) | copy-start | bytes 196612

commit v6 on v4

--- a/solution.py
+++ b/solution.py
@@ -146,32 +146,34 @@
         mixed[d] = m
 
 
-def squares_body(full1, full0, pay):
-    lane = lax.broadcasted_iota(jnp.int32, (LS, 128), 1)
-    acc = jnp.zeros((LS, 128), f32)
-    for i, full in enumerate((full1, full0)):
-        out = full[...].astype(f32).reshape(256, 256)
-        parts = split3(jnp.sum(out * out, axis=1, keepdims=True))
-        for d in range(DP):
-            for j in range(3):
-                acc = jnp.where(lane == 48 * i + 16 * j + d, parts[j][LS * d : LS * d + LS], acc)
-    acc = acc.astype(bf16)
+def squares_body(arrived, own0, total, pay):
+    out = arrived[0].astype(f32)
+    for t in range(1, TP):
+        out = out + arrived[t].astype(f32)
+    total[...] = out
+    before = own0[0].astype(f32)
+    lane = lax.broadcasted_iota(jnp.int32, (8, 128), 1)
+    parts = []
+    for value in (out, before):
+        parts += split3(jnp.sum(value * value, axis=1, keepdims=True))
+    acc = place(jnp.zeros((8, 128), f32), lane, 0, parts).astype(bf16)
     for d in range(DP):
         pay[d] = acc
 
 
-def final_body(got, full1, full0, tokens, post, hidden):
-    total = got[0].astype(f32)
+def final_body(got, total, own0, tokens, post, out):
+    came = got[0].astype(f32)
     for d in range(1, DP):
-        total = total + got[d].astype(f32)
-    total = total + pltpu.roll(total, 112, 1) + pltpu.roll(total, 96, 1)
-    scale = lax.rsqrt(total / D + epsilon)
-    for d in range(DP):
-        at = slice(LS * d, LS * d + LS)
-        outs = [full[2 * d : 2 * d + 2].astype(f32).reshape(LS, 256) for full in (full1, full0)]
-        x = tokens[at, :].astype(f32) + outs[1] * scale[:, 48 + d : 49 + d] * post[0:1, :]
-        x = x.astype(bf16).astype(f32)
-        hidden[at, :] = (x + outs[0] * scale[:, d : d + 1] * post[1:2, :]).astype(bf16)
+        came = came + got[d].astype(f32)
+    rates = []
+    for i in range(2):
+        squares = came[:, 3 * i : 3 * i + 1] + came[:, 3 * i + 1 : 3 * i + 2] + came[:, 3 * i + 2 : 3 * i + 3]
+        rates.append(lax.rsqrt(squares / D + epsilon))
+    x = tokens[lax.axis_index("tp")].astype(f32)
+    x = (x + own0[0].astype(f32) * rates[1] * post[0:1, :]).astype(bf16).astype(f32)
+    x = (x + total[...] * rates[0] * post[1:2, :]).astype(bf16)
+    for t in range(TP):
+        out[t] = x
 
 
 def attend(tiles, squares, bias, gain, old, new_ref, wide, reads):
@@ -231,16 +233,14 @@
     scratch = [pltpu.VMEM((8, 128), f32), pltpu.VMEM((64 * LS, 128), f32)]
     out_spec = whole((TP, 8, 256))
 
-    def shared(mixed, b):
+    def reduced(mixed, b):
         spread = call(
             first_out_body,
             shape((TP, 8, 256)),
             [whole((DP, LS, 128)), whole((1, 128, 256), (b, 0, 0))],
             out_spec,
         )(mixed, w_out)
-        arrived = exchange(spread, "tp")
-        own = call(total_body, shape((TP, 8, 256)), [out_spec], out_spec)(arrived)
-        return exchange(own, "tp")
+        return exchange(spread, "tp")
 
     pay = call(
         partial_body,
@@ -258,7 +258,9 @@
         scratch,
     )(got, decay_bias, head_gain, recurrent_state, tokens, pre_gain, weights[0], weights[1])
     first, mid = got, exchange(mixed, "dp")
-    full0 = shared(mid, 0)
+    arrived = reduced(mid, 0)
+    own0 = call(total_body, shape((TP, 8, 256)), [out_spec], out_spec)(arrived)
+    full0 = exchange(own0, "tp")
     pay = call(
         second_partial_body,
         shape((DP, LS, 768)),
@@ -276,20 +278,23 @@
         scratch,
         {6: 0},
     )(got, first, mid, decay_bias, head_gain, recurrent_state, state)
-    full1 = shared(exchange(mixed, "dp"), 1)
-    pay = call(
+    arrived = reduced(exchange(mixed, "dp"), 1)
+    rows = whole((8, 256))
+    one = whole((1, 8, 256))
+    total, pay = call(
         squares_body,
-        shape((DP, LS, 128)),
-        [out_spec, out_spec],
-        whole((DP, LS, 128)),
-    )(full1, full0)
+        [shape((8, 256), f32), shape((DP, 8, 128))],
+        [out_spec, one],
+        [rows, whole((DP, 8, 128))],
+    )(arrived, own0)
     got = exchange(pay, "dp")
-    hidden = call(
+    own = call(
         final_body,
-        shape((256, 256)),
-        [whole((DP, LS, 128)), out_spec, out_spec, whole((256, 256)), pair],
-        whole((256, 256)),
-    )(got, full1, full0, tokens, post_gain)
+        shape((TP, 8, 256)),
+        [whole((DP, 8, 128)), rows, one, out_spec, pair],
+        out_spec,
+    )(got, total, own0, tokens.reshape(TP, 8, 256), post_gain)
+    hidden = exchange(own, "tp").reshape(256, 256)
     return (hidden, state)
 
 

time: 144 us -> 142 us (0.986)
  blocking collectives: 136 us -> 134 us
    all_to_all x9, blocking collectives: 136 us -> 134 us  [exchange(): return lax.all_to_all(array, axis, 0, 0, tiled=True)]
where the time goes in v6:
time: 142 us; the launch traced here: 141 us
  blocking collectives  134 us (94%)
  Pallas kernels  5.68 us (4%)
    all_to_all x9, blocking collectives, exchange(): return lax.all_to_all(array, axis, 0, 0, tiled=True)  134 us

profile of v6, /device:TPU:1, one launch (start us, length us, event | category | flops | bytes accessed | tf_op | source)
XLA Modules:
  0.0 141.2 jit_solution(10205850827829054895)
XLA Ops:
  0.6 0.0 copy-start
  0.6 1.5 %shard_map.131 = bf16[16,16,512]{2,1,0:T(8,128)(2,1)S(1)} custom-call(bf16[256,256]{1,0:T(8,128)(2,1)} %tokens.5, f32[2,256]{1,0:T(2,128)} %pre.5, bf16[2,64,256]{2,1,0:T(8,128)(2,1)} %bitcast.9, bf16[2,64,256]{2,1,0:T(8,128)(2,1)} %bitcast.12, bf16[2,256,128]{2,1,0:T(8,128)(2,1)} %wv.3, bf16[2,256,128]{2,1,0:T(8,128)(2,1)} %wg.3, ...), custom_call_target="tpu_custom_call" | custom-call | tf_op jit(solution)/shard_map/pallas_call | solution.py:245
  2.1 0.0 copy-start.1
  2.2 0.0 copy-start.3
  2.2 0.0 copy-start.4
  2.2 0.0 copy-start.8
  2.2 0.0 copy-start.10
  2.2 0.0 copy-start.11
  2.2 21.1 %all_to_all.45.got.first = bf16[16,16,512]{2,1,0:T(8,128)(2,1)S(1)} all-to-all(bf16[16,16,512]{2,1,0:T(8,128)(2,1)S(1)} %shard_map.131), channel_id=1, replica_groups=mesh['tp'=32,'dp'=16] {'dp'}, dimensions={0} | all-to-all | bytes 524288 | tf_op jit(solution)/shard_map/all_to_all | solution.py:229
  23.3 0.0 copy-done
  23.3 0.0 copy-done.1
  23.3 0.0 copy-done.3
  23.4 0.0 copy-done.4
  23.4 0.0 copy-done.8
  23.4 0.0 copy-done.10
  23.4 0.0 copy-done.11
  23.4 1.5 %shard_map.132 = (f32[2,16,8192]{2,1,0:T(8,128)}, bf16[16,16,256]{2,1,0:T(8,128)(2,1)S(1)}) custom-call(bf16[16,16,512]{2,1,0:T(8,128)(2,1)S(1)} %all_to_all.45.got.first, f32[2,64]{1,0:T(2,128)S(1)} %copy-done.10, f32[2,128]{1,0:T(2,128)S(1)} %copy-done.11, f32[2,16,8192]{2,1,0:T(8,128)S(1)} %copy-done, bf16[256,256]{1,0:T(8,128)(2,1)S(1)} %copy-done.1, ...), custom_call_target="tpu_custom_call" | custom-call | tf_op jit(solution)/shard_map/pallas_call | solution.py:252
  24.9 0.0 copy-start.7
  24.9 11.7 %all_to_all.46.mixed.mid = bf16[16,16,256]{2,1,0:T(8,128)(2,1)S(1)} all-to-all(bf16[16,16,256]{2,1,0:T(8,128)(2,1)S(1)} %get-tuple-element.8), channel_id=1, replica_groups=mesh['tp'=32,'dp'=16] {'dp'}, dimensions={0} | all-to-all | bytes 262144 | tf_op jit(solution)/shard_map/all_to_all | solution.py:229
  36.5 0.0 copy-done.7
  36.5 0.2 shard_map.133
  36.7 21.7 %all_to_all.47.arrived = bf16[32,8,256]{2,1,0:T(8,128)(2,1)S(1)} all-to-all(bf16[32,8,256]{2,1,0:T(8,128)(2,1)S(1)} %shard_map.133), channel_id=1, replica_groups=mesh['tp'=32,'dp'=16] {'tp'}, dimensions={0} | all-to-all | bytes 262144 | tf_op jit(solution)/shard_map/all_to_all | solution.py:229
  58.4 0.0 copy-start.6
  58.5 0.0 copy-start.2
  58.5 0.0 copy-start.5
  58.5 0.0 copy-start.9
  58.5 12.8 %all_to_all.48.full = bf16[32,8,256]{2,1,0:T(8,128)(2,1)S(1)} all-to-all(bf16[32,8,256]{2,1,0:T(8,128)(2,1)S(1)} %shard_map.134.own0), channel_id=1, replica_groups=mesh['tp'=32,'dp'=16] {'tp'}, dimensions={0} | all-to-all | bytes 262144 | tf_op jit(solution)/shard_map/all_to_all | solution.py:229
  71.3 0.0 copy-done.6
  71.3 0.0 copy-done.2
  71.3 0.0 copy-done.5
  71.3 0.0 copy-done.9
  71.3 0.5 shard_map.135
  71.8 19.6 %all_to_all.49.got = bf16[16,16,768]{2,1,0:T(8,128)(2,1)S(1)} all-to-all(bf16[16,16,768]{2,1,0:T(8,128)(2,1)S(1)} %shard_map.135), channel_id=1, replica_groups=mesh['tp'=32,'dp'=16] {'dp'}, dimensions={0} | all-to-all | bytes 786432 | tf_op jit(solution)/shard_map/all_to_all | solution.py:229
  91.5 1.5 %shard_map.136 = (f32[2,16,8192]{2,1,0:T(8,128)}, bf16[16,16,128]{2,1,0:T(8,128)(2,1)S(1)}) custom-call(bf16[16,16,768]{2,1,0:T(8,128)(2,1)S(1)} %all_to_all.49.got, bf16[16,16,512]{2,1,0:T(8,128)(2,1)S(1)} %all_to_all.45.got.first, bf16[16,16,256]{2,1,0:T(8,128)(2,1)S(1)} %all_to_all.46.mixed.mid, ...), custom_call_target="tpu_custom_call", output_to_operand_aliasing={{0}: (6, {})} | custom-call | tf_op jit(solution)/shard_map/pallas_call | solution.py:271
  93.0 10.5 %all_to_all.50.mixed = bf16[16,16,128]{2,1,0:T(8,128)(2,1)S(1)} all-to-all(bf16[16,16,128]{2,1,0:T(8,128)(2,1)S(1)} %get-tuple-element.10), channel_id=1, replica_groups=mesh['tp'=32,'dp'=16] {'dp'}, dimensions={0} | all-to-all | bytes 131072 | tf_op jit(solution)/shard_map/all_to_all | solution.py:229
  103.5 0.2 shard_map.137
  103.6 12.8 %all_to_all.51.arrived = bf16[32,8,256]{2,1,0:T(8,128)(2,1)S(1)} all-to-all(bf16[32,8,256]{2,1,0:T(8,128)(2,1)S(1)} %shard_map.137), channel_id=1, replica_groups=mesh['tp'=32,'dp'=16] {'tp'}, dimensions={0} | all-to-all | bytes 262144 | tf_op jit(solution)/shard_map/all_to_all | solution.py:229
  116.4 0.1 shard_map.138
  116.5 11.4 %all_to_all.52.got = bf16[16,8,128]{2,1,0:T(8,128)(2,1)S(1)} all-to-all(bf16[16,8,128]{2,1,0:T(8,128)(2,1)S(1)} %get-tuple-element.11), channel_id=1, replica_groups=mesh['tp'=32,'dp'=16] {'dp'}, dimensions={0} | all-to-all | bytes 65536 | tf_op jit(solution)/shard_map/all_to_all | solution.py:229
  127.9 0.2 shard_map.139
  128.1 12.4 %all_to_all.53 = bf16[32,8,256]{2,1,0:T(8,128)(2,1)S(1)} all-to-all(bf16[32,8,256]{2,1,0:T(8,128)(2,1)S(1)} %shard_map.139), channel_id=1, replica_groups=mesh['tp'=32,'dp'=16] {'tp'}, dimensions={0} | all-to-all | bytes 262144 | tf_op jit(solution)/shard_map/all_to_all | solution.py:229
  140.5 0.7 copy.17
  (1 shorter events, 0.0 us)
Async XLA Ops:
  0.6 22.7 %copy-start = (f32[2,16,8192]{2,1,0:T(8,128)S(1)}, f32[2,16,8192]{2,1,0:T(8,128)}, u32[]{:S(2)}) copy-start(f32[2,16,8192]{2,1,0:T(8,128)} %old.3) | copy-start | bytes 3145732
  2.1 21.2 %copy-start.1 = (bf16[256,256]{1,0:T(8,128)(2,1)S(1)}, bf16[256,256]{1,0:T(8,128)(2,1)}, u32[]{:S(2)}) copy-start(bf16[256,256]{1,0:T(8,128)(2,1)} %tokens.5) | copy-start | bytes 393220
  2.2 21.2 %copy-start.3 = (bf16[2,256,64]{1,2,0:T(8,128)(2,1)S(1)}, bf16[2,256,64]{1,2,0:T(8,128)(2,1)}, u32[]{:S(2)}) copy-start(bf16[2,256,64]{1,2,0:T(8,128)(2,1)} %param.15) | copy-start | bytes 196612
  2.2 21.2 %copy-start.4 = (bf16[2,256,64]{1,2,0:T(8,128)(2,1)S(1)}, bf16[2,256,64]{1,2,0:T(8,128)(2,1)}, u32[]{:S(2)}) copy-start(bf16[2,256,64]{1,2,0:T(8,128)(2,1)} %param.16) | copy-start | bytes 196612
  2.2 21.2 %copy-start.8 = (f32[2,256]{1,0:T(2,128)S(1)}, f32[2,256]{1,0:T(2,128)}, u32[]{:S(2)}) copy-start(f32[2,256]{1,0:T(2,128)} %pre.5) | copy-start | bytes 6148
  2.2 21.2 %copy-start.10 = (f32[2,64]{1,0:T(2,128)S(1)}, f32[2,64]{1,0:T(2,128)}, u32[]{:S(2)}) copy-start(f32[2,64]{1,0:T(2,128)} %bias.3) | copy-start | bytes 1540
  2.2 21.2 %copy-start.11 = (f32[2,128]{1,0:T(2,128)S(1)}, f32[2,128]{1,0:T(2,128)}, u32[]{:S(2)}) copy-start(f32[2,128]{1,0:T(2,128)} %gain.3) | copy-start | bytes 3076
  24.9 11.7 %copy-start.7 = (bf16[2,128,256]{2,1,0:T(8,128)(2,1)S(1)}, bf16[2,128,256]{2,1,0:T(8,128)(2,1)}, u32[]{:S(2)}) copy-start(bf16[2,128,256]{2,1,0:T(8,128)(2,1)} %wo.3) | copy-start | bytes 393220
  58.4 12.9 %copy-start.6 = (bf16[2,256,128]{2,1,0:T(8,128)(2,1)S(1)}, bf16[2,256,128]{2,1,0:T(8,128)(2,1)}, u32[]{:S(2)}) copy-start(bf16[2,256,128]{2,1,0:T(8,128)(2,1)} %wg.3) | copy-start | bytes 393220
  58.5 12.8 %copy-start.2 = (bf16[2,256,64]{1,2,0:T(8,128)(2,1)S(1)}, bf16[2,256,64]{1,2,0:T(8,128)(2,1)}, u32[]{:S(2)}) copy-start(bf16[2,256,64]{1,2,0:T(8,128)(2,1)} %param.19) | copy-start | bytes 196612
  58.5 12.8 %copy-start.5 = (bf16[2,256,128]{2,1,0:T(8,128)(2,1)S(1)}, bf16[2,256,128]{2,1,0:T(8,128)(2,1)}, u32[]{:S(2)}) copy-start(bf16[2,256,128]{2,1,0:T(8,128)(2,1)} %wv.3) | copy-start | bytes 393220
  58.5 12.8 %copy-start.9 = (f32[2,256]{1,0:T(2,128)S(1)}, f32[2,256]{1,0:T(2,128)}, u32[]{:S(2)}) copy-start(f32[2,256]{1,0:T(2,128)} %post.3) | copy-start | bytes 6148

commit v7 on v6

--- a/solution.py
+++ b/solution.py
@@ -84,14 +84,16 @@
     return tile[:, 125:126] + tile[:, 126:127] + tile[:, 127:128]
 
 
-def first_state_body(got, bias, gain, old, tokens, pre, wq1, wk1, new_ref, pay, wide, reads):
+def first_state_body(got, bias, gain, old, tokens, pre, wq1, wk1, new_ref, pay, *scratch):
     tiles = [summed(got, 128 * i) for i in range(4)]
-    m = attend(tiles, last_three(tiles[3]), bias[0:1, :], gain[0:1, :], old, new_ref, wide, reads)
+    m, copies = attend(0, tiles, last_three(tiles[3]), bias[0:1, :], gain[0:1, :], old, new_ref, *scratch)
     late = (tokens[...].astype(f32) * pre[1:2, :]).astype(bf16)
     part = jnp.dot(late, turned_columns(wq1, wk1), preferred_element_type=f32)
     pay[:, :, 128:256] = part.astype(bf16).reshape(DP, LS, 128)
     for d in range(DP):
         pay[d, :, 0:128] = m
+    for copy in copies:
+        copy.wait()
 
 
 def first_out_body(mixed, wo, out):
@@ -128,7 +130,7 @@
         pay[:, :, 128 * i : 128 * i + 128] = acc.astype(bf16).reshape(DP, LS, 128)
 
 
-def second_state_body(got, first, mid, bias, gain, old, kept, new_ref, mixed, wide, reads):
+def second_state_body(got, first, mid, bias, gain, old, kept, new_ref, mixed, *scratch):
     step = [summed(got, 128 * i) for i in range(4)]
     early = summed(first, 0)
     stats = []
@@ -141,9 +143,11 @@
     decay = pltpu.roll(jnp.where(lane >= 125, step[3], early), 64, 1)
     base = [summed(mid, 0), summed(got, 512), summed(got, 640), decay]
     tiles = [x + scale * b for x, b in zip(base, step)]
-    m = attend(tiles, jnp.maximum(squares, 0.0), bias[1:2, :], gain[1:2, :], old, new_ref, wide, reads)
+    m, copies = attend(1, tiles, jnp.maximum(squares, 0.0), bias[1:2, :], gain[1:2, :], old, new_ref, *scratch)
     for d in range(DP):
         mixed[d] = m
+    for copy in copies:
+        copy.wait()
 
 
 def squares_body(arrived, own0, total, pay):
@@ -176,7 +180,7 @@
         out[t] = x
 
 
-def attend(tiles, squares, bias, gain, old, new_ref, wide, reads):
+def attend(block, tiles, squares, bias, gain, old, out, wide, reads, fresh, sems):
     scale = lax.rsqrt(squares / D + epsilon)
     lane = lax.broadcasted_iota(jnp.int32, (LS, 128), 1)
     low = lane < 64
@@ -193,11 +197,17 @@
     decay = jnp.exp(log_decay)
     decay = jnp.where(low, decay, pltpu.roll(decay, 64, 1))
     right = (lane >= 64).astype(jnp.int32)
+    copies = []
     for b in range(64):
         v = jnp.take_along_axis(value, right + 2 * b, axis=1)
         new = decay * old[0, :, b * 128 : b * 128 + 128] + key * v
-        new_ref[0, :, b * 128 : b * 128 + 128] = new
+        fresh[:, b * 128 : b * 128 + 128] = new
         reads[b * LS : b * LS + LS, :] = query * new
+        if b % 16 == 15:
+            at = pl.ds((b // 16) * 2048, 2048)
+            copy = pltpu.make_async_copy(fresh.at[:, at], out.at[block, :, at], sems.at[b // 16])
+            copy.start()
+            copies.append(copy)
     row = lax.broadcasted_iota(jnp.int32, (128, 128), 0)
     col = lax.broadcasted_iota(jnp.int32, (128, 128), 1)
     fold = ((row >= 64) == (col % 2 == 1)).astype(f32).astype(bf16)
@@ -211,7 +221,7 @@
     readout = readout * KEY ** (-0.5)
     mean = jnp.sum(readout * readout, axis=1, keepdims=True) / VAL
     silu = gate / (1.0 + jnp.exp(-gate))
-    return (readout * lax.rsqrt(mean + epsilon) * gain * silu).astype(bf16)
+    return (readout * lax.rsqrt(mean + epsilon) * gain * silu).astype(bf16), copies
 
 
 def shape(s, t=bf16):
@@ -230,7 +240,13 @@
 
     pair = whole((2, 256))
     second_narrow = whole((1, 64, 256), (1, 0, 0))
-    scratch = [pltpu.VMEM((8, 128), f32), pltpu.VMEM((64 * LS, 128), f32)]
+    scratch = [
+        pltpu.VMEM((8, 128), f32),
+        pltpu.VMEM((64 * LS, 128), f32),
+        pltpu.VMEM((LS, 8192), f32),
+        pltpu.SemaphoreType.DMA((4,)),
+    ]
+    anywhere = pl.BlockSpec(memory_space=pl.ANY)
     out_spec = whole((TP, 8, 256))
 
     def reduced(mixed, b):
@@ -254,7 +270,7 @@
         [shape((2, LS, 8192), f32), shape((DP, LS, 256))],
         [whole((DP, LS, 512)), whole((2, 64)), whole((2, 128)), whole((1, LS, 8192))]
         + [whole((256, 256)), pair, second_narrow, second_narrow],
-        [whole((1, LS, 8192)), whole((DP, LS, 256))],
+        [anywhere, whole((DP, LS, 256))],
         scratch,
     )(got, decay_bias, head_gain, recurrent_state, tokens, pre_gain, weights[0], weights[1])
     first, mid = got, exchange(mixed, "dp")
@@ -273,8 +289,8 @@
         [shape((2, LS, 8192), f32), shape((DP, LS, 128))],
         [whole((DP, LS, 768)), whole((DP, LS, 128), (0, 0, 3)), whole((DP, LS, 128), (0, 0, 1))]
         + [whole((2, 64)), whole((2, 128))]
-        + [whole((1, LS, 8192), (1, 0, 0)), pl.BlockSpec(memory_space=pl.ANY)],
-        [whole((1, LS, 8192), (1, 0, 0)), whole((DP, LS, 128))],
+        + [whole((1, LS, 8192), (1, 0, 0)), anywhere],
+        [anywhere, whole((DP, LS, 128))],
         scratch,
         {6: 0},
     )(got, first, mid, decay_bias, head_gain, recurrent_state, state)

time: 142 us -> 141 us (level)
  no operation moved by 1% of the time
where the time goes in v7:
time: 141 us
  blocking collectives  134 us (95%)
  Pallas kernels  5.37 us (4%)
    all_to_all x9, blocking collectives, exchange(): return lax.all_to_all(array, axis, 0, 0, tiled=True)  134 us

profile of v7, /device:TPU:1, one launch (start us, length us, event | category | flops | bytes accessed | tf_op | source)
XLA Modules:
  0.0 141.0 jit_solution(3068890444815118061)
XLA Ops:
  0.6 0.0 copy-start
  0.6 1.5 %shard_map.131 = bf16[16,16,512]{2,1,0:T(8,128)(2,1)S(1)} custom-call(bf16[256,256]{1,0:T(8,128)(2,1)} %tokens.5, f32[2,256]{1,0:T(2,128)} %pre.5, bf16[2,64,256]{2,1,0:T(8,128)(2,1)} %bitcast.9, bf16[2,64,256]{2,1,0:T(8,128)(2,1)} %bitcast.12, bf16[2,256,128]{2,1,0:T(8,128)(2,1)} %wv.3, bf16[2,256,128]{2,1,0:T(8,128)(2,1)} %wg.3, ...), custom_call_target="tpu_custom_call" | custom-call | tf_op jit(solution)/shard_map/pallas_call | solution.py:261
  2.1 0.0 copy-start.1
  2.2 0.0 copy-start.3
  2.2 0.0 copy-start.4
  2.2 0.0 copy-start.8
  2.2 0.0 copy-start.10
  2.2 0.0 copy-start.11
  2.2 21.1 %all_to_all.45.got.first = bf16[16,16,512]{2,1,0:T(8,128)(2,1)S(1)} all-to-all(bf16[16,16,512]{2,1,0:T(8,128)(2,1)S(1)} %shard_map.131), channel_id=1, replica_groups=mesh['tp'=32,'dp'=16] {'dp'}, dimensions={0} | all-to-all | bytes 524288 | tf_op jit(solution)/shard_map/all_to_all | solution.py:239
  23.3 0.0 copy-done
  23.3 0.0 copy-done.1
  23.3 0.0 copy-done.3
  23.4 0.0 copy-done.4
  23.4 0.0 copy-done.8
  23.4 0.0 copy-done.10
  23.4 0.0 copy-done.11
  23.4 1.3 shard_map.132
  24.7 0.0 copy-start.7
  24.7 11.7 %all_to_all.46.mixed.mid = bf16[16,16,256]{2,1,0:T(8,128)(2,1)S(1)} all-to-all(bf16[16,16,256]{2,1,0:T(8,128)(2,1)S(1)} %get-tuple-element.8), channel_id=1, replica_groups=mesh['tp'=32,'dp'=16] {'dp'}, dimensions={0} | all-to-all | bytes 262144 | tf_op jit(solution)/shard_map/all_to_all | solution.py:239
  36.4 0.0 copy-done.7
  36.4 0.2 shard_map.133
  36.5 21.7 %all_to_all.47.arrived = bf16[32,8,256]{2,1,0:T(8,128)(2,1)S(1)} all-to-all(bf16[32,8,256]{2,1,0:T(8,128)(2,1)S(1)} %shard_map.133), channel_id=1, replica_groups=mesh['tp'=32,'dp'=16] {'tp'}, dimensions={0} | all-to-all | bytes 262144 | tf_op jit(solution)/shard_map/all_to_all | solution.py:239
  58.2 0.0 copy-start.6
  58.2 0.0 copy-start.2
  58.3 0.0 copy-start.5
  58.3 0.0 copy-start.9
  58.3 12.9 %all_to_all.48.full = bf16[32,8,256]{2,1,0:T(8,128)(2,1)S(1)} all-to-all(bf16[32,8,256]{2,1,0:T(8,128)(2,1)S(1)} %shard_map.134.own0), channel_id=1, replica_groups=mesh['tp'=32,'dp'=16] {'tp'}, dimensions={0} | all-to-all | bytes 262144 | tf_op jit(solution)/shard_map/all_to_all | solution.py:239
  71.2 0.0 copy-done.6
  71.2 0.0 copy-done.2
  71.2 0.0 copy-done.5
  71.2 0.0 copy-done.9
  71.2 0.5 shard_map.135
  71.7 19.6 %all_to_all.49.got = bf16[16,16,768]{2,1,0:T(8,128)(2,1)S(1)} all-to-all(bf16[16,16,768]{2,1,0:T(8,128)(2,1)S(1)} %shard_map.135), channel_id=1, replica_groups=mesh['tp'=32,'dp'=16] {'dp'}, dimensions={0} | all-to-all | bytes 786432 | tf_op jit(solution)/shard_map/all_to_all | solution.py:239
  91.3 1.4 %shard_map.136 = (f32[2,16,8192]{2,1,0:T(8,128)}, bf16[16,16,128]{2,1,0:T(8,128)(2,1)S(1)}) custom-call(bf16[16,16,768]{2,1,0:T(8,128)(2,1)S(1)} %all_to_all.49.got, bf16[16,16,512]{2,1,0:T(8,128)(2,1)S(1)} %all_to_all.45.got.first, bf16[16,16,256]{2,1,0:T(8,128)(2,1)S(1)} %all_to_all.46.mixed.mid, ...), custom_call_target="tpu_custom_call", output_to_operand_aliasing={{0}: (6, {})} | custom-call | tf_op jit(solution)/shard_map/pallas_call | solution.py:287
  92.7 10.5 %all_to_all.50.mixed = bf16[16,16,128]{2,1,0:T(8,128)(2,1)S(1)} all-to-all(bf16[16,16,128]{2,1,0:T(8,128)(2,1)S(1)} %get-tuple-element.10), channel_id=1, replica_groups=mesh['tp'=32,'dp'=16] {'dp'}, dimensions={0} | all-to-all | bytes 131072 | tf_op jit(solution)/shard_map/all_to_all | solution.py:239
  103.2 0.2 shard_map.137
  103.4 12.8 %all_to_all.51.arrived = bf16[32,8,256]{2,1,0:T(8,128)(2,1)S(1)} all-to-all(bf16[32,8,256]{2,1,0:T(8,128)(2,1)S(1)} %shard_map.137), channel_id=1, replica_groups=mesh['tp'=32,'dp'=16] {'tp'}, dimensions={0} | all-to-all | bytes 262144 | tf_op jit(solution)/shard_map/all_to_all | solution.py:239
  116.2 0.1 shard_map.138
  116.3 11.4 %all_to_all.52.got = bf16[16,8,128]{2,1,0:T(8,128)(2,1)S(1)} all-to-all(bf16[16,8,128]{2,1,0:T(8,128)(2,1)S(1)} %get-tuple-element.11), channel_id=1, replica_groups=mesh['tp'=32,'dp'=16] {'dp'}, dimensions={0} | all-to-all | bytes 65536 | tf_op jit(solution)/shard_map/all_to_all | solution.py:239
  127.7 0.2 shard_map.139
  127.9 12.4 %all_to_all.53 = bf16[32,8,256]{2,1,0:T(8,128)(2,1)S(1)} all-to-all(bf16[32,8,256]{2,1,0:T(8,128)(2,1)S(1)} %shard_map.139), channel_id=1, replica_groups=mesh['tp'=32,'dp'=16] {'tp'}, dimensions={0} | all-to-all | bytes 262144 | tf_op jit(solution)/shard_map/all_to_all | solution.py:239
  140.3 0.7 copy.17
  (1 shorter events, 0.0 us)
Async XLA Ops:
  0.6 22.7 %copy-start = (f32[2,16,8192]{2,1,0:T(8,128)S(1)}, f32[2,16,8192]{2,1,0:T(8,128)}, u32[]{:S(2)}) copy-start(f32[2,16,8192]{2,1,0:T(8,128)} %old.3) | copy-start | bytes 3145732
  2.1 21.2 %copy-start.1 = (bf16[256,256]{1,0:T(8,128)(2,1)S(1)}, bf16[256,256]{1,0:T(8,128)(2,1)}, u32[]{:S(2)}) copy-start(bf16[256,256]{1,0:T(8,128)(2,1)} %tokens.5) | copy-start | bytes 393220
  2.2 21.2 %copy-start.3 = (bf16[2,256,64]{1,2,0:T(8,128)(2,1)S(1)}, bf16[2,256,64]{1,2,0:T(8,128)(2,1)}, u32[]{:S(2)}) copy-start(bf16[2,256,64]{1,2,0:T(8,128)(2,1)} %param.15) | copy-start | bytes 196612
  2.2 21.2 %copy-start.4 = (bf16[2,256,64]{1,2,0:T(8,128)(2,1)S(1)}, bf16[2,256,64]{1,2,0:T(8,128)(2,1)}, u32[]{:S(2)}) copy-start(bf16[2,256,64]{1,2,0:T(8,128)(2,1)} %param.16) | copy-start | bytes 196612
  2.2 21.2 %copy-start.8 = (f32[2,256]{1,0:T(2,128)S(1)}, f32[2,256]{1,0:T(2,128)}, u32[]{:S(2)}) copy-start(f32[2,256]{1,0:T(2,128)} %pre.5) | copy-start | bytes 6148
  2.2 21.2 %copy-start.10 = (f32[2,64]{1,0:T(2,128)S(1)}, f32[2,64]{1,0:T(2,128)}, u32[]{:S(2)}) copy-start(f32[2,64]{1,0:T(2,128)} %bias.3) | copy-start | bytes 1540
  2.2 21.2 %copy-start.11 = (f32[2,128]{1,0:T(2,128)S(1)}, f32[2,128]{1,0:T(2,128)}, u32[]{:S(2)}) copy-start(f32[2,128]{1,0:T(2,128)} %gain.3) | copy-start | bytes 3076
  24.7 11.7 %copy-start.7 = (bf16[2,128,256]{2,1,0:T(8,128)(2,1)S(1)}, bf16[2,128,256]{2,1,0:T(8,128)(2,1)}, u32[]{:S(2)}) copy-start(bf16[2,128,256]{2,1,0:T(8,128)(2,1)} %wo.3) | copy-start | bytes 393220
  58.2 13.0 %copy-start.6 = (bf16[2,256,128]{2,1,0:T(8,128)(2,1)S(1)}, bf16[2,256,128]{2,1,0:T(8,128)(2,1)}, u32[]{:S(2)}) copy-start(bf16[2,256,128]{2,1,0:T(8,128)(2,1)} %wg.3) | copy-start | bytes 393220
  58.2 12.9 %copy-start.2 = (bf16[2,256,64]{1,2,0:T(8,128)(2,1)S(1)}, bf16[2,256,64]{1,2,0:T(8,128)(2,1)}, u32[]{:S(2)}) copy-start(bf16[2,256,64]{1,2,0:T(8,128)(2,1)} %param.19) | copy-start | bytes 196612
  58.3 12.9 %copy-start.5 = (bf16[2,256,128]{2,1,0:T(8,128)(2,1)S(1)}, bf16[2,256,128]{2,1,0:T(8,128)(2,1)}, u32[]{:S(2)}) copy-start(bf16[2,256,128]{2,1,0:T(8,128)(2,1)} %wv.3) | copy-start | bytes 393220
  58.3 12.9 %copy-start.9 = (f32[2,256]{1,0:T(2,128)S(1)}, f32[2,256]{1,0:T(2,128)}, u32[]{:S(2)}) copy-start(f32[2,256]{1,0:T(2,128)} %post.3) | copy-start | bytes 6148

commit v8 on v7

--- a/solution.py
+++ b/solution.py
@@ -202,19 +202,16 @@
         v = jnp.take_along_axis(value, right + 2 * b, axis=1)
         new = decay * old[0, :, b * 128 : b * 128 + 128] + key * v
         fresh[:, b * 128 : b * 128 + 128] = new
-        reads[b * LS : b * LS + LS, :] = query * new
-        if b % 16 == 15:
-            at = pl.ds((b // 16) * 2048, 2048)
-            copy = pltpu.make_async_copy(fresh.at[:, at], out.at[block, :, at], sems.at[b // 16])
+        reads[b * LS : b * LS + LS, :] = (query * new).astype(bf16)
+        if b % 8 == 7:
+            at = pl.ds((b // 8) * 1024, 1024)
+            copy = pltpu.make_async_copy(fresh.at[:, at], out.at[block, :, at], sems.at[b // 8])
             copy.start()
             copies.append(copy)
     row = lax.broadcasted_iota(jnp.int32, (128, 128), 0)
     col = lax.broadcasted_iota(jnp.int32, (128, 128), 1)
     fold = ((row >= 64) == (col % 2 == 1)).astype(f32).astype(bf16)
-    product = reads[...]
-    high = product.astype(bf16)
-    rest = (product - high.astype(f32)).astype(bf16)
-    sums = jnp.dot(high, fold, preferred_element_type=f32) + jnp.dot(rest, fold, preferred_element_type=f32)
+    sums = jnp.dot(reads[...], fold, preferred_element_type=f32)
     readout = jnp.zeros((LS, 128), f32)
     for b in range(64):
         readout = jnp.where(lane // 2 == b, sums[b * LS : b * LS + LS, :], readout)
@@ -242,9 +239,9 @@
     second_narrow = whole((1, 64, 256), (1, 0, 0))
     scratch = [
         pltpu.VMEM((8, 128), f32),
-        pltpu.VMEM((64 * LS, 128), f32),
+        pltpu.VMEM((64 * LS, 128), bf16),
         pltpu.VMEM((LS, 8192), f32),
-        pltpu.SemaphoreType.DMA((4,)),
+        pltpu.SemaphoreType.DMA((8,)),
     ]
     anywhere = pl.BlockSpec(memory_space=pl.ANY)
     out_spec = whole((TP, 8, 256))

time: 141 us -> 142 us (level)
  no operation moved by 1% of the time
where the time goes in v8:
time: 142 us; the launch traced here: 141 us
  blocking collectives  134 us (94%)
  Pallas kernels  5.49 us (4%)
    all_to_all x9, blocking collectives, exchange(): return lax.all_to_all(array, axis, 0, 0, tiled=True)  134 us

profile of v8, /device:TPU:1, one launch (start us, length us, event | category | flops | bytes accessed | tf_op | source)
XLA Modules:
  0.0 141.1 jit_solution(18062711243977440959)
XLA Ops:
  0.6 0.0 copy-start
  0.6 1.5 %shard_map.131 = bf16[16,16,512]{2,1,0:T(8,128)(2,1)S(1)} custom-call(bf16[256,256]{1,0:T(8,128)(2,1)} %tokens.5, f32[2,256]{1,0:T(2,128)} %pre.5, bf16[2,64,256]{2,1,0:T(8,128)(2,1)} %bitcast.9, bf16[2,64,256]{2,1,0:T(8,128)(2,1)} %bitcast.12, bf16[2,256,128]{2,1,0:T(8,128)(2,1)} %wv.3, bf16[2,256,128]{2,1,0:T(8,128)(2,1)} %wg.3, ...), custom_call_target="tpu_custom_call" | custom-call | tf_op jit(solution)/shard_map/pallas_call | solution.py:258
  2.1 0.0 copy-start.1
  2.2 0.0 copy-start.3
  2.2 0.0 copy-start.4
  2.2 0.0 copy-start.8
  2.2 0.0 copy-start.10
  2.2 0.0 copy-start.11
  2.2 21.1 %all_to_all.45.got.first = bf16[16,16,512]{2,1,0:T(8,128)(2,1)S(1)} all-to-all(bf16[16,16,512]{2,1,0:T(8,128)(2,1)S(1)} %shard_map.131), channel_id=1, replica_groups=mesh['tp'=32,'dp'=16] {'dp'}, dimensions={0} | all-to-all | bytes 524288 | tf_op jit(solution)/shard_map/all_to_all | solution.py:236
  23.3 0.0 copy-done
  23.3 0.0 copy-done.1
  23.3 0.0 copy-done.3
  23.4 0.0 copy-done.4
  23.4 0.0 copy-done.8
  23.4 0.0 copy-done.10
  23.4 0.0 copy-done.11
  23.4 1.3 shard_map.132
  24.7 0.0 copy-start.7
  24.8 11.7 %all_to_all.46.mixed.mid = bf16[16,16,256]{2,1,0:T(8,128)(2,1)S(1)} all-to-all(bf16[16,16,256]{2,1,0:T(8,128)(2,1)S(1)} %get-tuple-element.8), channel_id=1, replica_groups=mesh['tp'=32,'dp'=16] {'dp'}, dimensions={0} | all-to-all | bytes 262144 | tf_op jit(solution)/shard_map/all_to_all | solution.py:236
  36.4 0.0 copy-done.7
  36.4 0.2 shard_map.133
  36.6 21.6 %all_to_all.47.arrived = bf16[32,8,256]{2,1,0:T(8,128)(2,1)S(1)} all-to-all(bf16[32,8,256]{2,1,0:T(8,128)(2,1)S(1)} %shard_map.133), channel_id=1, replica_groups=mesh['tp'=32,'dp'=16] {'tp'}, dimensions={0} | all-to-all | bytes 262144 | tf_op jit(solution)/shard_map/all_to_all | solution.py:236
  58.2 0.0 copy-start.6
  58.3 0.0 copy-start.2
  58.3 0.0 copy-start.5
  58.3 0.0 copy-start.9
  58.3 12.9 %all_to_all.48.full = bf16[32,8,256]{2,1,0:T(8,128)(2,1)S(1)} all-to-all(bf16[32,8,256]{2,1,0:T(8,128)(2,1)S(1)} %shard_map.134.own0), channel_id=1, replica_groups=mesh['tp'=32,'dp'=16] {'tp'}, dimensions={0} | all-to-all | bytes 262144 | tf_op jit(solution)/shard_map/all_to_all | solution.py:236
  71.3 0.0 copy-done.6
  71.3 0.0 copy-done.2
  71.3 0.0 copy-done.5
  71.3 0.0 copy-done.9
  71.3 0.5 shard_map.135
  71.8 19.6 %all_to_all.49.got = bf16[16,16,768]{2,1,0:T(8,128)(2,1)S(1)} all-to-all(bf16[16,16,768]{2,1,0:T(8,128)(2,1)S(1)} %shard_map.135), channel_id=1, replica_groups=mesh['tp'=32,'dp'=16] {'dp'}, dimensions={0} | all-to-all | bytes 786432 | tf_op jit(solution)/shard_map/all_to_all | solution.py:236
  91.4 1.5 %shard_map.136 = (f32[2,16,8192]{2,1,0:T(8,128)}, bf16[16,16,128]{2,1,0:T(8,128)(2,1)S(1)}) custom-call(bf16[16,16,768]{2,1,0:T(8,128)(2,1)S(1)} %all_to_all.49.got, bf16[16,16,512]{2,1,0:T(8,128)(2,1)S(1)} %all_to_all.45.got.first, bf16[16,16,256]{2,1,0:T(8,128)(2,1)S(1)} %all_to_all.46.mixed.mid, ...), custom_call_target="tpu_custom_call", output_to_operand_aliasing={{0}: (6, {})} | custom-call | tf_op jit(solution)/shard_map/pallas_call | solution.py:284
  92.8 10.5 %all_to_all.50.mixed = bf16[16,16,128]{2,1,0:T(8,128)(2,1)S(1)} all-to-all(bf16[16,16,128]{2,1,0:T(8,128)(2,1)S(1)} %get-tuple-element.10), channel_id=1, replica_groups=mesh['tp'=32,'dp'=16] {'dp'}, dimensions={0} | all-to-all | bytes 131072 | tf_op jit(solution)/shard_map/all_to_all | solution.py:236
  103.3 0.2 shard_map.137
  103.5 12.8 %all_to_all.51.arrived = bf16[32,8,256]{2,1,0:T(8,128)(2,1)S(1)} all-to-all(bf16[32,8,256]{2,1,0:T(8,128)(2,1)S(1)} %shard_map.137), channel_id=1, replica_groups=mesh['tp'=32,'dp'=16] {'tp'}, dimensions={0} | all-to-all | bytes 262144 | tf_op jit(solution)/shard_map/all_to_all | solution.py:236
  116.3 0.1 shard_map.138
  116.4 11.4 %all_to_all.52.got = bf16[16,8,128]{2,1,0:T(8,128)(2,1)S(1)} all-to-all(bf16[16,8,128]{2,1,0:T(8,128)(2,1)S(1)} %get-tuple-element.11), channel_id=1, replica_groups=mesh['tp'=32,'dp'=16] {'dp'}, dimensions={0} | all-to-all | bytes 65536 | tf_op jit(solution)/shard_map/all_to_all | solution.py:236
  127.8 0.2 shard_map.139
  128.0 12.4 %all_to_all.53 = bf16[32,8,256]{2,1,0:T(8,128)(2,1)S(1)} all-to-all(bf16[32,8,256]{2,1,0:T(8,128)(2,1)S(1)} %shard_map.139), channel_id=1, replica_groups=mesh['tp'=32,'dp'=16] {'tp'}, dimensions={0} | all-to-all | bytes 262144 | tf_op jit(solution)/shard_map/all_to_all | solution.py:236
  140.4 0.7 copy.17
  (1 shorter events, 0.0 us)
Async XLA Ops:
  0.6 22.7 %copy-start = (f32[2,16,8192]{2,1,0:T(8,128)S(1)}, f32[2,16,8192]{2,1,0:T(8,128)}, u32[]{:S(2)}) copy-start(f32[2,16,8192]{2,1,0:T(8,128)} %old.3) | copy-start | bytes 3145732
  2.1 21.2 %copy-start.1 = (bf16[256,256]{1,0:T(8,128)(2,1)S(1)}, bf16[256,256]{1,0:T(8,128)(2,1)}, u32[]{:S(2)}) copy-start(bf16[256,256]{1,0:T(8,128)(2,1)} %tokens.5) | copy-start | bytes 393220
  2.2 21.2 %copy-start.3 = (bf16[2,256,64]{1,2,0:T(8,128)(2,1)S(1)}, bf16[2,256,64]{1,2,0:T(8,128)(2,1)}, u32[]{:S(2)}) copy-start(bf16[2,256,64]{1,2,0:T(8,128)(2,1)} %param.15) | copy-start | bytes 196612
  2.2 21.2 %copy-start.4 = (bf16[2,256,64]{1,2,0:T(8,128)(2,1)S(1)}, bf16[2,256,64]{1,2,0:T(8,128)(2,1)}, u32[]{:S(2)}) copy-start(bf16[2,256,64]{1,2,0:T(8,128)(2,1)} %param.16) | copy-start | bytes 196612
  2.2 21.2 %copy-start.8 = (f32[2,256]{1,0:T(2,128)S(1)}, f32[2,256]{1,0:T(2,128)}, u32[]{:S(2)}) copy-start(f32[2,256]{1,0:T(2,128)} %pre.5) | copy-start | bytes 6148
  2.2 21.2 %copy-start.10 = (f32[2,64]{1,0:T(2,128)S(1)}, f32[2,64]{1,0:T(2,128)}, u32[]{:S(2)}) copy-start(f32[2,64]{1,0:T(2,128)} %bias.3) | copy-start | bytes 1540
  2.2 21.2 %copy-start.11 = (f32[2,128]{1,0:T(2,128)S(1)}, f32[2,128]{1,0:T(2,128)}, u32[]{:S(2)}) copy-start(f32[2,128]{1,0:T(2,128)} %gain.3) | copy-start | bytes 3076
  24.7 11.7 %copy-start.7 = (bf16[2,128,256]{2,1,0:T(8,128)(2,1)S(1)}, bf16[2,128,256]{2,1,0:T(8,128)(2,1)}, u32[]{:S(2)}) copy-start(bf16[2,128,256]{2,1,0:T(8,128)(2,1)} %wo.3) | copy-start | bytes 393220
  58.2 13.0 %copy-start.6 = (bf16[2,256,128]{2,1,0:T(8,128)(2,1)S(1)}, bf16[2,256,128]{2,1,0:T(8,128)(2,1)}, u32[]{:S(2)}) copy-start(bf16[2,256,128]{2,1,0:T(8,128)(2,1)} %wg.3) | copy-start | bytes 393220
  58.3 13.0 %copy-start.2 = (bf16[2,256,64]{1,2,0:T(8,128)(2,1)S(1)}, bf16[2,256,64]{1,2,0:T(8,128)(2,1)}, u32[]{:S(2)}) copy-start(bf16[2,256,64]{1,2,0:T(8,128)(2,1)} %param.19) | copy-start | bytes 196612
  58.3 12.9 %copy-start.5 = (bf16[2,256,128]{2,1,0:T(8,128)(2,1)S(1)}, bf16[2,256,128]{2,1,0:T(8,128)(2,1)}, u32[]{:S(2)}) copy-start(bf16[2,256,128]{2,1,0:T(8,128)(2,1)} %wv.3) | copy-start | bytes 393220
  58.3 12.9 %copy-start.9 = (f32[2,256]{1,0:T(2,128)S(1)}, f32[2,256]{1,0:T(2,128)}, u32[]{:S(2)}) copy-start(f32[2,256]{1,0:T(2,128)} %post.3) | copy-start | bytes 6148
